TPU v7x, 32 devices: a whole 2x2x4 slice. The times are simulated.
32 devices in a mesh: st: 8 (over z, x), tp: 4 (over y, core).
Axes of the slice: x: 2, y: 2, z: 4, core: 2. Of those that a mesh axis runs over, the one named last changes fastest.
Arguments:
- tokens: bfloat16 [4096, 2048], P('st'), may hold values from -6 to 6
- mix_query: bfloat16 [2048, 1024], P(None, 'tp'), may hold values from -0.125 to 0.125
- mix_key: bfloat16 [2048, 1024], P(None, 'tp'), may hold values from -0.125 to 0.125
- mix_value: bfloat16 [2048, 1024], P(None, 'tp'), may hold values from -0.125 to 0.125
- decay_lower_map: bfloat16 [2048, 64], replicated, may hold values from -0.125 to 0.125
- decay_upper_map: bfloat16 [64, 1024], P(None, 'tp'), may hold values from -1 to 1
- decay_base: float32 [1024], P('tp'), may hold values from -7.5 to -2.5
- decay_shift: float32 [4096, 16], P('st', 'tp'), may hold values from -3.8 to 9.8
- rate_lower_map: bfloat16 [2048, 64], replicated, may hold values from -0.125 to 0.125
- rate_upper_map: bfloat16 [64, 1024], P(None, 'tp'), may hold values from -0.75 to 0.75
- norm_gain: float32 [1024], P('tp'), may hold values from 0.1 to 1.9
- mix_out: bfloat16 [1024, 2048], P(None, 'tp'), may hold values from -0.1875 to 0.1875
- cross_query: bfloat16 [2048, 2048], P(None, 'tp'), may hold values from -0.125 to 0.125
- score_gain: float32 [2048], P('tp'), may hold values from 0.1 to 1.9
- passage_key: bfloat16 [2048, 2048], P(None, 'tp'), may hold values from -0.125 to 0.125
- passage_value: bfloat16 [2048, 2048], P(None, 'tp'), may hold values from -0.125 to 0.125
- cross_out: bfloat16 [2048, 2048], P(None, 'tp'), may hold values from -0.5 to 0.5
- gate_down: bfloat16 [2048, 128], replicated, may hold values from -0.125 to 0.125
- gate_up: bfloat16 [128, 2048], P(None, 'tp'), may hold values from -0.5 to 0.5
- store: bfloat16 [96, 96, 2048], P('st'), may hold values from -6 to 6
- passage_ids: int32 [64, 4], P('st'), may hold values from 0 to 95, as said below
Outputs:
- mixed: bfloat16 [4096, 2048], P('st', 'tp')
Inputs may be any that keep to these rules, and one draw needn't show every extreme that they name: `passage_ids`: among the 32 passages named by the rows of one sequence, at most 4 are held by one index of st (passage p by index p // 12); in every draw exactly 4 are held by the index before the sequence's own.
All inputs are finite; a program needn't handle non-finite values.
Results may differ from a plain program's by a relative error of at most 0.0075.
Values may be sent and summed in bfloat16 or wider, within the bound.
No kernel may reach another device: no remote copies, remote signals or barrier semaphores. Data moves between devices by JAX's collectives and lax.ppermute only.
A program may use at most 128 MiB of HBM per device.

v0:
```python
import jax
import jax.numpy as jnp
from jax import lax
from jax.sharding import PartitionSpec as P

XHEAD = 256
QBLOCK = 64
MBLOCK = 64


FLOAT32 = jnp.float32
BFLOAT = jnp.bfloat16
PRECISE = lax.Precision.HIGHEST


def rounded(values):
    return lax.optimization_barrier(values.astype(BFLOAT)).astype(FLOAT32)


def head_norm(values, head_size):
    shaped = values.reshape(values.shape[:-1] + (values.shape[-1] // head_size, head_size))
    scaled = shaped * lax.rsqrt(jnp.mean(shaped * shaped, axis=-1, keepdims=True) + 1e-06)
    return scaled.reshape(values.shape)


def pair_dots(left, right):
    return jnp.einsum("hsc,htc->hst", left, right, precision=PRECISE)


def apply_mat(matrix, vectors):
    return jnp.einsum("hst,htc->hsc", matrix, vectors, precision=PRECISE)


def block_step(state, inputs):
    query_vec, key_vec, value_vec, minus_key, rate_key, log_fade = inputs
    length = query_vec.shape[1]
    cumul_log = jnp.cumsum(log_fade, axis=1)
    before = cumul_log - log_fade
    block_end = cumul_log[:, -1:, :]
    row_idx = lax.broadcasted_iota(jnp.int32, (length, length), 0)
    col_idx = lax.broadcasted_iota(jnp.int32, (length, length), 1)
    strict = (col_idx < row_idx).astype(FLOAT32)
    upto_mask = (col_idx <= row_idx).astype(FLOAT32)
    minus_scaled = minus_key * jnp.exp(before)
    query_scaled = query_vec * jnp.exp(cumul_log)
    key_inverse = key_vec * jnp.exp(-cumul_log)
    rate_inverse = rate_key * jnp.exp(-cumul_log)
    key_pull = pair_dots(minus_scaled, key_inverse) * strict
    rate_pull = pair_dots(minus_scaled, rate_inverse) * strict
    key_read = pair_dots(query_scaled, key_inverse) * upto_mask
    rate_read = pair_dots(query_scaled, rate_inverse) * upto_mask
    solved = jnp.einsum("hsj,hij->hsi", minus_scaled, state, precision=PRECISE) + apply_mat(
        key_pull, value_vec
    )
    power_mat = rate_pull
    for repeat_idx in range((length - 1).bit_length()):
        solved = solved + apply_mat(power_mat, solved)
        power_mat = jnp.einsum("hst,htu->hsu", power_mat, power_mat, precision=PRECISE)
    outputs = (
        jnp.einsum("hsj,hij->hsi", query_scaled, state, precision=PRECISE)
        + apply_mat(key_read, value_vec)
        + apply_mat(rate_read, solved)
    )
    fade_out = jnp.exp(block_end - cumul_log)
    state = (
        state * jnp.exp(block_end)
        + jnp.einsum("hsi,hsj->hij", value_vec, key_vec * fade_out, precision=PRECISE)
        + jnp.einsum("hsi,hsj->hij", solved, rate_key * fade_out, precision=PRECISE)
    )
    return (state, outputs)


def mixer(
    tokens,
    mix_query,
    mix_key,
    mix_value,
    decay_lower_map,
    decay_upper_map,
    decay_base,
    decay_shift,
    rate_lower_map,
    rate_upper_map,
    norm_gain,
):
    tok_rows = tokens.shape[0]
    head_count = decay_shift.shape[1]
    mix_width = mix_query.shape[1]
    head_size = mix_width // head_count

    def project(weight):
        return rounded(jnp.dot(tokens, weight, preferred_element_type=FLOAT32))

    query_vec = project(mix_query)
    key_vec = project(mix_key)
    value_vec = project(mix_value)
    decay_low = jnp.tanh(jnp.dot(tokens, decay_lower_map, preferred_element_type=FLOAT32)).astype(
        BFLOAT
    )
    decay_pre = (
        decay_base
        + jnp.dot(decay_low, decay_upper_map, preferred_element_type=FLOAT32)
        + jnp.repeat(decay_shift, head_size, axis=1)
    )
    log_fade = -jnp.exp(-jax.nn.softplus(-decay_pre) - 0.5)
    rate_low = jnp.dot(tokens, rate_lower_map, preferred_element_type=FLOAT32).astype(BFLOAT)
    rate_gate = jax.nn.sigmoid(jnp.dot(rate_low, rate_upper_map, preferred_element_type=FLOAT32))

    def to_blocks(values):
        shaped = values.reshape(tok_rows // MBLOCK, MBLOCK, head_count, head_size)
        return shaped.transpose(0, 2, 1, 3)

    keyed = key_vec.reshape(tok_rows, head_count, head_size)
    unit_key = keyed * lax.rsqrt(jnp.sum(keyed * keyed, axis=-1, keepdims=True) + 1e-06)
    rate_key = unit_key * rate_gate.reshape(tok_rows, head_count, head_size)
    block_in = (
        to_blocks(query_vec),
        to_blocks(key_vec),
        to_blocks(value_vec),
        to_blocks(-unit_key),
        to_blocks(rate_key),
        to_blocks(log_fade),
    )
    state_zero = jnp.zeros((head_count, head_size, head_size), FLOAT32)
    _, head_out = lax.scan(block_step, state_zero, block_in)
    head_out = head_out.transpose(0, 2, 1, 3).reshape(tok_rows, head_count, head_size)
    centred = head_out - jnp.mean(head_out, axis=-1, keepdims=True)
    spread = jnp.mean(centred * centred, axis=-1, keepdims=True)
    normed = (centred * lax.rsqrt(spread + 0.00064)).reshape(tok_rows, mix_width)
    return (normed * norm_gain).astype(BFLOAT)


def local(
    tokens,
    mix_query,
    mix_key,
    mix_value,
    decay_lower_map,
    decay_upper_map,
    decay_base,
    decay_shift,
    rate_lower_map,
    rate_upper_map,
    norm_gain,
    mix_out,
    cross_query,
    score_gain,
    passage_key,
    passage_value,
    cross_out,
    gate_down,
    gate_up,
    store,
    passage_ids,
):
    mixer_heads = mixer(
        tokens,
        mix_query,
        mix_key,
        mix_value,
        decay_lower_map,
        decay_upper_map,
        decay_base,
        decay_shift,
        rate_lower_map,
        rate_upper_map,
        norm_gain,
    )
    tok_rows = tokens.shape[0]
    model_width = tokens.shape[1]
    owner_count = lax.axis_size("st")
    pass_dev = store.shape[0]
    passage_len = store.shape[1]
    cross_width = cross_query.shape[1]
    head_count = cross_width // XHEAD
    flat_ids = passage_ids.reshape(-1)
    slot_count = flat_ids.shape[0]
    capacity = max(2, -(-slot_count // owner_count))
    owner_of = flat_ids // pass_dev
    local_idx = flat_ids % pass_dev
    slot_order = jnp.arange(slot_count)
    earlier_same = (owner_of[:, None] == owner_of[None, :]) & (
        slot_order[None, :] < slot_order[:, None]
    )
    slot_rank = jnp.sum(earlier_same.astype(jnp.int32), axis=1)
    to_owner = owner_of[:, None] == jnp.arange(owner_count)[None, :]
    to_slot = slot_rank[:, None] == jnp.arange(capacity)[None, :]
    wanted = jnp.sum(
        jnp.where(to_owner[:, :, None] & to_slot[:, None, :], local_idx[:, None, None] + 1, 0),
        axis=0,
    )
    asked = lax.all_to_all(wanted, "st", split_axis=0, concat_axis=0, tiled=True)
    served = jnp.maximum(asked.reshape(-1) - 1, 0)
    where_from = owner_of * capacity + slot_rank
    row_share = passage_len // lax.axis_size("tp")
    own_rows = lax.dynamic_slice_in_dim(store, lax.axis_index("tp") * row_share, row_share, 1)
    outgoing = own_rows[served].reshape(owner_count, capacity, row_share, model_width)
    incoming = lax.all_to_all(outgoing, "st", split_axis=0, concat_axis=0, tiled=True)
    picked = incoming.reshape(owner_count * capacity, row_share, model_width)[where_from]
    piece = lax.all_gather(picked, "tp", axis=1, tiled=True)
    flat_rows = piece.reshape(-1, model_width)
    keyed = head_norm(
        jnp.dot(flat_rows, passage_key, preferred_element_type=FLOAT32), XHEAD
    ).astype(BFLOAT)
    valued = jnp.dot(flat_rows, passage_value, preferred_element_type=FLOAT32).astype(BFLOAT)
    joined = jnp.concatenate([keyed, valued], axis=-1)
    projected = joined.reshape(piece.shape[0], piece.shape[1], 2 * cross_width)
    block_count = tok_rows // QBLOCK
    queries = (
        head_norm(jnp.dot(tokens, cross_query, preferred_element_type=FLOAT32), XHEAD) * score_gain
    )
    queries = queries.astype(BFLOAT).reshape(block_count, QBLOCK, head_count, XHEAD)
    block_keys = projected[:, :, :cross_width].reshape(block_count, -1, head_count, XHEAD)
    block_values = projected[:, :, cross_width:].reshape(block_count, -1, head_count, XHEAD)
    scores = jnp.einsum(
        "bqhd,bkhd->bhqk", queries, block_keys, preferred_element_type=FLOAT32
    ) * XHEAD ** (-0.5)
    expon = jnp.exp(scores)
    weights = (expon / jnp.sum(expon, axis=-1, keepdims=True)).astype(BFLOAT)
    attended = jnp.einsum("bhqk,bkhd->bqhd", weights, block_values, preferred_element_type=FLOAT32)
    attended = attended.astype(BFLOAT).reshape(tok_rows, cross_width)
    shard_total = lax.axis_size("tp")
    out_cols = mix_out.shape[1]
    mix_rows = mix_out.reshape(shard_total, -1, out_cols)
    cross_rows = cross_out.reshape(shard_total, -1, out_cols)
    mixer_part = jnp.einsum(
        "ntc,ncd->td",
        lax.all_gather(mixer_heads[None], "tp", axis=0, tiled=True),
        mix_rows,
        preferred_element_type=FLOAT32,
    )
    cross_part = jnp.einsum(
        "ntc,ncd->td",
        lax.all_gather(attended[None], "tp", axis=0, tiled=True),
        cross_rows,
        preferred_element_type=FLOAT32,
    )
    gate_low = jnp.dot(tokens, gate_down, preferred_element_type=FLOAT32).astype(BFLOAT)
    gate_open = jax.nn.sigmoid(jnp.dot(gate_low, gate_up, preferred_element_type=FLOAT32))
    return (mixer_part + gate_open * cross_part).astype(BFLOAT)


def solution(mesh):
    placed = (
        P("st", None),
        P(None, "tp"),
        P(None, "tp"),
        P(None, "tp"),
        P(),
        P(None, "tp"),
        P("tp"),
        P("st", "tp"),
        P(),
        P(None, "tp"),
        P("tp"),
        P(None, "tp"),
        P(None, "tp"),
        P("tp"),
        P(None, "tp"),
        P(None, "tp"),
        P(None, "tp"),
        P(),
        P(None, "tp"),
        P("st", None, None),
        P("st", None),
    )
    return jax.shard_map(
        local, mesh=mesh, in_specs=placed, out_specs=P("st", "tp"), check_vma=False
    )
```

profile of v0, /device:TPU:0, one launch (start us, length us, event | category | flops | bytes accessed | tf_op | source)
XLA Modules:
  0.0 410.4 jit_solution(7020253587191063117)
XLA Ops:
  9.6 7.3 %all-to-all-start = ((s32[8,1,4]{2,1,0:T(1,128)}), s32[8,1,4]{2,1,0:T(1,128)S(1)}, u32[]{:S(2)}, u32[]{:S(2)}) async-start(s32[8,1,4]{2,1,0:T(1,128)} %copy.148), calls=%async_computation | async-start | bytes 8192 | tf_op jit(solution)/shard_map/all_to_all | solution.py:192
  16.9 1.3 constant_dynamic-slice_fusion
  18.3 5.1 %all-to-all-done = s32[8,1,4]{2,1,0:T(1,128)S(1)} async-done(((s32[8,1,4]{2,1,0:T(1,128)}), s32[8,1,4]{2,1,0:T(1,128)S(1)}, u32[]{:S(2)}, u32[]{:S(2)}) %all-to-all-start) | async-done | bytes 160 | tf_op jit(solution)/shard_map/all_to_all | solution.py:192
  23.4 2.4 gather_fusion
  25.9 4.4 %all-to-all-start.1 = ((bf16[8,4,24,2048]{3,2,1,0:T(8,128)(2,1)}), bf16[8,4,24,2048]{3,2,1,0:T(8,128)(2,1)}, u32[]{:S(2)}, u32[]{:S(2)}) async-start(bf16[8,4,24,2048]{3,2,1,0:T(8,128)(2,1)} %bitcast.271), calls=%async_computation.1 | async-start | bytes 6291456 | tf_op jit(solution)/shard_map/all_to_all | solution.py:198
  30.7 69.2 %all-to-all-done.1 = bf16[8,4,24,2048]{3,2,1,0:T(8,128)(2,1)} async-done(((bf16[8,4,24,2048]{3,2,1,0:T(8,128)(2,1)}), bf16[8,4,24,2048]{3,2,1,0:T(8,128)(2,1)}, u32[]{:S(2)}, u32[]{:S(2)}) %all-to-all-start.1) | async-done | bytes 3145760 | tf_op jit(solution)/shard_map/all_to_all | solution.py:198
  99.9 4.3 %gather_fusion.1 = bf16[32,24,2048]{2,1,0:T(8,128)(2,1)} fusion(bf16[32,24,2048]{2,1,0:T(8,128)(2,1)} %bitcast.15, s32[1024]{0:T(1024)S(1)} %pad_clamp_fusion), kind=kCustom, calls=%fused_computation.1 | custom fusion | bytes 6291584 | tf_op jit(solution)/shard_map/gather | solution.py:199
  104.3 4.0 copy.161
  108.3 4.2 %bitcast_reduce_fusion = (f32[512,2]{0,1:T(2,128)S(1)}, f32[512,512]{0,1:T(8,128)S(1)}) fusion(bf16[512,2048]{1,0:T(8,128)(2,1)} %param.23, bf16[2048,512]{1,0:T(8,128)(2,1)} %param.35), kind=kOutput, calls=%fused_computation.101 | convolution fusion | flops 1074265088 | bytes 5246976 | tf_op jit(solution)/shard_map/dot_general | solution.py:210
  112.7 1.5 reshape.416
  114.2 2.9 convolution_convert_fusion.2
  117.2 1.5 reshape.380
  119.1 2.7 fusion.52
  121.8 1.4 reshape.381
  123.5 2.9 fusion.65
  126.4 1.5 reshape.378
  127.9 2.6 convolution_convert_fusion.1
  130.5 1.4 reshape.394
  131.9 2.6 convolution_convert_fusion.3
  134.9 1.3 copy.133
  136.3 3.0 copy_bitcast_fusion
  139.3 2.1 fusion.59
  141.4 44.1 %all-gather.9.cloned.1.call-done = bf16[32,96,2048]{2,1,0:T(8,128)(2,1)} async-done(((bf16[32,24,2048]{2,1,0:T(8,128)(2,1)}), bf16[32,96,2048]{2,1,0:T(8,128)(2,1)}) %all-gather.9.cloned.1.call-update) | async-done | bytes 12582928 | tf_op jit(solution)/shard_map/all_gather | solution.py:200
  185.5 10.0 %multiply_reduce_fusion = (f32[3072,2]{0,1:T(2,128)S(1)}, f32[3072,2,256]{0,2,1:T(8,128)S(1)}) fusion(bf16[3072,2048,1]{1,0,2:T(8,128)(2,1)} %bitcast.282, bf16[2,256,2048]{2,1,0:T(8,128)(2,1)} %bitcast.276), kind=kOutput, calls=%fused_computation.63 | convolution fusion | flops 6445590528 | bytes 20996096 | tf_op jit(solution)/shard_map/dot_general | solution.py:203
  196.4 11.2 %convolution_convert_fusion = bf16[3072,512]{0,1:T(8,128)(2,1)} fusion(bf16[3072,2048]{1,0:T(8,128)(2,1)} %bitcast.283, bf16[2048,512]{1,0:T(8,128)(2,1)S(1)} %copy-done), kind=kOutput, calls=%fused_computation.64 | convolution fusion | flops 6444023808 | bytes 17825792 | tf_op jit(solution)/shard_map/dot_general | solution.py:205
  207.5 5.0 %pad_maximum_fusion = bf16[3072,1024]{0,1:T(8,128)(2,1)} fusion(bf16[3072,512]{0,1:T(8,128)(2,1)} %convolution_convert_fusion, bf16[3072,512]{0,1:T(8,128)(2,1)S(1)} %bitcast.272), kind=kLoop, calls=%fused_computation.61 | loop fusion | flops 12582912 | bytes 12582912 | tf_op jit(solution)/shard_map/concatenate | solution.py:206
  212.5 8.6 %copy.152 = bf16[3072,1024]{1,0:T(8,128)(2,1)} copy(bf16[3072,1024]{0,1:T(8,128)(2,1)} %pad_maximum_fusion) | data formatting | bytes 12582912 | tf_op jit(solution)/shard_map/concatenate | solution.py:206
  221.1 6.2 %fusion.76 = (bf16[32,96,512]{2,1,0:T(8,128)(2,1)}, bf16[32,96,512]{2,1,0:T(8,128)(2,1)}) fusion(bf16[32,96,1024]{2,1,0:T(8,128)(2,1)} %bitcast.270), kind=kLoop, calls=%fused_computation.152 | loop fusion | bytes 12582912 | tf_op jit(solution)/shard_map/slice | solution.py:213
  227.3 5.5 %reshape.391 = bf16[8,384,2,256]{3,2,1,0:T(2,128)(2,1)} reshape(bf16[32,96,512]{2,1,0:T(8,128)(2,1)} %get-tuple-element.105) | data formatting | bytes 6291456 | tf_op jit(solution)/shard_map/reshape | solution.py:213
  232.9 5.6 %reshape.389 = bf16[8,384,2,256]{3,2,1,0:T(2,128)(2,1)} reshape(bf16[32,96,512]{2,1,0:T(8,128)(2,1)} %get-tuple-element.106) | data formatting | bytes 6291456 | tf_op jit(solution)/shard_map/reshape | solution.py:214
  238.5 4.1 %multiply_exponential_fusion = f32[8,2,64,384]{3,2,1,0:T(8,128)} fusion(bf16[8,384,2,256]{3,2,1,0:T(2,128)(2,1)} %reshape.391, bf16[8,64,2,256]{1,0,3,2:T(8,128)(2,1)S(1)} %copy-done.5), kind=kOutput, calls=%fused_computation.70 | convolution fusion | flops 201719808 | bytes 5242880 | tf_op jit(solution)/shard_map/bqhd,bkhd->bhqk/dot_general | solution.py:215
  242.6 4.4 %fusion.47 = bf16[8,64,2,256]{3,1,2,0:T(8,128)(2,1)} fusion(bf16[8,384,2,256]{3,2,1,0:T(2,128)(2,1)} %reshape.389, f32[8,2,64,384]{3,2,1,0:T(8,128)} %multiply_exponential_fusion), kind=kOutput, calls=%fused_computation.82 | convolution fusion | flops 202376576 | bytes 5242880 | tf_op jit(solution)/shard_map/bhqk,bkhd->bqhd/dot_general | solution.py:220
  247.0 1.7 copy.157
  249.9 131.2 %while.13 = (s32[]{:T(128)}, f32[4,64,64]{2,1,0:T(8,128)S(1)}, f32[8,4,64,64]{3,2,1,0:T(8,128)S(1)}, f32[8,4,64,64]{3,2,1,0:T(8,128)S(1)}, f32[8,4,64,64]{2,3,1,...) while((s32[]{:T(128)}, f32[4,64,64]{2,1,0:T(8,128)S(1)}, ...), condition=%wide.region_3.4_spmd.clone, body=%wide.region_1.3_spmd.clone.sunk | while | flops 278528000 | bytes 7845517 | solution.py:125
  251.5 1.3 convolution_multiply_fusion.8
  254.1 1.3 convolution_multiply_fusion.9
  267.9 1.3 convolution_multiply_fusion.8
  270.5 1.3 convolution_multiply_fusion.9
  284.3 1.3 convolution_multiply_fusion.8
  286.9 1.3 convolution_multiply_fusion.9
  319.6 1.3 convolution_multiply_fusion.9
  336.0 1.3 convolution_multiply_fusion.9
  349.7 1.3 convolution_multiply_fusion.8
  366.1 1.3 convolution_multiply_fusion.8
  383.9 3.7 fusion.41
  387.7 4.9 %fusion.38 = f32[512,512]{1,0:T(8,128)} fusion(f32[512,512]{1,0:T(8,128)} %fusion.41, bf16[4,512,512]{2,1,0:T(8,128)(2,1)} %all-gather.7.cloned.1.call-done, bf16[4,512,512]{2,1,0:T(8,128)(2,1)} %bitcast.284), kind=kOutput, calls=%fused_computation.73 | convolution fusion | flops 1074003968 | bytes 6291456 | tf_op jit(solution)/shard_map/ntc,ncd->td/dot_general | solution.py:232
  392.6 8.2 %all-gather.5.cloned.1.call-done = bf16[4,512,256]{2,1,0:T(8,128)(2,1)} async-done(((bf16[1,512,256]{2,1,0:T(8,128)(2,1)}), bf16[4,512,256]{2,1,0:T(8,128)(2,1)}) %all-gather.5.cloned.1.call-update) | async-done | bytes 1048592 | tf_op jit(solution)/shard_map/all_gather | solution.py:228
  400.8 3.0 fusion.43
  (290 shorter events, 125.6 us)
Async XLA Ops:
  6.5 189.8 %copy-start = (bf16[2048,512]{1,0:T(8,128)(2,1)S(1)}, bf16[2048,512]{1,0:T(8,128)(2,1)}, u32[]{:S(2)}) copy-start(bf16[2048,512]{1,0:T(8,128)(2,1)} %param.38) | copy-start | bytes 6291460
  9.6 13.7 %all-to-all-start = ((s32[8,1,4]{2,1,0:T(1,128)}), s32[8,1,4]{2,1,0:T(1,128)S(1)}, u32[]{:S(2)}, u32[]{:S(2)}) async-start(s32[8,1,4]{2,1,0:T(1,128)} %copy.148), calls=%async_computation | async-start | bytes 8192 | tf_op jit(solution)/shard_map/all_to_all | solution.py:192
  25.9 74.0 %all-to-all-start.1 = ((bf16[8,4,24,2048]{3,2,1,0:T(8,128)(2,1)}), bf16[8,4,24,2048]{3,2,1,0:T(8,128)(2,1)}, u32[]{:S(2)}, u32[]{:S(2)}) async-start(bf16[8,4,24,2048]{3,2,1,0:T(8,128)(2,1)} %bitcast.271), calls=%async_computation.1 | async-start | bytes 6291456 | tf_op jit(solution)/shard_map/all_to_all | solution.py:198
  30.3 155.2 %all-gather.9.cloned.1.call-start = ((), (), s32[]{:S(2)}) async-start(), calls=%async_computation.4 | async-start | bytes 15728640 | tf_op jit(solution)/shard_map/all_gather | solution.py:200
  104.2 283.5 %all-gather.7.cloned.1.call-start = ((), (), s32[]{:S(2)}) async-start(), calls=%async_computation.3 | async-start | bytes 2621440 | tf_op jit(solution)/shard_map/all_gather | solution.py:234
  108.3 4.2 %copy-start.7 = (f32[512]{0:T(512)S(1)}, f32[512]{0:T(512)}, u32[]{:S(2)}) copy-start(f32[512]{0:T(512)} %param.36) | copy-start | bytes 6148
  117.2 1.9 copy-start.11
  119.0 4.2 %copy-start.6 = (f32[512,4]{0,1:T(4,128)S(1)}, f32[512,4]{0,1:T(4,128)}, u32[]{:S(2)}) copy-start(f32[512,4]{0,1:T(4,128)} %param.30) | copy-start | bytes 24580
  121.8 1.7 copy-start.12
  136.3 3.0 copy-start.3
  136.3 3.0 copy-start.4
  232.9 5.6 %copy-start.5 = (bf16[8,64,2,256]{1,0,3,2:T(8,128)(2,1)S(1)}, bf16[8,64,2,256]{1,0,3,2:T(8,128)(2,1)}, u32[]{:S(2)}) copy-start(bf16[8,64,2,256]{1,0,3,2:T(8,128)(2,1)} %reshape.416) | copy-start | bytes 1572868
  247.0 2.9 copy-start.2
  249.8 151.0 %all-gather.5.cloned.1.call-start = ((), (), s32[]{:S(2)}) async-start(), calls=%async_computation.2 | async-start | bytes 1310720 | tf_op jit(solution)/shard_map/all_gather | solution.py:228
  382.1 0.8 copy-start.8
  382.6 1.3 copy-start.10
  382.6 1.3 copy-start.13
  387.6 13.1 %copy-start.9 = (bf16[1024,512]{1,0:T(8,128)(2,1)S(1)}, bf16[1024,512]{1,0:T(8,128)(2,1)}, u32[]{:S(2)}) copy-start(bf16[1024,512]{1,0:T(8,128)(2,1)} %param.34) | copy-start | bytes 3145732
  387.7 16.2 %copy-start.1 = (bf16[2048,512]{1,0:T(8,128)(2,1)S(1)}, bf16[2048,512]{1,0:T(8,128)(2,1)}, u32[]{:S(2)}) copy-start(bf16[2048,512]{1,0:T(8,128)(2,1)} %param.38) | copy-start | bytes 6291460
Sparse Core Ops, SparseCore 0:
  104.3 81.1 all-gather.8
  249.9 22.5 all-gather.6
  384.0 16.6 all-gather.4
where the time goes:
time: 413 us; the launch traced here: 410 us
  matrix products  187 us (45%)
  waiting for transfers between devices  127 us (31%)
  local copies, waits for them, and re-layouts  57 us (14%)
  between operations  13.5 us (3%)
  other arithmetic  12.5 us (3%)
  starting transfers between devices  11.8 us (3%)
    all_to_all x1, waiting for transfers between devices, local(): lax.all_to_all(outgoing, 'st', split_axis=0, concat_axis=0, tiled=True)  69.2 us
    all_gather x1, waiting for transfers between devices, local(): piece = lax.all_gather(picked, 'tp', axis=1, tiled=True)  44.1 us
    dot_general x32, matrix products, pair_dots(): return jnp.einsum('hsc,htc->hst', left, right, precision=PRECISE)  42.7 us
    dot_general x72, matrix products, apply_mat(): return jnp.einsum('hst,htc->hsc', matrix, vectors, precision=PRECISE)  34.4 us
    dot_general x1, matrix products, local(): jnp.dot(flat_rows, passage_value, preferred_element_type=FLOAT32)  11.2 us
    dot_general x8, matrix products, block_step(): jnp.einsum('hsi,hsj->hij', solved, rate_key * fade_out, precision=PRECISE)  10.4 us
    dot_general x40, matrix products, block_step(): jnp.einsum('hst,htu->hsu', power_mat, power_mat, precision=PRECISE)  10.2 us
    dot_general x8, matrix products, block_step(): jnp.einsum('hsj,hij->hsi', query_scaled, state, precision=PRECISE)  10.1 us
  transfers between devices with their start and end apart: 5, of which 4 were waited for; matrix products, arithmetic and copies ran while one was open for 44% of the time, Pallas kernels for 0%

commit v1 on v0

v1 whole, which is shorter than its diff:
```python
import functools
import jax
import jax.numpy as jnp
from jax import lax
from jax.experimental import pallas as pl
from jax.experimental.pallas import tpu as pltpu
from jax.sharding import PartitionSpec as P

XHEAD = 256
QBLOCK = 64
MBLOCK = 64
RHEAD = 64
LROWS = 16

FLOAT32 = jnp.float32
BFLOAT = jnp.bfloat16
PRECISE = lax.Precision.HIGHEST
VMEM = pltpu.VMEM
SMEM = pltpu.SMEM
NT = (((1,), (1,)), ((), ()))
NN = (((1,), (0,)), ((), ()))
TN = (((0,), (0,)), ((), ()))


def dot(left, right, dims=NN, precision=None):
    return lax.dot_general(left, right, dims, precision=precision, preferred_element_type=FLOAT32)


def iota(shape, dim):
    return lax.broadcasted_iota(jnp.int32, shape, dim)


def whole(count):
    return [pl.BlockSpec(memory_space=VMEM)] * count


def table_kernel(pass_dev, per_block, ids_ref, want_ref, blk_ref, own_ref, rank_ref, fill_ref):
    owners, capacity = want_ref.shape
    slots = ids_ref.shape[0] * ids_ref.shape[1]

    def clear(o, carry):
        fill_ref[o] = 0
        for r in range(capacity):
            want_ref[o, r] = 0
            blk_ref[o, r] = 0
        return carry

    lax.fori_loop(0, owners, clear, 0)

    def put(n, carry):
        passage = ids_ref[n // per_block, n % per_block]
        owner = passage // pass_dev
        rank = fill_ref[owner]
        fill_ref[owner] = rank + 1
        own_ref[n] = owner
        rank_ref[n] = rank
        want_ref[owner, rank] = passage - owner * pass_dev
        blk_ref[owner, rank] = n // per_block
        return carry

    lax.fori_loop(0, slots, put, 0)


def make_tables(passage_ids, owners, capacity, pass_dev):
    slots = passage_ids.shape[0] * passage_ids.shape[1]
    smem = pl.BlockSpec(memory_space=SMEM)
    return pl.pallas_call(
        functools.partial(table_kernel, pass_dev, passage_ids.shape[1]),
        out_shape=[
            jax.ShapeDtypeStruct((owners, capacity), jnp.int32),
            jax.ShapeDtypeStruct((owners, capacity), jnp.int32),
            jax.ShapeDtypeStruct((slots,), jnp.int32),
            jax.ShapeDtypeStruct((slots,), jnp.int32),
        ],
        in_specs=[smem],
        out_specs=[smem] * 4,
        scratch_shapes=[SMEM((owners,), jnp.int32)],
        name="tables",
    )(passage_ids)


def query_kernel(blk_ref, tok_ref, w_ref, gain_ref, out_ref, q_ref):
    width = w_ref.shape[1]
    for h in range(width // XHEAD):
        cols = slice(h * XHEAD, (h + 1) * XHEAD)
        raw = dot(tok_ref[...], w_ref[:, cols])
        scale = lax.rsqrt(jnp.mean(raw * raw, axis=-1, keepdims=True) + 1e-06)
        q_ref[:, cols] = (raw * scale * gain_ref[:, cols]).astype(BFLOAT)
    owners, capacity = blk_ref.shape

    def copy(o, carry):
        for r in range(capacity):
            start = pl.multiple_of(blk_ref[o, r] * QBLOCK, QBLOCK)
            out_ref[o, r * QBLOCK : (r + 1) * QBLOCK, :] = q_ref[pl.ds(start, QBLOCK), :]
        return carry

    lax.fori_loop(0, owners, copy, 0)


def make_queries(blk, tokens, cross_query, score_gain):
    owners, capacity = blk.shape
    width = cross_query.shape[1]
    return pl.pallas_call(
        query_kernel,
        out_shape=jax.ShapeDtypeStruct((owners, capacity * QBLOCK, width), BFLOAT),
        in_specs=[pl.BlockSpec(memory_space=SMEM)] + whole(3),
        out_specs=pl.BlockSpec(memory_space=VMEM),
        scratch_shapes=[VMEM((tokens.shape[0], width), BFLOAT)],
        name="queries",
    )(blk, tokens, cross_query, score_gain.reshape(1, -1))


def keyval_kernel(rows_ref, wk_ref, wv_ref, k_ref, v_ref):
    width = wk_ref.shape[1]
    rows = rows_ref[...]
    for h in range(width // XHEAD):
        cols = slice(h * XHEAD, (h + 1) * XHEAD)
        raw = dot(rows, wk_ref[:, cols])
        scale = lax.rsqrt(jnp.mean(raw * raw, axis=-1, keepdims=True) + 1e-06)
        k_ref[:, cols] = (raw * scale).astype(BFLOAT)
        v_ref[:, cols] = dot(rows, wv_ref[:, cols]).astype(BFLOAT)


def make_keyvals(store, passage_key, passage_value):
    pass_dev, plen, model = store.shape
    width = passage_key.shape[1]
    group = max(g for g in range(1, 5) if pass_dev % g == 0)
    tile = group * plen
    weight = pl.BlockSpec((model, width), lambda i: (0, 0))
    out = pl.BlockSpec((tile, width), lambda i: (i, 0))
    shape = jax.ShapeDtypeStruct((pass_dev * plen, width), BFLOAT)
    return pl.pallas_call(
        keyval_kernel,
        grid=(pass_dev // group,),
        out_shape=[shape, shape],
        in_specs=[pl.BlockSpec((tile, model), lambda i: (i, 0)), weight, weight],
        out_specs=[out, out],
        name="keyvals",
    )(store.reshape(-1, model), passage_key, passage_value)


def project_kernel(
    tok_ref, mq_ref, mk_ref, mv_ref, dl_ref, rl_ref, gd_ref, du_ref, ru_ref, gu_ref,
    base_ref, shift_ref,
    q_ref, k_ref, v_ref, u_ref, rk_ref, lf_ref, gate_ref,
):
    tokens = tok_ref[...]
    width = mq_ref.shape[1]
    rank = dl_ref.shape[1]
    lows = dot(tokens, jnp.concatenate([dl_ref[...], rl_ref[...], gd_ref[...]], axis=1))
    decay_low = jnp.tanh(lows[:, :rank]).astype(BFLOAT)
    rate_low = lows[:, rank : 2 * rank].astype(BFLOAT)
    gate_low = lows[:, 2 * rank :].astype(BFLOAT)
    gate_ref[...] = jax.nn.sigmoid(dot(gate_low, gu_ref[...]))
    pre = base_ref[...] + dot(decay_low, du_ref[...])
    head = iota(pre.shape, 1) // RHEAD
    shift = jnp.zeros_like(pre)
    for h in range(width // RHEAD):
        shift = jnp.where(head == h, shift_ref[:, h : h + 1], shift)
    lf_ref[...] = -jax.nn.sigmoid(pre + shift) * (2.718281828459045 ** -0.5)
    q_ref[...] = dot(tokens, mq_ref[...]).astype(BFLOAT)
    v_ref[...] = dot(tokens, mv_ref[...]).astype(BFLOAT)
    key = dot(tokens, mk_ref[...]).astype(BFLOAT)
    k_ref[...] = key
    key = key.astype(FLOAT32)
    same = (iota((width, width), 0) // RHEAD == iota((width, width), 1) // RHEAD).astype(FLOAT32)
    unit = key * lax.rsqrt(dot(key * key, same, precision=PRECISE) + 1e-06)
    u_ref[...] = unit
    rk_ref[...] = unit * jax.nn.sigmoid(dot(rate_low, ru_ref[...]))


def project(tokens, mix_query, mix_key, mix_value, decay_lower, decay_upper, decay_base,
            decay_shift, rate_lower, rate_upper, gate_down, gate_up):
    rows = tokens.shape[0]
    width = mix_query.shape[1]
    half = jax.ShapeDtypeStruct((rows, width), BFLOAT)
    full = jax.ShapeDtypeStruct((rows, width), FLOAT32)
    return pl.pallas_call(
        project_kernel,
        out_shape=[half, half, half, full, full, full,
                   jax.ShapeDtypeStruct((rows, gate_up.shape[1]), FLOAT32)],
        in_specs=whole(12),
        out_specs=whole(7),
        name="project",
    )(tokens, mix_query, mix_key, mix_value, decay_lower, rate_lower, gate_down,
      decay_upper, rate_upper, gate_up, decay_base.reshape(1, -1), decay_shift)


def spread(value):
    rows, width = value.shape
    heads = width // RHEAD
    tiled = jnp.concatenate([value] * heads, axis=0)
    keep = iota(tiled.shape, 0) // rows == iota(tiled.shape, 1) // RHEAD
    return jnp.where(keep, tiled, jnp.zeros_like(tiled))


def fold(value):
    width = value.shape[1]
    keep = iota(value.shape, 0) // RHEAD == iota(value.shape, 1) // RHEAD
    kept = jnp.where(keep, value, jnp.zeros_like(value))
    total = kept[:RHEAD]
    for h in range(1, width // RHEAD):
        total = total + kept[h * RHEAD : (h + 1) * RHEAD]
    return total


def prepare_chunk(query, key, value, unit, rate_key, log_fade):
    length, width = query.shape
    mm = functools.partial(dot, precision=PRECISE)
    lower = (iota((length, length), 1) <= iota((length, length), 0)).astype(FLOAT32)
    cumul = mm(lower, log_fade)
    before = cumul - log_fade
    end = cumul[length - 1 :, :]
    grown = jnp.exp(-cumul)
    pulled = -unit * jnp.exp(before)
    read = query * jnp.exp(cumul)
    both = jnp.concatenate([pulled, read], axis=0)
    row = iota((length, width), 0)
    col = iota((length, width), 1) % RHEAD
    from_key = mm(both, spread(key * grown), NT)
    from_rate = mm(both, spread(rate_key * grown), NT)
    key_pull = jnp.where(col < row, from_key[:length], 0.0)
    rate_pull = jnp.where(col < row, from_rate[:length], 0.0)
    key_read = jnp.where(col <= row, from_key[length:], 0.0)
    rate_read = jnp.where(col <= row, from_rate[length:], 0.0)

    def pick(size):
        keep = (row // (2 * size) == col // (2 * size)) & ((row // size) % 2 == 1)
        return jnp.where(keep & ((col // size) % 2 == 0), rate_pull, 0.0)

    inverse = (row == col).astype(FLOAT32) + pick(1)
    size = 2
    while size < length:
        inverse = inverse + mm(mm(inverse, spread(pick(size))), spread(inverse))
        size *= 2
    wide_value = spread(value)
    moved = mm(inverse, spread(pulled))
    base = mm(inverse, spread(mm(key_pull, wide_value)))
    query_end = read + mm(rate_read, spread(moved))
    out_base = mm(key_read, wide_value) + mm(rate_read, spread(base))
    left = jnp.exp(end - cumul)
    key_left = key * left
    rate_left = rate_key * left
    fade = (iota((RHEAD, width), 0) == iota((RHEAD, width), 1) % RHEAD).astype(FLOAT32) * jnp.exp(end)
    step = fade + fold(mm(moved, rate_left, TN))
    add = fold(mm(value, key_left, TN) + mm(base, rate_left, TN))
    return query_end, out_base, step, add


def prepare_kernel(q_ref, k_ref, v_ref, u_ref, rk_ref, lf_ref, qe_ref, ob_ref, st_ref, ad_ref):
    for c in range(q_ref.shape[0] // MBLOCK):
        rows = slice(c * MBLOCK, (c + 1) * MBLOCK)
        outs = prepare_chunk(
            q_ref[rows].astype(FLOAT32), k_ref[rows].astype(FLOAT32), v_ref[rows].astype(FLOAT32),
            u_ref[rows], rk_ref[rows], lf_ref[rows])
        for ref, out in zip((qe_ref, ob_ref, st_ref, ad_ref), outs):
            ref[rows] = out


def prepare(query, key, value, unit, rate_key, log_fade):
    rows, width = query.shape
    tile = 2 * MBLOCK
    spec = pl.BlockSpec((tile, width), lambda i: (i, 0))
    full = jax.ShapeDtypeStruct((rows, width), FLOAT32)
    return pl.pallas_call(
        prepare_kernel,
        grid=(rows // tile,),
        out_shape=[full] * 4,
        in_specs=[spec] * 6,
        out_specs=[spec] * 4,
        name="prepare",
    )(query, key, value, unit, rate_key, log_fade)


def scan_kernel(qe_ref, ob_ref, st_ref, ad_ref, gain_ref, out_ref, state_ref):
    width = qe_ref.shape[1]
    mm = functools.partial(dot, precision=PRECISE)
    mean_of = (iota((width, width), 0) // RHEAD == iota((width, width), 1) // RHEAD).astype(FLOAT32)
    state_ref[...] = jnp.zeros_like(state_ref)

    def step(c, carry):
        rows = pl.ds(pl.multiple_of(c * MBLOCK, MBLOCK), MBLOCK)
        state = state_ref[...]
        out = mm(qe_ref[rows, :], spread(state), NT) + ob_ref[rows, :]
        state_ref[...] = mm(state, spread(st_ref[rows, :])) + ad_ref[rows, :]
        centred = out - mm(out, mean_of) * (1.0 / RHEAD)
        var = mm(centred * centred, mean_of) * (1.0 / RHEAD)
        out_ref[rows, :] = (centred * lax.rsqrt(var + 0.00064) * gain_ref[...]).astype(BFLOAT)
        return carry

    lax.fori_loop(0, qe_ref.shape[0] // MBLOCK, step, 0)


def scan(query_end, out_base, step, add, norm_gain):
    rows, width = query_end.shape
    return pl.pallas_call(
        scan_kernel,
        out_shape=jax.ShapeDtypeStruct((rows, width), BFLOAT),
        in_specs=whole(5),
        out_specs=pl.BlockSpec(memory_space=VMEM),
        scratch_shapes=[VMEM((RHEAD, width), FLOAT32)],
        name="scan",
    )(query_end, out_base, step, add, norm_gain.reshape(1, -1))


def attend_kernel(plen, asked_ref, q_ref, k_ref, v_ref, out_ref):
    seq = pl.program_id(0)
    width = q_ref.shape[2]
    heads = width // XHEAD
    capacity = asked_ref.shape[2]
    ones = jnp.ones((8, plen), BFLOAT)
    sums = jnp.zeros((LROWS, QBLOCK), FLOAT32)
    rowid = iota((LROWS, QBLOCK), 0)
    for r in range(capacity):
        rows = pl.ds(pl.multiple_of(asked_ref[seq, 0, r] * plen, plen), plen)
        mine = slice(r * QBLOCK, (r + 1) * QBLOCK)
        for h in range(heads):
            cols = slice(h * XHEAD, (h + 1) * XHEAD)
            scores = dot(q_ref[0, mine, cols], k_ref[rows, cols], NT) * XHEAD ** (-0.5)
            expon = jnp.exp(scores).astype(BFLOAT)
            out_ref[0, mine, cols] = dot(expon, v_ref[rows, cols]).astype(BFLOAT)
            total = dot(ones, expon, NT)[:1]
            high = total.astype(BFLOAT).astype(FLOAT32)
            where = 2 * (r * heads + h)
            sums = jnp.where(rowid == where, high, sums)
            sums = jnp.where(rowid == where + 1, total - high, sums)
    out_ref[0, capacity * QBLOCK :, :] = jnp.zeros((LROWS, width), BFLOAT)
    out_ref[0, capacity * QBLOCK :, :QBLOCK] = sums.astype(BFLOAT)


def attend(asked, queries, keys, values, plen):
    owners, qrows, width = queries.shape
    everything = pl.BlockSpec(keys.shape, lambda i, a: (0, 0))
    return pl.pallas_call(
        functools.partial(attend_kernel, plen),
        grid_spec=pltpu.PrefetchScalarGridSpec(
            num_scalar_prefetch=1,
            grid=(owners,),
            in_specs=[pl.BlockSpec((1, qrows, width), lambda i, a: (i, 0, 0)), everything, everything],
            out_specs=pl.BlockSpec((1, qrows + LROWS, width), lambda i, a: (i, 0, 0)),
        ),
        out_shape=jax.ShapeDtypeStruct((owners, qrows + LROWS, width), BFLOAT),
        name="attend",
    )(asked, queries, keys, values)


def combine_kernel(per_block, own_ref, rank_ref, part_ref, out_ref):
    width = part_ref.shape[2]
    heads = width // XHEAD
    qrows = part_ref.shape[1] - LROWS
    rowid = iota((LROWS, QBLOCK), 0)
    selrow = iota((LROWS, XHEAD), 0)

    def block(b, carry):
        total = jnp.zeros((QBLOCK, width), FLOAT32)
        sums = jnp.zeros((LROWS, QBLOCK), FLOAT32)
        for i in range(per_block):
            owner = own_ref[b * per_block + i]
            rank = rank_ref[b * per_block + i]
            rows = pl.ds(pl.multiple_of(rank * QBLOCK, QBLOCK), QBLOCK)
            total = total + part_ref[owner, rows, :].astype(FLOAT32)
            lines = part_ref[owner, qrows:, :QBLOCK].astype(FLOAT32)
            sums = sums + jnp.where(rowid // (2 * heads) == rank, lines, 0.0)
        mine = pl.ds(pl.multiple_of(b * QBLOCK, QBLOCK), QBLOCK)
        for h in range(heads):
            cols = slice(h * XHEAD, (h + 1) * XHEAD)
            choose = ((selrow // 2) % heads == h).astype(FLOAT32)
            weight = dot(sums, choose, TN, precision=PRECISE)
            out_ref[mine, cols] = (total[:, cols] / weight).astype(BFLOAT)
        return carry

    lax.fori_loop(0, out_ref.shape[0] // QBLOCK, block, 0)


def combine(own, rank, parts, rows, per_block):
    smem = pl.BlockSpec(memory_space=SMEM)
    return pl.pallas_call(
        functools.partial(combine_kernel, per_block),
        out_shape=jax.ShapeDtypeStruct((rows, parts.shape[2]), BFLOAT),
        in_specs=[smem, smem] + whole(1),
        out_specs=pl.BlockSpec(memory_space=VMEM),
        name="combine",
    )(own, rank, parts)


def gathered_dot(pieces, me, w_ref):
    total = None
    for j, piece in enumerate(pieces):
        depth = piece.shape[1]
        rows = pl.ds(pl.multiple_of((me ^ j) * depth, depth), depth)
        part = dot(piece[...], w_ref[rows, :])
        total = part if total is None else total + part
    return total


def mixer_out_kernel(me_ref, *refs):
    *pieces, w_ref, out_ref = refs
    out_ref[...] = gathered_dot(pieces, me_ref[0], w_ref)


def final_kernel(me_ref, *refs):
    *pieces, w_ref, gate_ref, mixer_ref, out_ref = refs
    cross = gathered_dot(pieces, me_ref[0], w_ref)
    out_ref[...] = (mixer_ref[...] + gate_ref[...] * cross).astype(BFLOAT)


def over_tp(body, me, pieces, others, dtype, name):
    shape = (pieces[0].shape[0], others[0].shape[1])
    return pl.pallas_call(
        body,
        out_shape=jax.ShapeDtypeStruct(shape, dtype),
        in_specs=[pl.BlockSpec(memory_space=SMEM)] + whole(len(pieces) + len(others)),
        out_specs=pl.BlockSpec(memory_space=VMEM),
        name=name,
    )(me, *pieces, *others)


def gather_tp(piece, count):
    pieces = {0: piece}
    bit = count // 2
    while bit:
        pairs = [(i, i ^ bit) for i in range(count)]
        for j in list(pieces):
            pieces[j ^ bit] = lax.ppermute(pieces[j], "tp", pairs)
        bit //= 2
    return [pieces[j] for j in range(count)]


def local(
    tokens, mix_query, mix_key, mix_value, decay_lower_map, decay_upper_map, decay_base,
    decay_shift, rate_lower_map, rate_upper_map, norm_gain, mix_out, cross_query, score_gain,
    passage_key, passage_value, cross_out, gate_down, gate_up, store, passage_ids,
):
    rows = tokens.shape[0]
    owners = lax.axis_size("st")
    shards = lax.axis_size("tp")
    pass_dev, plen, _ = store.shape
    per_block = passage_ids.shape[1]
    slots = passage_ids.shape[0] * per_block
    capacity = max(2, -(-slots // owners))
    me = lax.axis_index("tp").astype(jnp.int32).reshape(1)

    want, blk, own, rank = make_tables(passage_ids, owners, capacity, pass_dev)
    asked = lax.all_to_all(want[:, None, :], "st", split_axis=0, concat_axis=0, tiled=True)
    queries = make_queries(blk, tokens, cross_query, score_gain)
    queries = lax.all_to_all(queries, "st", split_axis=0, concat_axis=0, tiled=True)
    keys, values = make_keyvals(store, passage_key, passage_value)
    *mixer_in, gate = project(
        tokens, mix_query, mix_key, mix_value, decay_lower_map, decay_upper_map, decay_base,
        decay_shift, rate_lower_map, rate_upper_map, gate_down, gate_up)
    prepared = prepare(*mixer_in)
    parts = attend(asked, queries, keys, values, plen)
    parts = lax.all_to_all(parts, "st", split_axis=0, concat_axis=0, tiled=True)
    mixer_heads = scan(*prepared, norm_gain)
    mixer_part = over_tp(mixer_out_kernel, me, gather_tp(mixer_heads, shards), [mix_out],
                         FLOAT32, "mixer_out")
    attended = combine(own, rank, parts, rows, per_block)
    return over_tp(final_kernel, me, gather_tp(attended, shards), [cross_out, gate, mixer_part],
                   BFLOAT, "final")


def solution(mesh):
    placed = (
        P("st", None), P(None, "tp"), P(None, "tp"), P(None, "tp"), P(), P(None, "tp"), P("tp"),
        P("st", "tp"), P(), P(None, "tp"), P("tp"), P(None, "tp"), P(None, "tp"), P("tp"),
        P(None, "tp"), P(None, "tp"), P(None, "tp"), P(), P(None, "tp"), P("st", None, None),
        P("st", None),
    )
    return jax.shard_map(
        local, mesh=mesh, in_specs=placed, out_specs=P("st", "tp"), check_vma=False
    )
```

time: 413 us -> 234 us (0.57)
  matrix products: 187 us -> 0 us
  Pallas kernels: 0 us -> 109 us
  waiting for transfers between devices: 127 us -> 46.8 us
  blocking collectives: 0 us -> 55.3 us
  local copies, waits for them, and re-layouts: 57 us -> 7.8 us
  between operations: 13.5 us -> 0.08 us
  other arithmetic: 12.5 us -> 0 us
    dot_general x189 -> x0, matrix products: 187 us -> none  [the longest x32 42.7 us: pair_dots(): return jnp.einsum('hsc,htc->hst', left, right, precision=PRECISE)]
    pallas_call x0 -> x10, Pallas kernels: none -> 109 us  [the longest x1 47.9 us: prepare(): pl.pallas_call(prepare_kernel, grid=(rows // tile,), out_shape=[full] * 4...]
    all_to_all x0 -> x1, blocking collectives: none -> 55.3 us  [local(): parts = lax.all_to_all(parts, 'st', split_axis=0, concat_axis=0, tiled=True)]
    all_gather x3 -> x0, waiting for transfers between devices: 52.3 us -> none  [the longest x1 44.1 us: local(): piece = lax.all_gather(picked, 'tp', axis=1, tiled=True)]
    all_to_all x2, waiting for transfers between devices: 74.3 us -> 39.8 us  [the longest x1 38.4 us: local(): lax.all_to_all(queries, 'st', split_axis=0, concat_axis=0, tiled=True)]
    reshape x8 -> x0, local copies, waits for them, and re-layouts: 17.5 us -> none  [the longest x1 5.58 us: local(): projected[:, :, cross_width:].reshape(block_count, -1, head_count, XHEAD)]
    concatenate x1 -> x0, local copies, waits for them, and re-layouts: 8.62 us -> none  [local(): joined = jnp.concatenate([keyed, valued], axis=-1)]
    unnamed x28, local copies, waits for them, and re-layouts: 0.06 us -> 7.8 us
  transfers between devices with their start and end apart: 5 -> 8, of which waited for: 4 -> 4; matrix products, arithmetic and copies ran while one was open for 44% -> 1% of each run, Pallas kernels for 0% -> 36%
where the time goes in v1:
time: 234 us; the launch traced here: 233 us
  Pallas kernels  109 us (47%)
  blocking collectives  55.3 us (24%)
  waiting for transfers between devices  46.8 us (20%)
  starting transfers between devices  14.5 us (6%)
  local copies, waits for them, and re-layouts  7.8 us (3%)
    all_to_all x1, blocking collectives, local(): parts = lax.all_to_all(parts, 'st', split_axis=0, concat_axis=0, tiled=True)  55.3 us
    pallas_call x1, Pallas kernels, prepare(): pl.pallas_call(prepare_kernel, grid=(rows // tile,), out_shape=[full] * 4...  47.9 us
    all_to_all x1, waiting for transfers between devices, local(): lax.all_to_all(queries, 'st', split_axis=0, concat_axis=0, tiled=True)  38.4 us
    pallas_call x1, Pallas kernels, attend(): pl.pallas_call(functools.partial(attend_kernel, plen), grid_spec=pltpu.Pr...  11.4 us
    pallas_call x1, Pallas kernels, scan(): pl.pallas_call(scan_kernel, out_shape=jax.ShapeDtypeStruct((rows, width),...  11.1 us
    pallas_call x1, Pallas kernels, make_keyvals(): pl.pallas_call(keyval_kernel, grid=(pass_dev // group,), out_shape=[shape...  9.24 us
    pallas_call x1, Pallas kernels, project(): pl.pallas_call(project_kernel, out_shape=[half, half, half, full, full, f...  8.57 us
    pallas_call x2, Pallas kernels, over_tp(): pl.pallas_call(body, out_shape=jax.ShapeDtypeStruct(shape, dtype), in_spe...  8.07 us
  transfers between devices with their start and end apart: 8, of which 4 were waited for; matrix products, arithmetic and copies ran while one was open for 1% of the time, Pallas kernels for 36%

profile of v1, /device:TPU:0, one launch (start us, length us, event | category | flops | bytes accessed | tf_op | source)
XLA Modules:
  0.0 233.4 jit_solution(5701324106286980429)
XLA Ops:
  0.0 1.3 copy.22.ids_ref
  1.3 2.4 %tables.1 = (s32[8,4]{1,0:T(8,128)}, s32[8,4]{1,0:T(8,128)}, s32[32]{0:T(128)}, s32[32]{0:T(128)}) custom-call(s32[8,4]{1,0:T(8,128)} %copy.22.ids_ref), custom_call_target="tpu_custom_call" | custom-call | tf_op jit(solution)/shard_map/tables/pallas_call | solution.py:67
  3.8 7.3 %all-to-all-start = ((s32[8,1,4]{2,1,0:T(1,128)}), s32[8,1,4]{2,1,0:T(1,128)S(1)}, u32[]{:S(2)}, u32[]{:S(2)}) async-start(s32[8,1,4]{2,1,0:T(1,128)} %bitcast.9), calls=%async_computation | async-start | bytes 8192 | tf_op jit(solution)/shard_map/all_to_all | solution.py:444
  11.1 5.1 %queries.1 = bf16[8,256,512]{2,1,0:T(8,128)(2,1)} custom-call(s32[8,4]{1,0:T(8,128)} %get-tuple-element.25.blk_ref, bf16[512,2048]{1,0:T(8,128)(2,1)} %tok_ref.3, bf16[2048,512]{1,0:T(8,128)(2,1)} %w_ref.1, f32[1,512]{1,0:T(1,128)} %bitcast.10), custom_call_target="tpu_custom_call" | custom-call | tf_op jit(solution)/shard_map/queries/pallas_call | solution.py:103
  16.2 1.4 all-to-all-done.asked_ref
  17.6 0.0 copy-start.10
  17.6 0.6 copy-done.10
  18.1 4.6 %all-to-all-start.1 = ((bf16[8,256,512]{2,1,0:T(8,128)(2,1)}), bf16[8,256,512]{2,1,0:T(8,128)(2,1)S(1)}, u32[]{:S(2)}, u32[]{:S(2)}) async-start(bf16[8,256,512]{2,1,0:T(8,128)(2,1)} %queries.1), calls=%async_computation.1 | async-start | bytes 4194304 | tf_op jit(solution)/shard_map/all_to_all | solution.py:446
  22.8 9.2 %keyvals.1 = (bf16[1152,512]{1,0:T(8,128)(2,1)}, bf16[1152,512]{1,0:T(8,128)(2,1)}) custom-call(bf16[1152,2048]{1,0:T(8,128)(2,1)} %bitcast.8, bf16[2048,512]{1,0:T(8,128)(2,1)} %wk_ref.1, bf16[2048,512]{1,0:T(8,128)(2,1)} %wv_ref.1), custom_call_target="tpu_custom_call" | custom-call | tf_op jit(solution)/shard_map/keyvals/pallas_call | solution.py:132
  32.0 38.4 %all-to-all-done.1.q_ref = bf16[8,256,512]{2,1,0:T(8,128)(2,1)S(1)} async-done(((bf16[8,256,512]{2,1,0:T(8,128)(2,1)}), bf16[8,256,512]{2,1,0:T(8,128)(2,1)S(1)}, u32[]{:S(2)}, u32[]{:S(2)}) %all-to-all-start.1) | async-done | bytes 2097184 | tf_op jit(solution)/shard_map/all_to_all | solution.py:446
  70.4 0.0 copy-start
  70.4 1.3 copy-done
  71.8 11.4 %attend.1 = bf16[8,272,512]{2,1,0:T(8,128)(2,1)} custom-call(s32[8,1,4]{2,1,0:T(1,128)} %copy-done.10, bf16[8,256,512]{2,1,0:T(8,128)(2,1)} %copy-done, bf16[1152,512]{1,0:T(8,128)(2,1)} %get-tuple-element.26.k_ref, bf16[1152,512]{1,0:T(8,128)(2,1)} %get-tuple-element.27.v_ref), custom_call_target="tpu_custom_call" | custom-call | tf_op jit(solution)/shard_map/attend/pallas_call | solution.py:334
  83.2 55.3 %all_to_all.15.part_ref = bf16[8,272,512]{2,1,0:T(8,128)(2,1)} all-to-all(bf16[8,272,512]{2,1,0:T(8,128)(2,1)} %attend.1), channel_id=1, replica_groups=mesh['st'=8,'tp'=4] {'st'}, dimensions={0} | all-to-all | bytes 4456448 | tf_op jit(solution)/shard_map/all_to_all | solution.py:453
  138.5 5.2 %combine.1.refs_0_ = bf16[512,512]{1,0:T(8,128)(2,1)} custom-call(s32[32]{0:T(128)} %get-tuple-element.22.own_ref, s32[32]{0:T(128)} %get-tuple-element.23.rank_ref, bf16[8,272,512]{2,1,0:T(8,128)(2,1)} %all_to_all.15.part_ref), custom_call_target="tpu_custom_call" | custom-call | tf_op jit(solution)/shard_map/combine/pallas_call | solution.py:377
  143.7 1.5 collective-permute-start.1
  145.2 0.0 copy-done.5
  145.2 1.0 copy.25.dl_ref
  146.2 0.0 copy-done.6
  146.2 1.0 copy.26.rl_ref
  147.2 0.0 copy-done.11
  147.2 0.8 copy.27.shift_ref
  148.0 8.6 %project.1 = (bf16[512,256]{1,0:T(8,128)(2,1)}, bf16[512,256]{1,0:T(8,128)(2,1)}, bf16[512,256]{1,0:T(8,128)(2,1)}, f32[512,256]{1,0:T(8,128)}, f32[512,256]{1,0...) custom-call(bf16[512,2048]{1,0:T(8,128)(2,1)} %tok_ref.3, bf16[2048,256]{1,0:T(8,128)(2,1)} %mq_ref.1, ...), custom_call_target="tpu_custom_call" | custom-call | tf_op jit(solution)/shard_map/project/pallas_call | solution.py:178
  156.6 47.9 %prepare.1 = (f32[512,256]{1,0:T(8,128)}, f32[512,256]{1,0:T(8,128)}, f32[512,256]{1,0:T(8,128)}, f32[512,256]{1,0:T(8,128)}) custom-call(bf16[512,256]{1,0:T(8,128)(2,1)} %get-tuple-element.29.q_ref, bf16[512,256]{1,0:T(8,128)(2,1)} %get-tuple-element.30.k_ref, bf16[512,256]{1,0:T(8,128)(2,1)} %get-tuple-element.31.v_ref, ...), custom_call_target="tpu_custom_call" | custom-call | tf_op jit(solution)/shard_map/prepare/pallas_call | solution.py:265
  204.5 11.1 %scan.1.refs_0_ = bf16[512,256]{1,0:T(8,128)(2,1)} custom-call(f32[512,256]{1,0:T(8,128)} %get-tuple-element.35.qe_ref, f32[512,256]{1,0:T(8,128)} %get-tuple-element.36.ob_ref, f32[512,256]{1,0:T(8,128)} %get-tuple-element.37.st_ref, f32[512,256]{1,0:T(8,128)} %get-tuple-element.38.ad_ref, f32[1,256]{1,0:T(1,128)} %bitcast.11), custom_call_target="tpu_custom_call" | custom-call | tf_op jit(solution)/shard_map/scan/pallas_call | solution.py:296
  215.5 0.5 collective-permute-start.4
  216.0 0.0 copy-done.1
  216.0 0.0 collective-permute-start
  216.0 0.0 collective-permute-done.1.refs_2_
  216.0 0.0 copy-start.2
  216.1 0.5 collective-permute-start.2
  216.6 0.1 collective-permute-start.3
  216.6 5.5 %collective-permute-done.4.refs_2_ = bf16[512,256]{1,0:T(8,128)(2,1)S(1)} collective-permute-done((bf16[512,256]{1,0:T(8,128)(2,1)}, bf16[512,256]{1,0:T(8,128)(2,1)S(1)}, u32[]{:S(2)}, u32[]{:S(2)}) %collective-permute-start.4) | collective-permute-done | bytes 262176 | tf_op jit(solution)/shard_map/ppermute | solution.py:424
  222.1 0.0 collective-permute-start.5
  222.1 0.0 collective-permute-done.3.refs_1_
  222.1 0.0 copy-start.8
  222.1 1.5 collective-permute-done.5.refs_3_
  223.7 0.0 copy-done.7
  223.7 0.0 copy-done.8
  223.7 0.7 copy-done.9
  224.4 3.2 %mixer_out.1.refs_6_ = f32[512,512]{1,0:T(8,128)} custom-call(s32[1]{0:T(128)} %bitcast.me_ref, bf16[512,256]{1,0:T(8,128)(2,1)} %scan.1.refs_0_, bf16[512,256]{1,0:T(8,128)(2,1)} %copy-done.8, bf16[512,256]{1,0:T(8,128)(2,1)} %copy-done.7, bf16[512,256]{1,0:T(8,128)(2,1)} %copy-done.9, bf16[1024,512]{1,0:T(8,128)(2,1)} %refs_4_.2), custom_call_target="tpu_custom_call" | custom-call | tf_op jit(solution)/shard_map/mixer_out/pallas_call | solution.py:409
  227.6 0.0 collective-permute-done.refs_1_
  227.6 0.0 collective-permute-done.2.refs_3_
  227.6 0.0 copy-start.4
  227.6 0.0 copy-done.2
  227.6 0.8 copy-done.3
  228.4 0.2 copy-done.4
  228.6 4.8 %final.1 = bf16[512,512]{1,0:T(8,128)(2,1)} custom-call(s32[1]{0:T(128)} %bitcast.me_ref, bf16[512,512]{1,0:T(8,128)(2,1)} %combine.1.refs_0_, bf16[512,512]{1,0:T(8,128)(2,1)} %copy-done.3, bf16[512,512]{1,0:T(8,128)(2,1)} %copy-done.2, bf16[512,512]{1,0:T(8,128)(2,1)} %copy-done.4, bf16[2048,512]{1,0:T(8,128)(2,1)} %refs_4_.3, ...), custom_call_target="tpu_custom_call" | custom-call | tf_op jit(solution)/shard_map/final/pallas_call | solution.py:409
  (7 shorter events, 0.0 us)
Async XLA Ops:
  3.8 13.8 %all-to-all-start = ((s32[8,1,4]{2,1,0:T(1,128)}), s32[8,1,4]{2,1,0:T(1,128)S(1)}, u32[]{:S(2)}, u32[]{:S(2)}) async-start(s32[8,1,4]{2,1,0:T(1,128)} %bitcast.9), calls=%async_computation | async-start | bytes 8192 | tf_op jit(solution)/shard_map/all_to_all | solution.py:444
  17.6 0.6 copy-start.10
  18.1 52.3 %all-to-all-start.1 = ((bf16[8,256,512]{2,1,0:T(8,128)(2,1)}), bf16[8,256,512]{2,1,0:T(8,128)(2,1)S(1)}, u32[]{:S(2)}, u32[]{:S(2)}) async-start(bf16[8,256,512]{2,1,0:T(8,128)(2,1)} %queries.1), calls=%async_computation.1 | async-start | bytes 4194304 | tf_op jit(solution)/shard_map/all_to_all | solution.py:446
  70.4 1.3 copy-start
  138.5 6.7 %copy-start.5 = (bf16[2048,64]{0,1:T(8,128)(2,1)S(1)}, bf16[2048,64]{0,1:T(8,128)(2,1)}, u32[]{:S(2)}) copy-start(bf16[2048,64]{0,1:T(8,128)(2,1)} %param.25) | copy-start | bytes 786436
  138.5 7.7 %copy-start.6 = (bf16[2048,64]{0,1:T(8,128)(2,1)S(1)}, bf16[2048,64]{0,1:T(8,128)(2,1)}, u32[]{:S(2)}) copy-start(bf16[2048,64]{0,1:T(8,128)(2,1)} %param.29) | copy-start | bytes 786436
  138.5 8.7 %copy-start.11 = (f32[512,4]{0,1:T(4,128)S(1)}, f32[512,4]{0,1:T(4,128)}, u32[]{:S(2)}) copy-start(f32[512,4]{0,1:T(4,128)} %param.28) | copy-start | bytes 24580
  143.7 72.4 %collective-permute-start.1 = (bf16[512,512]{1,0:T(8,128)(2,1)}, bf16[512,512]{1,0:T(8,128)(2,1)S(1)}, u32[]{:S(2)}, u32[]{:S(2)}) collective-permute-start(bf16[512,512]{1,0:T(8,128)(2,1)} %combine.1.refs_0_), channel_id=1, source_target_pairs={{0,2},{1,3},{2,0},{3,1},{4,6},{5,7},{6,4},{7,5},{8,10},{9,11},{10,... | collective-permute-start | bytes 1572872 | tf_op jit(solution)/shard_map/ppermute | solution.py:424
  156.6 59.4 %copy-start.1 = (bf16[512,512]{1,0:T(8,128)(2,1)S(1)}, bf16[512,512]{1,0:T(8,128)(2,1)}, u32[]{:S(2)}) copy-start(bf16[512,512]{1,0:T(8,128)(2,1)} %combine.1.refs_0_) | copy-start | bytes 1572868
  215.5 6.6 %collective-permute-start.4 = (bf16[512,256]{1,0:T(8,128)(2,1)}, bf16[512,256]{1,0:T(8,128)(2,1)S(1)}, u32[]{:S(2)}, u32[]{:S(2)}) collective-permute-start(bf16[512,256]{1,0:T(8,128)(2,1)} %scan.1.refs_0_), channel_id=1, source_target_pairs={{0,2},{1,3},{2,0},{3,1},{4,6},{5,7},{6,4},{7,5},{8,10},{9,11},{10,... | collective-permute-start | bytes 786440 | tf_op jit(solution)/shard_map/ppermute | solution.py:424
  216.0 11.5 %collective-permute-start = (bf16[512,512]{1,0:T(8,128)(2,1)S(1)}, bf16[512,512]{1,0:T(8,128)(2,1)S(1)}, u32[]{:S(2)}, u32[]{:S(2)}) collective-permute-start(bf16[512,512]{1,0:T(8,128)(2,1)S(1)} %copy-done.1), channel_id=1, source_target_pairs={{0,1},{1,0},{2,3},{3,2},{4,5},{5,4},{6,7},{7,6},{8,9},{9,8},{10,11... | collective-permute-start | bytes 1572872 | tf_op jit(solution)/shard_map/ppermute | solution.py:424
  216.0 11.6 %copy-start.2 = (bf16[512,512]{1,0:T(8,128)(2,1)}, bf16[512,512]{1,0:T(8,128)(2,1)S(1)}, u32[]{:S(2)}) copy-start(bf16[512,512]{1,0:T(8,128)(2,1)S(1)} %collective-permute-done.1.refs_2_) | copy-start | bytes 1572868
  216.1 11.5 %collective-permute-start.2 = (bf16[512,512]{1,0:T(8,128)(2,1)S(1)}, bf16[512,512]{1,0:T(8,128)(2,1)S(1)}, u32[]{:S(2)}, u32[]{:S(2)}) collective-permute-start(bf16[512,512]{1,0:T(8,128)(2,1)S(1)} %collective-permute-done.1.refs_2_), channel_id=1, source_target_pairs={{0,1},{1,0},{2,3},{3,2},{4,5},{5,4},{6,7},{7,6},{8,9},{9,8},{10,11... | collective-permute-start | bytes 1572872 | tf_op jit(solution)/shard_map/ppermute | solution.py:424
  216.6 5.6 %collective-permute-start.3 = (bf16[512,256]{1,0:T(8,128)(2,1)}, bf16[512,256]{1,0:T(8,128)(2,1)S(1)}, u32[]{:S(2)}, u32[]{:S(2)}) collective-permute-start(bf16[512,256]{1,0:T(8,128)(2,1)} %scan.1.refs_0_), channel_id=1, source_target_pairs={{0,1},{1,0},{2,3},{3,2},{4,5},{5,4},{6,7},{7,6},{8,9},{9,8},{10,11... | collective-permute-start | bytes 786440 | tf_op jit(solution)/shard_map/ppermute | solution.py:424
  222.1 1.5 copy-start.7
  222.1 1.5 collective-permute-start.5
  222.1 1.5 copy-start.8
  223.7 0.7 copy-start.9
  227.6 0.8 copy-start.3
  227.6 1.0 copy-start.4

commit v2 on v1

v2 whole, which is shorter than its diff:
```python
import functools
import jax
import jax.numpy as jnp
from jax import lax
from jax.experimental import pallas as pl
from jax.experimental.pallas import tpu as pltpu
from jax.sharding import PartitionSpec as P

XHEAD = 256
QBLOCK = 64
MBLOCK = 64
RHEAD = 64
LROWS = 16

FLOAT32 = jnp.float32
BFLOAT = jnp.bfloat16
PRECISE = lax.Precision.HIGHEST
VMEM = pltpu.VMEM
SMEM = pltpu.SMEM
NT = (((1,), (1,)), ((), ()))
NN = (((1,), (0,)), ((), ()))
TN = (((0,), (0,)), ((), ()))


def dot(left, right, dims=NN, precision=None):
    return lax.dot_general(left, right, dims, precision=precision, preferred_element_type=FLOAT32)


def iota(shape, dim):
    return lax.broadcasted_iota(jnp.int32, shape, dim)


def whole(count):
    return [pl.BlockSpec(memory_space=VMEM)] * count


def after(refs, count):
    return [pl.BlockSpec(memory_space=pl.ANY)] * count


def up16(count):
    return -(-count // 16) * 16


def entry(lines, row, lane):
    hit = (iota(lines.shape, 0) == row) & (iota(lines.shape, 1) == lane)
    return jnp.sum(jnp.where(hit, lines, 0.0)).astype(jnp.int32)


def write_group(out_ref, q_ref, blocks, passages):
    capacity = len(blocks)
    width = out_ref.shape[1]
    line = jnp.zeros((LROWS, width), FLOAT32)
    row, lane = iota(line.shape, 0), iota(line.shape, 1)
    for r in range(capacity):
        start = pl.multiple_of(jnp.maximum(blocks[r] - 1, 0) * QBLOCK, QBLOCK)
        out_ref[r * QBLOCK : (r + 1) * QBLOCK, :] = q_ref[pl.ds(start, QBLOCK), :]
        line = jnp.where((row == 0) & (lane == r), passages[r].astype(FLOAT32), line)
    out_ref[capacity * QBLOCK :, :] = line.astype(BFLOAT)


def query_kernel(pass_dev, owners, me_ref, ids_ref, tok_ref, w_ref, gain_ref, q_ref, blk_ref,
                 *refs):
    *group_refs, pidx_ref, fill_ref = refs
    capacity = blk_ref.shape[1]
    per_block = ids_ref.shape[1]
    rows = tok_ref.shape[0]
    width = w_ref.shape[1]

    def clear(o, carry):
        fill_ref[o] = 0
        for r in range(capacity):
            pidx_ref[o, r] = 0
            blk_ref[o, r] = 0
        return carry

    lax.fori_loop(0, owners, clear, 0)

    def put(n, carry):
        passage = ids_ref[n // per_block, n % per_block]
        owner = passage // pass_dev
        rank = fill_ref[owner]
        fill_ref[owner] = rank + 1
        pidx_ref[owner, rank] = passage - owner * pass_dev
        blk_ref[owner, rank] = n // per_block + 1
        return carry

    lax.fori_loop(0, ids_ref.shape[0] * per_block, put, 0)

    for h in range(width // XHEAD):
        cols = slice(h * XHEAD, (h + 1) * XHEAD)
        raw = dot(tok_ref[...], w_ref[:, cols])
        scale = lax.rsqrt(jnp.mean(raw * raw, axis=-1, keepdims=True) + 1e-06)
        q_ref[:rows, cols] = (raw * scale * gain_ref[:, cols]).astype(BFLOAT)

    tail = q_ref.shape[0] - rows
    row, lane = iota((tail, 128), 0), iota((tail, 128), 1)

    def line(o, table):
        for r in range(capacity):
            table = jnp.where((row == o) & (lane == r), blk_ref[o, r].astype(FLOAT32), table)
            table = jnp.where((row == o) & (lane == capacity + r),
                              pidx_ref[o, r].astype(FLOAT32), table)
        return table

    table = lax.fori_loop(0, owners, line, jnp.zeros((tail, 128), FLOAT32))
    q_ref[rows:, :] = jnp.zeros((tail, width), BFLOAT)
    q_ref[rows:, :128] = table.astype(BFLOAT)
    for k, ref in enumerate(group_refs):
        owner = me_ref[0] ^ k
        write_group(ref, q_ref, [blk_ref[owner, r] for r in range(capacity)],
                    [pidx_ref[owner, r] for r in range(capacity)])


def make_queries(me, ids, owners, capacity, pass_dev, tokens, cross_query, score_gain):
    rows, width = tokens.shape[0], cross_query.shape[1]
    smem = pl.BlockSpec(memory_space=SMEM)
    group = jax.ShapeDtypeStruct((capacity * QBLOCK + LROWS, width), BFLOAT)
    count = owners // 2
    outs = pl.pallas_call(
        functools.partial(query_kernel, pass_dev, owners),
        out_shape=[jax.ShapeDtypeStruct((rows + up16(owners), width), BFLOAT),
                   jax.ShapeDtypeStruct((owners, capacity), jnp.int32)] + [group] * count,
        in_specs=[smem, smem] + whole(3),
        out_specs=whole(1) + [smem] + whole(count),
        scratch_shapes=[SMEM((owners, capacity), jnp.int32), SMEM((owners,), jnp.int32)],
        name="queries",
    )(me, ids, tokens, cross_query, score_gain.reshape(1, -1))
    return outs[0], outs[1], outs[2:]


def relay_kernel(rows, deps, me_ref, q_ref, *refs):
    blk_ref, *group_refs = refs[deps:]
    owners, capacity = blk_ref.shape
    table = q_ref[rows:, :128].astype(FLOAT32)
    for k, ref in enumerate(group_refs):
        owner = me_ref[0] ^ k
        blocks = [entry(table, owner, r) for r in range(capacity)]
        for r in range(capacity):
            blk_ref[owner, r] = blocks[r]
        write_group(ref, q_ref, blocks, [entry(table, owner, capacity + r) for r in range(capacity)])


def relay(me, queries, rows, owners, capacity, deps):
    width = queries.shape[1]
    smem = pl.BlockSpec(memory_space=SMEM)
    group = jax.ShapeDtypeStruct((capacity * QBLOCK + LROWS, width), BFLOAT)
    count = owners // 2
    outs = pl.pallas_call(
        functools.partial(relay_kernel, rows, len(deps)),
        out_shape=[jax.ShapeDtypeStruct((owners, capacity), jnp.int32)] + [group] * count,
        in_specs=[smem] + whole(1) + after(deps, len(deps)),
        out_specs=[smem] + whole(count),
        name="relay",
    )(me, queries, *deps)
    return outs[0], outs[1:]


def keyval_kernel(rows_ref, wk_ref, wv_ref, k_ref, v_ref):
    width = wk_ref.shape[1]
    rows = rows_ref[...]
    for h in range(width // XHEAD):
        cols = slice(h * XHEAD, (h + 1) * XHEAD)
        raw = dot(rows, wk_ref[:, cols])
        scale = lax.rsqrt(jnp.mean(raw * raw, axis=-1, keepdims=True) + 1e-06)
        k_ref[:, cols] = (raw * scale).astype(BFLOAT)
        v_ref[:, cols] = dot(rows, wv_ref[:, cols]).astype(BFLOAT)


def make_keyvals(store, passage_key, passage_value):
    pass_dev, plen, model = store.shape
    width = passage_key.shape[1]
    group = max(g for g in range(1, 5) if pass_dev % g == 0)
    tile = group * plen
    weight = pl.BlockSpec((model, width), lambda i: (0, 0))
    out = pl.BlockSpec((tile, width), lambda i: (i, 0))
    shape = jax.ShapeDtypeStruct((pass_dev * plen, width), BFLOAT)
    return pl.pallas_call(
        keyval_kernel,
        grid=(pass_dev // group,),
        out_shape=[shape, shape],
        in_specs=[pl.BlockSpec((tile, model), lambda i: (i, 0)), weight, weight],
        out_specs=[out, out],
        name="keyvals",
    )(store.reshape(-1, model), passage_key, passage_value)


def project_kernel(
    tok_ref, mq_ref, mk_ref, mv_ref, dl_ref, rl_ref, gd_ref, du_ref, ru_ref, gu_ref,
    base_ref, shift_ref,
    q_ref, k_ref, v_ref, u_ref, rk_ref, lf_ref, gate_ref,
):
    tokens = tok_ref[...]
    width = mq_ref.shape[1]
    rank = dl_ref.shape[1]
    lows = dot(tokens, jnp.concatenate([dl_ref[...], rl_ref[...], gd_ref[...]], axis=1))
    decay_low = jnp.tanh(lows[:, :rank]).astype(BFLOAT)
    rate_low = lows[:, rank : 2 * rank].astype(BFLOAT)
    gate_low = lows[:, 2 * rank :].astype(BFLOAT)
    gate_ref[...] = jax.nn.sigmoid(dot(gate_low, gu_ref[...]))
    pre = base_ref[...] + dot(decay_low, du_ref[...])
    head = iota(pre.shape, 1) // RHEAD
    shift = jnp.zeros_like(pre)
    for h in range(width // RHEAD):
        shift = jnp.where(head == h, shift_ref[:, h : h + 1], shift)
    lf_ref[...] = -jax.nn.sigmoid(pre + shift) * (2.718281828459045 ** -0.5)
    q_ref[...] = dot(tokens, mq_ref[...]).astype(BFLOAT)
    v_ref[...] = dot(tokens, mv_ref[...]).astype(BFLOAT)
    key = dot(tokens, mk_ref[...]).astype(BFLOAT)
    k_ref[...] = key
    key = key.astype(FLOAT32)
    same = (iota((width, width), 0) // RHEAD == iota((width, width), 1) // RHEAD).astype(FLOAT32)
    unit = key * lax.rsqrt(dot(key * key, same, precision=PRECISE) + 1e-06)
    u_ref[...] = unit
    rk_ref[...] = unit * jax.nn.sigmoid(dot(rate_low, ru_ref[...]))


def project(tokens, mix_query, mix_key, mix_value, decay_lower, decay_upper, decay_base,
            decay_shift, rate_lower, rate_upper, gate_down, gate_up):
    rows = tokens.shape[0]
    width = mix_query.shape[1]
    half = jax.ShapeDtypeStruct((rows, width), BFLOAT)
    full = jax.ShapeDtypeStruct((rows, width), FLOAT32)
    return pl.pallas_call(
        project_kernel,
        out_shape=[half, half, half, full, full, full,
                   jax.ShapeDtypeStruct((rows, gate_up.shape[1]), FLOAT32)],
        in_specs=whole(12),
        out_specs=whole(7),
        name="project",
    )(tokens, mix_query, mix_key, mix_value, decay_lower, rate_lower, gate_down,
      decay_upper, rate_upper, gate_up, decay_base.reshape(1, -1), decay_shift)


def parts2(value):
    high = value.astype(BFLOAT)
    return high, (value - high.astype(FLOAT32)).astype(BFLOAT)


def parts3(value):
    high = value.astype(BFLOAT)
    rest = value - high.astype(FLOAT32)
    return (high,) + parts2(rest)


def spread(value):
    rows, width = value.shape
    lane = iota((1, 128), 1) // RHEAD
    blank = jnp.zeros((rows, 128), value.dtype)
    blocks = []
    for h in range(width // RHEAD):
        mine = (h * RHEAD) // 128
        keep = (lane == h % (128 // RHEAD)).astype(value.dtype)
        cells = [blank] * (width // 128)
        cells[mine] = value[:, mine * 128 : (mine + 1) * 128] * keep
        blocks.append(jnp.concatenate(cells, axis=1) if len(cells) > 1 else cells[0])
    return jnp.concatenate(blocks, axis=0)


def fold(value):
    width = value.shape[1]
    lane = iota((1, 128), 1) // RHEAD
    cells = []
    for t in range(width // 128):
        cell = value[t * 128 : t * 128 + RHEAD, t * 128 : (t + 1) * 128]
        for p in range(1, 128 // RHEAD):
            start = t * 128 + p * RHEAD
            cell = jnp.where(lane == p, value[start : start + RHEAD, t * 128 : (t + 1) * 128], cell)
        cells.append(cell)
    return jnp.concatenate(cells, axis=1) if len(cells) > 1 else cells[0]


def left_of(value):
    high, low = parts2(value)
    return jnp.concatenate([high, low, high], axis=1)


def right_of(value):
    high, low = parts2(value)
    high, low = spread(high), spread(low)
    return jnp.concatenate([high, high, low], axis=0)


def right_nt(value):
    high, low = parts2(value)
    high, low = spread(high), spread(low)
    return jnp.concatenate([high, high, low], axis=1)


def across(left, right):
    lh, ll = parts2(left)
    rh, rl = parts2(right)
    return fold(dot(jnp.concatenate([lh, ll, lh], axis=0), jnp.concatenate([rh, rh, rl], axis=0), TN))


def prepare_chunks(queries, keys, values, units, rate_keys, fades):
    n = range(len(queries))
    length, width = queries[0].shape
    row = iota((length, width), 0)
    col = iota((length, width), 1) % RHEAD
    lower = (iota((length, length), 1) <= iota((length, length), 0)).astype(BFLOAT)
    cumul = []
    for c in n:
        sums = dot(lower, jnp.concatenate(parts3(fades[c]), axis=1))
        cumul.append(sums[:, :width] + sums[:, width : 2 * width] + sums[:, 2 * width :])
    ends = [cumul[c][length - 1 :, :] for c in n]
    grown = [jnp.exp(-cumul[c]) for c in n]
    pulled = [-units[c] * jnp.exp(cumul[c] - fades[c]) for c in n]
    read = [queries[c] * jnp.exp(cumul[c]) for c in n]
    both = [left_of(jnp.concatenate([pulled[c], read[c]], axis=0)) for c in n]
    from_rate = [dot(both[c], right_nt(rate_keys[c] * grown[c]), NT) for c in n]
    from_key = [dot(both[c], right_nt(keys[c] * grown[c]), NT) for c in n]
    strict, upto = col < row, col <= row
    rate_pull = [jnp.where(strict, from_rate[c][:length], 0.0) for c in n]
    rate_read = [left_of(jnp.where(upto, from_rate[c][length:], 0.0)) for c in n]
    key_both = [
        left_of(jnp.concatenate([jnp.where(strict, from_key[c][:length], 0.0),
                                 jnp.where(upto, from_key[c][length:], 0.0)], axis=0)) for c in n]

    def pick(size):
        return (row // (2 * size) == col // (2 * size)) & (row // size > col // size)

    first = pick(1)
    eye = (row == col).astype(FLOAT32)
    inverse = [eye + jnp.where(first, rate_pull[c], 0.0) for c in n]
    size = 2
    while size < length:
        keep = pick(size)
        mids = [dot(left_of(inverse[c]), right_of(jnp.where(keep, rate_pull[c], 0.0))) for c in n]
        adds = [dot(left_of(mids[c]), right_of(inverse[c])) for c in n]
        inverse = [inverse[c] + adds[c] for c in n]
        size *= 2
    inverse = [left_of(inverse[c]) for c in n]
    from_value = []
    for c in n:
        wide = spread(values[c])
        from_value.append(dot(key_both[c][:, : 2 * width], jnp.concatenate([wide, wide], axis=0)))
    moved = [dot(inverse[c], right_of(pulled[c])) for c in n]
    base = [dot(inverse[c], right_of(from_value[c][:length])) for c in n]
    query_end = [read[c] + dot(rate_read[c], right_of(moved[c])) for c in n]
    out_base = [from_value[c][length:] + dot(rate_read[c], right_of(base[c])) for c in n]
    left = [jnp.exp(ends[c] - cumul[c]) for c in n]
    step, add = [], []
    diag = iota((RHEAD, width), 0) == iota((RHEAD, width), 1) % RHEAD
    for c in n:
        rate_left = rate_keys[c] * left[c]
        step.append(jnp.where(diag, jnp.exp(ends[c]), 0.0) + across(moved[c], rate_left))
        add.append(across(jnp.concatenate([values[c].astype(FLOAT32), base[c]], axis=0),
                          jnp.concatenate([keys[c] * left[c], rate_left], axis=0)))
    return query_end, out_base, step, add


def prepare_kernel(deps, q_ref, k_ref, v_ref, u_ref, rk_ref, lf_ref, *refs):
    outs = refs[deps:]
    spans = [slice(c * MBLOCK, (c + 1) * MBLOCK) for c in range(q_ref.shape[0] // MBLOCK)]
    results = prepare_chunks(
        [q_ref[s].astype(FLOAT32) for s in spans], [k_ref[s].astype(FLOAT32) for s in spans],
        [v_ref[s] for s in spans], [u_ref[s] for s in spans], [rk_ref[s] for s in spans],
        [lf_ref[s] for s in spans])
    for ref, values in zip(outs, results):
        for s, value in zip(spans, values):
            ref[s] = value


def prepare(inputs, start, count, deps):
    width = inputs[0].shape[1]
    tile = count * MBLOCK
    spec = pl.BlockSpec((tile, width), lambda i: (start // count, 0))
    full = jax.ShapeDtypeStruct((tile, width), FLOAT32)
    return pl.pallas_call(
        functools.partial(prepare_kernel, len(deps)),
        grid=(1,),
        out_shape=[full] * 4,
        in_specs=[spec] * 6 + after(deps, len(deps)),
        out_specs=[pl.BlockSpec((tile, width), lambda i: (0, 0))] * 4,
        name="prepare",
    )(*inputs, *deps)


def head_mean(value, same):
    high, low = parts2(value)
    return dot(jnp.concatenate([high, low], axis=1), same) * (1.0 / RHEAD)


def scan_kernel(deps, pieces, gain_ref, *refs):
    prepared = [refs[4 * p : 4 * p + 4] for p in range(pieces)]
    out_ref, raw_ref = refs[4 * pieces + deps :]
    width = out_ref.shape[1]
    same = (iota((width, width), 0) // RHEAD == iota((width, width), 1) // RHEAD).astype(BFLOAT)
    same = jnp.concatenate([same, same], axis=0)
    state = None
    done = 0
    for qe_ref, ob_ref, st_ref, ad_ref in prepared:
        for c in range(qe_ref.shape[0] // MBLOCK):
            rows = slice(c * MBLOCK, (c + 1) * MBLOCK)
            out = ob_ref[rows, :]
            if state is None:
                state = ad_ref[rows, :]
            else:
                out = out + dot(left_of(qe_ref[rows, :]), right_nt(state), NT)
                state = dot(left_of(state), right_of(st_ref[rows, :])) + ad_ref[rows, :]
            raw_ref[done : done + MBLOCK, :] = out
            done += MBLOCK
    raw = raw_ref[...]
    centred = raw - head_mean(raw, same)
    var = head_mean(centred * centred, same)
    out_ref[...] = (centred * lax.rsqrt(var + 0.00064) * gain_ref[...]).astype(BFLOAT)


def scan(prepared, norm_gain, deps):
    width = prepared[0][0].shape[1]
    rows = sum(p[0].shape[0] for p in prepared)
    flat = [a for p in prepared for a in p]
    return pl.pallas_call(
        functools.partial(scan_kernel, len(deps), len(prepared)),
        out_shape=jax.ShapeDtypeStruct((rows, width), BFLOAT),
        in_specs=whole(1 + len(flat)) + after(deps, len(deps)),
        out_specs=pl.BlockSpec(memory_space=VMEM),
        scratch_shapes=[VMEM((rows, width), FLOAT32)],
        name="scan",
    )(norm_gain.reshape(1, -1), *flat, *deps)


def attend_group(plen, q_ref, k_ref, v_ref, out_ref):
    width = q_ref.shape[1]
    heads = width // XHEAD
    capacity = (q_ref.shape[0] - LROWS) // QBLOCK
    line = q_ref[capacity * QBLOCK :, :128].astype(FLOAT32)
    units = [(r, h) for r in range(capacity) for h in range(heads)]
    spans = [pl.ds(pl.multiple_of(entry(line, 0, r) * plen, plen), plen) for r in range(capacity)]
    mine = [slice(r * QBLOCK, (r + 1) * QBLOCK) for r in range(capacity)]
    cols = [slice(h * XHEAD, (h + 1) * XHEAD) for h in range(heads)]
    scores = [dot(q_ref[mine[r], cols[h]], k_ref[spans[r], cols[h]], NT) for r, h in units]
    expon = [jnp.exp(s * XHEAD ** (-0.5)).astype(BFLOAT) for s in scores]
    ones = jnp.ones((8, plen), BFLOAT)
    totals = [dot(ones, e, NT)[:1] for e in expon]
    outs = [dot(e, v_ref[spans[r], cols[h]]) for e, (r, h) in zip(expon, units)]
    sums = jnp.zeros((LROWS, QBLOCK), FLOAT32)
    rowid = iota((LROWS, QBLOCK), 0)
    for (r, h), out, total in zip(units, outs, totals):
        out_ref[mine[r], cols[h]] = out.astype(BFLOAT)
        high = total.astype(BFLOAT).astype(FLOAT32)
        where = 2 * (r * heads + h)
        sums = jnp.where(rowid == where, high, sums)
        sums = jnp.where(rowid == where + 1, total - high, sums)
    out_ref[capacity * QBLOCK :, :] = jnp.zeros((LROWS, width), BFLOAT)
    out_ref[capacity * QBLOCK :, :QBLOCK] = sums.astype(BFLOAT)


def attend_kernel(plen, count, deps, k_ref, v_ref, *refs):
    for q_ref, out_ref in zip(refs[:count], refs[count + deps :]):
        attend_group(plen, q_ref, k_ref, v_ref, out_ref)


def attend(groups, keys, values, plen, deps):
    count = len(groups)
    return pl.pallas_call(
        functools.partial(attend_kernel, plen, count, len(deps)),
        out_shape=[jax.ShapeDtypeStruct(g.shape, BFLOAT) for g in groups],
        in_specs=whole(2 + count) + after(deps, len(deps)),
        out_specs=whole(count),
        name="attend",
    )(keys, values, *groups, *deps)


def add_group(blocks, part_ref, acc_ref, den_ref):
    width = part_ref.shape[1]
    heads = width // XHEAD
    qrows = part_ref.shape[0] - LROWS
    lines = part_ref[qrows:, :QBLOCK].astype(FLOAT32)
    for r, block in enumerate(blocks):
        @pl.when(block > 0)
        def _(r=r, block=block):
            rows = pl.ds(pl.multiple_of((block - 1) * QBLOCK, QBLOCK), QBLOCK)
            acc_ref[rows, :] += part_ref[r * QBLOCK : (r + 1) * QBLOCK, :].astype(FLOAT32)
            for h in range(heads):
                at = 2 * (r * heads + h)
                den_ref[pl.ds((block - 1) * heads + h, 1), :] += lines[at : at + 1] + lines[at + 1 : at + 2]


def gather_kernel(count, deps, me_ref, blk_ref, *refs):
    parts = refs[:count]
    out_ref, acc_ref, den_ref = refs[count + deps :]
    capacity = blk_ref.shape[1]
    acc_ref[...] = jnp.zeros_like(acc_ref)
    den_ref[...] = jnp.zeros_like(den_ref)
    for k, part_ref in enumerate(parts):
        owner = me_ref[0] ^ k
        add_group([blk_ref[owner, r] for r in range(capacity)], part_ref, acc_ref, den_ref)
    rows = acc_ref.shape[0]
    lines = den_ref.shape[0]
    out_ref[:rows, :] = acc_ref[...].astype(BFLOAT)
    out_ref[rows:, :] = jnp.zeros((out_ref.shape[0] - rows, out_ref.shape[1]), BFLOAT)
    high, low = parts2(den_ref[...])
    out_ref[rows : rows + lines, :QBLOCK] = high
    out_ref[rows : rows + lines, 128 : 128 + QBLOCK] = low


def gather(me, blk, parts, rows, deps):
    width = parts[0].shape[1]
    lines = up16(rows // QBLOCK * (width // XHEAD))
    smem = pl.BlockSpec(memory_space=SMEM)
    return pl.pallas_call(
        functools.partial(gather_kernel, len(parts), len(deps)),
        out_shape=jax.ShapeDtypeStruct((rows + lines, width), BFLOAT),
        in_specs=[smem, smem] + whole(len(parts)) + after(deps, len(deps)),
        out_specs=pl.BlockSpec(memory_space=VMEM),
        scratch_shapes=[VMEM((rows, width), FLOAT32), VMEM((lines, QBLOCK), FLOAT32)],
        name="gather",
    )(me, blk, *parts, *deps)


def combine_kernel(count, deps, me_ref, blk_ref, far_ref, *refs):
    parts = refs[:count]
    out_ref, acc_ref, den_ref = refs[count + deps :]
    capacity = blk_ref.shape[1]
    rows, width = acc_ref.shape
    heads = width // XHEAD
    lines = den_ref.shape[0]
    acc_ref[...] = far_ref[:rows, :].astype(FLOAT32)
    tail = far_ref[rows : rows + lines, :].astype(FLOAT32)
    den_ref[...] = tail[:, :QBLOCK] + tail[:, 128 : 128 + QBLOCK]
    for k, part_ref in enumerate(parts):
        owner = me_ref[0] ^ k
        add_group([blk_ref[owner, r] for r in range(capacity)], part_ref, acc_ref, den_ref)
    turned = jnp.transpose(den_ref[...])
    for b in range(rows // QBLOCK):
        mine = slice(b * QBLOCK, (b + 1) * QBLOCK)
        for h in range(heads):
            cols = slice(h * XHEAD, (h + 1) * XHEAD)
            at = b * heads + h
            out_ref[mine, cols] = (acc_ref[mine, cols] / turned[:, at : at + 1]).astype(BFLOAT)


def combine(me, blk, far, parts, rows, deps):
    width = far.shape[1]
    smem = pl.BlockSpec(memory_space=SMEM)
    return pl.pallas_call(
        functools.partial(combine_kernel, len(parts), len(deps)),
        out_shape=jax.ShapeDtypeStruct((rows, width), BFLOAT),
        in_specs=[smem, smem] + whole(1 + len(parts)) + after(deps, len(deps)),
        out_specs=pl.BlockSpec(memory_space=VMEM),
        scratch_shapes=[VMEM((rows, width), FLOAT32), VMEM((far.shape[0] - rows, QBLOCK), FLOAT32)],
        name="combine",
    )(me, blk, far, *parts, *deps)


def gathered_dot(pieces, me, w_ref):
    total = None
    for j, piece in enumerate(pieces):
        depth = piece.shape[1]
        rows = pl.ds(pl.multiple_of((me ^ j) * depth, depth), depth)
        part = dot(piece[...], w_ref[rows, :])
        total = part if total is None else total + part
    return total


def mixer_out_kernel(me_ref, *refs):
    *pieces, w_ref, out_ref = refs
    out_ref[...] = gathered_dot(pieces, me_ref[0], w_ref)


def final_kernel(me_ref, *refs):
    *pieces, w_ref, gate_ref, mixer_ref, out_ref = refs
    cross = gathered_dot(pieces, me_ref[0], w_ref)
    out_ref[...] = (mixer_ref[...] + gate_ref[...] * cross).astype(BFLOAT)


def over_tp(body, me, pieces, others, dtype, name):
    shape = (pieces[0].shape[0], others[0].shape[1])
    return pl.pallas_call(
        body,
        out_shape=jax.ShapeDtypeStruct(shape, dtype),
        in_specs=[pl.BlockSpec(memory_space=SMEM)] + whole(len(pieces) + len(others)),
        out_specs=pl.BlockSpec(memory_space=VMEM),
        name=name,
    )(me, *pieces, *others)


def gather_tp(piece, count):
    pieces = {0: piece}
    bit = count // 2
    while bit:
        pairs = [(i, i ^ bit) for i in range(count)]
        for j in list(pieces):
            pieces[j ^ bit] = lax.ppermute(pieces[j], "tp", pairs)
        bit //= 2
    return [pieces[j] for j in range(count)]


def local(
    tokens, mix_query, mix_key, mix_value, decay_lower_map, decay_upper_map, decay_base,
    decay_shift, rate_lower_map, rate_upper_map, norm_gain, mix_out, cross_query, score_gain,
    passage_key, passage_value, cross_out, gate_down, gate_up, store, passage_ids,
):
    rows = tokens.shape[0]
    owners = lax.axis_size("st")
    shards = lax.axis_size("tp")
    pass_dev, plen, _ = store.shape
    per_block = passage_ids.shape[1]
    slots = passage_ids.shape[0] * per_block
    capacity = max(2, -(-slots // owners))
    me = lax.axis_index("tp").astype(jnp.int32).reshape(1)
    place = lax.axis_index("st").astype(jnp.int32).reshape(1)
    half = owners // 2

    def swap(value, bit):
        return lax.ppermute(value, "st", [(i, i ^ bit) for i in range(owners)])

    def swap_groups(groups):
        return [groups[0]] + [swap(groups[k], k) for k in range(1, half)]

    queries, blk, near = make_queries(
        place, passage_ids, owners, capacity, pass_dev, tokens, cross_query, score_gain)
    far_queries = swap(queries, half)
    near = swap_groups(near)
    keys, values = make_keyvals(store, passage_key, passage_value)
    *mixer_in, gate = project(
        tokens, mix_query, mix_key, mix_value, decay_lower_map, decay_upper_map, decay_base,
        decay_shift, rate_lower_map, rate_upper_map, gate_down, gate_up)
    chunks = rows // MBLOCK
    pieces = [(0, 3), (3, 3), (6, 2)] if chunks == 8 else [(c, 1) for c in range(chunks)]
    early, *others, last = pieces
    prepared = [prepare(mixer_in, *early, [keys])]
    far_blk, far = relay(place, far_queries, rows, owners, capacity, [prepared[-1][0]])
    far = swap_groups(far)
    near_parts = attend(near, keys, values, plen, [far[0]])
    for piece in others:
        prepared.append(prepare(mixer_in, *piece, [near_parts[0]]))
    far_parts = attend(far, keys, values, plen, [prepared[-1][0]])
    prepared.append(prepare(mixer_in, *last, [far_parts[0]]))
    far_parts = swap_groups(far_parts)
    returned = gather(place, far_blk, far_parts, rows, [prepared[-1][0]])
    near_parts, returned = lax.optimization_barrier((near_parts, returned))
    returned = swap(returned, half)
    near_parts = swap_groups(near_parts)
    mixer_heads = scan(prepared, norm_gain, [])
    mixer_all = gather_tp(mixer_heads, shards)
    attended = combine(place, blk, returned, near_parts, rows, [mixer_heads])
    mixer_part = over_tp(mixer_out_kernel, me, mixer_all, [mix_out], FLOAT32, "mixer_out")
    return over_tp(final_kernel, me, gather_tp(attended, shards), [cross_out, gate, mixer_part],
                   BFLOAT, "final")


def solution(mesh):
    placed = (
        P("st", None), P(None, "tp"), P(None, "tp"), P(None, "tp"), P(), P(None, "tp"), P("tp"),
        P("st", "tp"), P(), P(None, "tp"), P("tp"), P(None, "tp"), P(None, "tp"), P("tp"),
        P(None, "tp"), P(None, "tp"), P(None, "tp"), P(), P(None, "tp"), P("st", None, None),
        P("st", None),
    )
    return jax.shard_map(
        local, mesh=mesh, in_specs=placed, out_specs=P("st", "tp"), check_vma=False
    )
```

time: 234 us -> 139 us (0.59)
  blocking collectives: 55.3 us -> 0 us
  Pallas kernels: 109 us -> 70.7 us
  waiting for transfers between devices: 46.8 us -> 37.3 us
  starting transfers between devices: 14.5 us -> 21 us
    all_to_all x1 -> x0, blocking collectives: 55.3 us -> none  [local(): parts = lax.all_to_all(parts, 'st', split_axis=0, concat_axis=0, tiled=True)]
    all_to_all x2 -> x0, waiting for transfers between devices: 39.8 us -> none  [the longest x1 38.4 us: local(): lax.all_to_all(queries, 'st', split_axis=0, concat_axis=0, tiled=True)]
    pallas_call x6 -> x10, Pallas kernels: 83 us -> 44.8 us  [the longest x3 18.1 us: prepare(): pl.pallas_call(functools.partial(prepare_kernel, len(deps)), grid=(1,), o...]
    ppermute x0 -> x14, waiting for transfers between devices: none -> 19.7 us  [swap(): return lax.ppermute(value, 'st', [(i, i ^ bit) for i in range(owners)])]
    ppermute x0 -> x14, starting transfers between devices: none -> 18.5 us  [swap(): return lax.ppermute(value, 'st', [(i, i ^ bit) for i in range(owners)])]
    all_to_all x2 -> x0, starting transfers between devices: 11.9 us -> none  [the longest x1 7.29 us: local(): lax.all_to_all(want[:, None, :], 'st', split_axis=0, concat_axis=0, tiled...]
    ppermute x6, waiting for transfers between devices: 7 us -> 17.6 us  [gather_tp(): pieces[j ^ bit] = lax.ppermute(pieces[j], 'tp', pairs)]
    unnamed x28 -> x58, local copies, waits for them, and re-layouts: 7.8 us -> 9.87 us
  transfers between devices with their start and end apart: 8 -> 20, of which waited for: 4 -> 9; matrix products, arithmetic and copies ran while one was open for 1% -> 2% of each run, Pallas kernels for 36% -> 36%
where the time goes in v2:
time: 139 us
  Pallas kernels  70.7 us (51%)
  waiting for transfers between devices  37.3 us (27%)
  starting transfers between devices  21 us (15%)
  local copies, waits for them, and re-layouts  9.87 us (7%)
    ppermute x14, waiting for transfers between devices, swap(): return lax.ppermute(value, 'st', [(i, i ^ bit) for i in range(owners)])  19.7 us
    ppermute x14, starting transfers between devices, swap(): return lax.ppermute(value, 'st', [(i, i ^ bit) for i in range(owners)])  18.5 us
    pallas_call x3, Pallas kernels, prepare(): pl.pallas_call(functools.partial(prepare_kernel, len(deps)), grid=(1,), o...  18.1 us
    ppermute x6, waiting for transfers between devices, gather_tp(): pieces[j ^ bit] = lax.ppermute(pieces[j], 'tp', pairs)  17.6 us
    unnamed x58, local copies, waits for them, and re-layouts  9.87 us
    pallas_call x1, Pallas kernels, make_keyvals(): pl.pallas_call(keyval_kernel, grid=(pass_dev // group,), out_shape=[shape...  9.19 us
    pallas_call x2, Pallas kernels, attend(): pl.pallas_call(functools.partial(attend_kernel, plen, count, len(deps)),...  8.71 us
    pallas_call x1, Pallas kernels, project(): pl.pallas_call(project_kernel, out_shape=[half, half, half, full, full, f...  8.58 us
  transfers between devices with their start and end apart: 20, of which 9 were waited for; matrix products, arithmetic and copies ran while one was open for 2% of the time, Pallas kernels for 36%

profile of v2, /device:TPU:0, one launch (start us, length us, event | category | flops | bytes accessed | tf_op | source)
XLA Modules:
  0.0 139.1 jit_solution(16162274578941811824)
XLA Ops:
  0.0 1.3 copy.22.ids_ref
  1.4 6.0 %queries.1 = (bf16[528,512]{1,0:T(8,128)(2,1)}, s32[8,4]{1,0:T(8,128)}, bf16[272,512]{1,0:T(8,128)(2,1)}, bf16[272,512]{1,0:T(8,128)(2,1)}, bf16[272,512]{1,0:T(8,128)(2,1)}, /*index=5*/bf16[272,512]{1,0:T(8,128)(2,1)}) custom-call(s32[1]{0:T(128)} %bitcast.1.me_ref, s32[8,4]{1,0:T(8,128)} %copy.22.ids_ref, bf16[512,2048]{1,0:T(8,128)(2,1)} %tok_ref.3, ...), custom_call_target="tpu_custom_call" | custom-call | tf_op jit(solution)/shard_map/queries/pallas_call | solution.py:120
  7.4 4.1 %collective-permute-start.3 = (bf16[528,512]{1,0:T(8,128)(2,1)}, bf16[528,512]{1,0:T(8,128)(2,1)S(1)}, u32[]{:S(2)}, u32[]{:S(2)}) collective-permute-start(bf16[528,512]{1,0:T(8,128)(2,1)} %get-tuple-element.57), channel_id=1, source_target_pairs={{0,16},{4,20},{8,24},{12,28},{16,0},{20,4},{24,8},{28,12},{1,17},{... | collective-permute-start | bytes 1622024 | tf_op jit(solution)/shard_map/ppermute | solution.py:608
  11.5 1.5 %collective-permute-start = (bf16[272,512]{1,0:T(8,128)(2,1)}, bf16[272,512]{1,0:T(8,128)(2,1)S(1)}, u32[]{:S(2)}, u32[]{:S(2)}) collective-permute-start(bf16[272,512]{1,0:T(8,128)(2,1)} %get-tuple-element.54), channel_id=1, source_target_pairs={{0,4},{4,0},{8,12},{12,8},{16,20},{20,16},{24,28},{28,24},{1,5},{5... | collective-permute-start | bytes 835592 | tf_op jit(solution)/shard_map/ppermute | solution.py:608
  13.0 1.6 %collective-permute-start.1 = (bf16[272,512]{1,0:T(8,128)(2,1)}, bf16[272,512]{1,0:T(8,128)(2,1)S(1)}, u32[]{:S(2)}, u32[]{:S(2)}) collective-permute-start(bf16[272,512]{1,0:T(8,128)(2,1)} %get-tuple-element.55), channel_id=1, source_target_pairs={{0,8},{4,12},{8,0},{12,4},{16,24},{20,28},{24,16},{28,20},{1,9},{5... | collective-permute-start | bytes 835592 | tf_op jit(solution)/shard_map/ppermute | solution.py:608
  14.6 0.4 collective-permute-start.2
  15.0 0.9 copy.25.shift_ref
  15.8 1.0 copy.23.dl_ref
  16.9 1.0 copy.24.rl_ref
  17.9 9.2 %keyvals.1 = (bf16[1152,512]{1,0:T(8,128)(2,1)}, bf16[1152,512]{1,0:T(8,128)(2,1)}) custom-call(bf16[1152,2048]{1,0:T(8,128)(2,1)} %bitcast.6, bf16[2048,512]{1,0:T(8,128)(2,1)} %wk_ref.1, bf16[2048,512]{1,0:T(8,128)(2,1)} %wv_ref.1), custom_call_target="tpu_custom_call" | custom-call | tf_op jit(solution)/shard_map/keyvals/pallas_call | solution.py:178
  27.1 8.6 %project.1 = (bf16[512,256]{1,0:T(8,128)(2,1)}, bf16[512,256]{1,0:T(8,128)(2,1)}, bf16[512,256]{1,0:T(8,128)(2,1)}, f32[512,256]{1,0:T(8,128)}, f32[512,256]{1,0...) custom-call(bf16[512,2048]{1,0:T(8,128)(2,1)} %tok_ref.3, bf16[2048,256]{1,0:T(8,128)(2,1)} %mq_ref.1, ...), custom_call_target="tpu_custom_call" | custom-call | tf_op jit(solution)/shard_map/project/pallas_call | solution.py:224
  35.6 6.1 %prepare.3 = (f32[192,256]{1,0:T(8,128)}, f32[192,256]{1,0:T(8,128)}, f32[192,256]{1,0:T(8,128)}, f32[192,256]{1,0:T(8,128)}) custom-call(bf16[512,256]{1,0:T(8,128)(2,1)} %get-tuple-element.58.q_ref, bf16[512,256]{1,0:T(8,128)(2,1)} %get-tuple-element.59.k_ref, bf16[512,256]{1,0:T(8,128)(2,1)} %get-tuple-element.60.v_ref, ...), custom_call_target="tpu_custom_call" | custom-call | tf_op jit(solution)/shard_map/prepare/pallas_call | solution.py:370
  41.7 0.8 copy-done.1
  42.6 2.2 %relay.1 = (s32[8,4]{1,0:T(8,128)}, bf16[272,512]{1,0:T(8,128)(2,1)}, bf16[272,512]{1,0:T(8,128)(2,1)}, bf16[272,512]{1,0:T(8,128)(2,1)}, bf16[272,512]{1,0:T(8,128)(2,1)}) custom-call(s32[1]{0:T(128)} %bitcast.1.me_ref, bf16[528,512]{1,0:T(8,128)(2,1)} %copy-done.1, f32[192,256]{1,0:T(8,128)} %get-tuple-element.64.refs_0_), custom_call_target="tpu_custom_call" | custom-call | tf_op jit(solution)/shard_map/relay/pallas_call | solution.py:149
  44.8 1.6 %collective-permute-start.4 = (bf16[272,512]{1,0:T(8,128)(2,1)}, bf16[272,512]{1,0:T(8,128)(2,1)S(1)}, u32[]{:S(2)}, u32[]{:S(2)}) collective-permute-start(bf16[272,512]{1,0:T(8,128)(2,1)} %get-tuple-element.71), channel_id=1, source_target_pairs={{0,4},{4,0},{8,12},{12,8},{16,20},{20,16},{24,28},{28,24},{1,5},{5... | collective-permute-start | bytes 835592 | tf_op jit(solution)/shard_map/ppermute | solution.py:608
  46.4 1.6 %collective-permute-start.5 = (bf16[272,512]{1,0:T(8,128)(2,1)}, bf16[272,512]{1,0:T(8,128)(2,1)S(1)}, u32[]{:S(2)}, u32[]{:S(2)}) collective-permute-start(bf16[272,512]{1,0:T(8,128)(2,1)} %get-tuple-element.72), channel_id=1, source_target_pairs={{0,8},{4,12},{8,0},{12,4},{16,24},{20,28},{24,16},{28,20},{1,9},{5... | collective-permute-start | bytes 835592 | tf_op jit(solution)/shard_map/ppermute | solution.py:608
  48.0 0.4 collective-permute-start.6
  49.2 4.4 %attend.2 = (bf16[272,512]{1,0:T(8,128)(2,1)}, bf16[272,512]{1,0:T(8,128)(2,1)}, bf16[272,512]{1,0:T(8,128)(2,1)}, bf16[272,512]{1,0:T(8,128)(2,1)}) custom-call(bf16[1152,512]{1,0:T(8,128)(2,1)} %get-tuple-element.51.refs_0_.k_ref, bf16[1152,512]{1,0:T(8,128)(2,1)} %get-tuple-element.52.v_ref, bf16[272,512]{1,0:T(8,128)(2,1)} %get-tuple-element.53.refs_0_, ...), custom_call_target="tpu_custom_call" | custom-call | tf_op jit(solution)/shard_map/attend/pallas_call | solution.py:457
  53.6 6.4 %prepare.4 = (f32[192,256]{1,0:T(8,128)}, f32[192,256]{1,0:T(8,128)}, f32[192,256]{1,0:T(8,128)}, f32[192,256]{1,0:T(8,128)}) custom-call(bf16[512,256]{1,0:T(8,128)(2,1)} %get-tuple-element.58.q_ref, bf16[512,256]{1,0:T(8,128)(2,1)} %get-tuple-element.59.k_ref, bf16[512,256]{1,0:T(8,128)(2,1)} %get-tuple-element.60.v_ref, ...), custom_call_target="tpu_custom_call" | custom-call | tf_op jit(solution)/shard_map/prepare/pallas_call | solution.py:370
  60.0 0.7 copy-done.9
  60.8 4.3 %attend.3 = (bf16[272,512]{1,0:T(8,128)(2,1)}, bf16[272,512]{1,0:T(8,128)(2,1)}, bf16[272,512]{1,0:T(8,128)(2,1)}, bf16[272,512]{1,0:T(8,128)(2,1)}) custom-call(bf16[1152,512]{1,0:T(8,128)(2,1)} %get-tuple-element.51.refs_0_.k_ref, bf16[1152,512]{1,0:T(8,128)(2,1)} %get-tuple-element.52.v_ref, bf16[272,512]{1,0:T(8,128)(2,1)} %get-tuple-element.65.refs_4_.refs_0_, ...), custom_call_target="tpu_custom_call" | custom-call | tf_op jit(solution)/shard_map/attend/pallas_call | solution.py:457
  65.2 1.5 %collective-permute-start.7 = (bf16[272,512]{1,0:T(8,128)(2,1)}, bf16[272,512]{1,0:T(8,128)(2,1)S(1)}, u32[]{:S(2)}, u32[]{:S(2)}) collective-permute-start(bf16[272,512]{1,0:T(8,128)(2,1)} %get-tuple-element.76), channel_id=1, source_target_pairs={{0,4},{4,0},{8,12},{12,8},{16,20},{20,16},{24,28},{28,24},{1,5},{5... | collective-permute-start | bytes 835592 | tf_op jit(solution)/shard_map/ppermute | solution.py:608
  66.7 1.6 %collective-permute-start.8 = (bf16[272,512]{1,0:T(8,128)(2,1)}, bf16[272,512]{1,0:T(8,128)(2,1)S(1)}, u32[]{:S(2)}, u32[]{:S(2)}) collective-permute-start(bf16[272,512]{1,0:T(8,128)(2,1)} %get-tuple-element.77), channel_id=1, source_target_pairs={{0,8},{4,12},{8,0},{12,4},{16,24},{20,28},{24,16},{28,20},{1,9},{5... | collective-permute-start | bytes 835592 | tf_op jit(solution)/shard_map/ppermute | solution.py:608
  68.3 0.4 collective-permute-start.9
  68.7 5.7 %prepare.5 = (f32[128,256]{1,0:T(8,128)}, f32[128,256]{1,0:T(8,128)}, f32[128,256]{1,0:T(8,128)}, f32[128,256]{1,0:T(8,128)}) custom-call(bf16[512,256]{1,0:T(8,128)(2,1)} %get-tuple-element.58.q_ref, bf16[512,256]{1,0:T(8,128)(2,1)} %get-tuple-element.59.k_ref, bf16[512,256]{1,0:T(8,128)(2,1)} %get-tuple-element.60.v_ref, ...), custom_call_target="tpu_custom_call" | custom-call | tf_op jit(solution)/shard_map/prepare/pallas_call | solution.py:370
  74.4 1.7 %collective-permute-done.8.refs_2_ = bf16[272,512]{1,0:T(8,128)(2,1)S(1)} collective-permute-done((bf16[272,512]{1,0:T(8,128)(2,1)}, bf16[272,512]{1,0:T(8,128)(2,1)S(1)}, u32[]{:S(2)}, u32[]{:S(2)}) %collective-permute-start.8) | collective-permute-done | bytes 278560 | tf_op jit(solution)/shard_map/ppermute | solution.py:608
  76.0 2.9 %collective-permute-done.9.refs_3_ = bf16[272,512]{1,0:T(8,128)(2,1)S(1)} collective-permute-done((bf16[272,512]{1,0:T(8,128)(2,1)}, bf16[272,512]{1,0:T(8,128)(2,1)S(1)}, u32[]{:S(2)}, u32[]{:S(2)}) %collective-permute-start.9) | collective-permute-done | bytes 278560 | tf_op jit(solution)/shard_map/ppermute | solution.py:608
  79.0 0.7 copy-done.14
  79.7 2.4 %gather.1 = bf16[528,512]{1,0:T(8,128)(2,1)} custom-call(s32[1]{0:T(128)} %bitcast.1.me_ref, s32[8,4]{1,0:T(8,128)} %get-tuple-element.70.blk_ref, bf16[272,512]{1,0:T(8,128)(2,1)} %get-tuple-element.75.refs_0_, bf16[272,512]{1,0:T(8,128)(2,1)} %copy-done.12, bf16[272,512]{1,0:T(8,128)(2,1)} %copy-done.13, bf16[272,512]{1,0:T(8,128)(2,1)} %copy-done.14, ...), custom_call_target="tpu_custom_call" | custom-call | tf_op jit(solution)/shard_map/gather/pallas_call | solution.py:503
  82.5 1.5 %collective-permute-start.11 = (bf16[272,512]{1,0:T(8,128)(2,1)S(1)}, bf16[272,512]{1,0:T(8,128)(2,1)S(1)}, u32[]{:S(2)}, u32[]{:S(2)}) collective-permute-start(bf16[272,512]{1,0:T(8,128)(2,1)S(1)} %copy-done.26), channel_id=1, source_target_pairs={{0,4},{4,0},{8,12},{12,8},{16,20},{20,16},{24,28},{28,24},{1,5},{5... | collective-permute-start | bytes 835592 | tf_op jit(solution)/shard_map/ppermute | solution.py:608
  84.0 1.6 %collective-permute-start.12 = (bf16[272,512]{1,0:T(8,128)(2,1)S(1)}, bf16[272,512]{1,0:T(8,128)(2,1)S(1)}, u32[]{:S(2)}, u32[]{:S(2)}) collective-permute-start(bf16[272,512]{1,0:T(8,128)(2,1)S(1)} %copy-done.25), channel_id=1, source_target_pairs={{0,8},{4,12},{8,0},{12,4},{16,24},{20,28},{24,16},{28,20},{1,9},{5... | collective-permute-start | bytes 835592 | tf_op jit(solution)/shard_map/ppermute | solution.py:608
  86.0 4.5 %scan.1.refs_4_.refs_0_ = bf16[512,256]{1,0:T(8,128)(2,1)} custom-call(f32[1,256]{1,0:T(1,128)} %bitcast.8, f32[192,256]{1,0:T(8,128)} %get-tuple-element.64.refs_0_, f32[192,256]{1,0:T(8,128)} %get-tuple-element.85.refs_1_, f32[192,256]{1,0:T(8,128)} %get-tuple-element.86.refs_2_, f32[192,256]{1,0:T(8,128)} %get-tuple-element.87.refs_3_, ...), custom_call_target="tpu_custom_call" | custom-call | tf_op jit(solution)/shard_map/scan/pallas_call | solution.py:414
  90.4 1.4 %collective-permute-done.11.refs_1_ = bf16[272,512]{1,0:T(8,128)(2,1)S(1)} collective-permute-done((bf16[272,512]{1,0:T(8,128)(2,1)S(1)}, bf16[272,512]{1,0:T(8,128)(2,1)S(1)}, u32[]{:S(2)}, u32[]{:S(2)}) %collective-permute-start.11) | collective-permute-done | bytes 278560 | tf_op jit(solution)/shard_map/ppermute | solution.py:608
  91.8 8.2 %collective-permute-done.12.refs_2_ = bf16[272,512]{1,0:T(8,128)(2,1)S(1)} collective-permute-done((bf16[272,512]{1,0:T(8,128)(2,1)S(1)}, bf16[272,512]{1,0:T(8,128)(2,1)S(1)}, u32[]{:S(2)}, u32[]{:S(2)}) %collective-permute-start.12) | collective-permute-done | bytes 278560 | tf_op jit(solution)/shard_map/ppermute | solution.py:608
  100.1 3.0 %collective-permute-done.13.refs_3_ = bf16[272,512]{1,0:T(8,128)(2,1)S(1)} collective-permute-done((bf16[272,512]{1,0:T(8,128)(2,1)S(1)}, bf16[272,512]{1,0:T(8,128)(2,1)S(1)}, u32[]{:S(2)}, u32[]{:S(2)}) %collective-permute-start.13) | collective-permute-done | bytes 278560 | tf_op jit(solution)/shard_map/ppermute | solution.py:608
  103.1 2.5 %collective-permute-done.10.far_ref = bf16[528,512]{1,0:T(8,128)(2,1)S(1)} collective-permute-done((bf16[528,512]{1,0:T(8,128)(2,1)}, bf16[528,512]{1,0:T(8,128)(2,1)S(1)}, u32[]{:S(2)}, u32[]{:S(2)}) %collective-permute-start.10) | collective-permute-done | bytes 540704 | tf_op jit(solution)/shard_map/ppermute | solution.py:608
  105.5 0.8 copy-done.2
  106.3 2.8 %combine.1.refs_0_ = bf16[512,512]{1,0:T(8,128)(2,1)} custom-call(s32[1]{0:T(128)} %bitcast.1.me_ref, s32[8,4]{1,0:T(8,128)} %get-tuple-element.50.blk_ref, bf16[528,512]{1,0:T(8,128)(2,1)} %copy-done.2, bf16[272,512]{1,0:T(8,128)(2,1)} %get-tuple-element.81.refs_0_, bf16[272,512]{1,0:T(8,128)(2,1)} %copy-done.15, bf16[272,512]{1,0:T(8,128)(2,1)} %copy-done.16, ...), custom_call_target="tpu_custom_call" | custom-call | tf_op jit(solution)/shard_map/combine/pallas_call | solution.py:538
  109.2 1.5 %collective-permute-start.15 = (bf16[512,512]{1,0:T(8,128)(2,1)}, bf16[512,512]{1,0:T(8,128)(2,1)S(1)}, u32[]{:S(2)}, u32[]{:S(2)}) collective-permute-start(bf16[512,512]{1,0:T(8,128)(2,1)} %combine.1.refs_0_), channel_id=1, source_target_pairs={{0,2},{1,3},{2,0},{3,1},{4,6},{5,7},{6,4},{7,5},{8,10},{9,11},{10,... | collective-permute-start | bytes 1572872 | tf_op jit(solution)/shard_map/ppermute | solution.py:586
  110.7 0.5 collective-permute-start.18
  111.2 13.0 %collective-permute-done.15.refs_2_ = bf16[512,512]{1,0:T(8,128)(2,1)S(1)} collective-permute-done((bf16[512,512]{1,0:T(8,128)(2,1)}, bf16[512,512]{1,0:T(8,128)(2,1)S(1)}, u32[]{:S(2)}, u32[]{:S(2)}) %collective-permute-start.15) | collective-permute-done | bytes 524320 | tf_op jit(solution)/shard_map/ppermute | solution.py:586
  124.2 0.5 collective-permute-start.17
  124.7 3.1 %collective-permute-done.18.refs_2_ = bf16[512,256]{1,0:T(8,128)(2,1)S(1)} collective-permute-done((bf16[512,256]{1,0:T(8,128)(2,1)S(1)}, bf16[512,256]{1,0:T(8,128)(2,1)S(1)}, u32[]{:S(2)}, u32[]{:S(2)}) %collective-permute-start.18) | collective-permute-done | bytes 262176 | tf_op jit(solution)/shard_map/ppermute | solution.py:586
  127.8 1.5 %collective-permute-done.19.refs_3_ = bf16[512,256]{1,0:T(8,128)(2,1)S(1)} collective-permute-done((bf16[512,256]{1,0:T(8,128)(2,1)S(1)}, bf16[512,256]{1,0:T(8,128)(2,1)S(1)}, u32[]{:S(2)}, u32[]{:S(2)}) %collective-permute-start.19) | collective-permute-done | bytes 262176 | tf_op jit(solution)/shard_map/ppermute | solution.py:586
  129.3 0.7 copy-done.22
  130.0 3.2 %mixer_out.1.refs_6_ = f32[512,512]{1,0:T(8,128)} custom-call(s32[1]{0:T(128)} %bitcast.me_ref, bf16[512,256]{1,0:T(8,128)(2,1)} %scan.1.refs_4_.refs_0_, bf16[512,256]{1,0:T(8,128)(2,1)} %copy-done.21, bf16[512,256]{1,0:T(8,128)(2,1)} %copy-done.20, bf16[512,256]{1,0:T(8,128)(2,1)} %copy-done.22, bf16[1024,512]{1,0:T(8,128)(2,1)} %refs_4_.2), custom_call_target="tpu_custom_call" | custom-call | tf_op jit(solution)/shard_map/mixer_out/pallas_call | solution.py:571
  133.3 0.8 copy-done.4
  134.2 4.8 %final.1 = bf16[512,512]{1,0:T(8,128)(2,1)} custom-call(s32[1]{0:T(128)} %bitcast.me_ref, bf16[512,512]{1,0:T(8,128)(2,1)} %combine.1.refs_0_, bf16[512,512]{1,0:T(8,128)(2,1)} %copy-done.4, bf16[512,512]{1,0:T(8,128)(2,1)} %copy-done.3, bf16[512,512]{1,0:T(8,128)(2,1)} %copy-done.5, bf16[2048,512]{1,0:T(8,128)(2,1)} %refs_4_.3, ...), custom_call_target="tpu_custom_call" | custom-call | tf_op jit(solution)/shard_map/final/pallas_call | solution.py:571
  (64 shorter events, 2.0 us)
Async XLA Ops:
  1.3 13.6 %copy-start.23 = (f32[512,4]{0,1:T(4,128)S(1)}, f32[512,4]{0,1:T(4,128)}, u32[]{:S(2)}) copy-start(f32[512,4]{0,1:T(4,128)} %param.28) | copy-start | bytes 24580
  1.4 14.5 %copy-start.18 = (bf16[2048,64]{0,1:T(8,128)(2,1)S(1)}, bf16[2048,64]{0,1:T(8,128)(2,1)}, u32[]{:S(2)}) copy-start(bf16[2048,64]{0,1:T(8,128)(2,1)} %param.25) | copy-start | bytes 786436
  1.4 15.5 %copy-start.19 = (bf16[2048,64]{0,1:T(8,128)(2,1)S(1)}, bf16[2048,64]{0,1:T(8,128)(2,1)}, u32[]{:S(2)}) copy-start(bf16[2048,64]{0,1:T(8,128)(2,1)} %param.29) | copy-start | bytes 786436
  7.4 34.4 %collective-permute-start.3 = (bf16[528,512]{1,0:T(8,128)(2,1)}, bf16[528,512]{1,0:T(8,128)(2,1)S(1)}, u32[]{:S(2)}, u32[]{:S(2)}) collective-permute-start(bf16[528,512]{1,0:T(8,128)(2,1)} %get-tuple-element.57), channel_id=1, source_target_pairs={{0,16},{4,20},{8,24},{12,28},{16,0},{20,4},{24,8},{28,12},{1,17},{... | collective-permute-start | bytes 1622024 | tf_op jit(solution)/shard_map/ppermute | solution.py:608
  11.5 36.5 %collective-permute-start = (bf16[272,512]{1,0:T(8,128)(2,1)}, bf16[272,512]{1,0:T(8,128)(2,1)S(1)}, u32[]{:S(2)}, u32[]{:S(2)}) collective-permute-start(bf16[272,512]{1,0:T(8,128)(2,1)} %get-tuple-element.54), channel_id=1, source_target_pairs={{0,4},{4,0},{8,12},{12,8},{16,20},{20,16},{24,28},{28,24},{1,5},{5... | collective-permute-start | bytes 835592 | tf_op jit(solution)/shard_map/ppermute | solution.py:608
  13.0 35.4 %collective-permute-start.1 = (bf16[272,512]{1,0:T(8,128)(2,1)}, bf16[272,512]{1,0:T(8,128)(2,1)S(1)}, u32[]{:S(2)}, u32[]{:S(2)}) collective-permute-start(bf16[272,512]{1,0:T(8,128)(2,1)} %get-tuple-element.55), channel_id=1, source_target_pairs={{0,8},{4,12},{8,0},{12,4},{16,24},{20,28},{24,16},{28,20},{1,9},{5... | collective-permute-start | bytes 835592 | tf_op jit(solution)/shard_map/ppermute | solution.py:608
  14.6 33.8 %collective-permute-start.2 = (bf16[272,512]{1,0:T(8,128)(2,1)}, bf16[272,512]{1,0:T(8,128)(2,1)S(1)}, u32[]{:S(2)}, u32[]{:S(2)}) collective-permute-start(bf16[272,512]{1,0:T(8,128)(2,1)} %get-tuple-element.56), channel_id=1, source_target_pairs={{0,12},{4,8},{8,4},{12,0},{16,28},{20,24},{24,20},{28,16},{1,13},{... | collective-permute-start | bytes 835592 | tf_op jit(solution)/shard_map/ppermute | solution.py:608
  41.7 0.8 copy-start.1
  44.8 15.1 %collective-permute-start.4 = (bf16[272,512]{1,0:T(8,128)(2,1)}, bf16[272,512]{1,0:T(8,128)(2,1)S(1)}, u32[]{:S(2)}, u32[]{:S(2)}) collective-permute-start(bf16[272,512]{1,0:T(8,128)(2,1)} %get-tuple-element.71), channel_id=1, source_target_pairs={{0,4},{4,0},{8,12},{12,8},{16,20},{20,16},{24,28},{28,24},{1,5},{5... | collective-permute-start | bytes 835592 | tf_op jit(solution)/shard_map/ppermute | solution.py:608
  46.4 13.6 %collective-permute-start.5 = (bf16[272,512]{1,0:T(8,128)(2,1)}, bf16[272,512]{1,0:T(8,128)(2,1)S(1)}, u32[]{:S(2)}, u32[]{:S(2)}) collective-permute-start(bf16[272,512]{1,0:T(8,128)(2,1)} %get-tuple-element.72), channel_id=1, source_target_pairs={{0,8},{4,12},{8,0},{12,4},{16,24},{20,28},{24,16},{28,20},{1,9},{5... | collective-permute-start | bytes 835592 | tf_op jit(solution)/shard_map/ppermute | solution.py:608
  48.0 0.7 copy-start.6
  48.0 12.0 %collective-permute-start.6 = (bf16[272,512]{1,0:T(8,128)(2,1)}, bf16[272,512]{1,0:T(8,128)(2,1)S(1)}, u32[]{:S(2)}, u32[]{:S(2)}) collective-permute-start(bf16[272,512]{1,0:T(8,128)(2,1)} %get-tuple-element.73), channel_id=1, source_target_pairs={{0,12},{4,8},{8,4},{12,0},{16,28},{20,24},{24,20},{28,16},{1,13},{... | collective-permute-start | bytes 835592 | tf_op jit(solution)/shard_map/ppermute | solution.py:608
  48.4 0.7 copy-start.7
  48.4 0.8 copy-start.8
  60.0 0.7 copy-start.9
  60.0 0.8 copy-start.10
  60.0 0.9 copy-start.11
  65.2 9.2 %collective-permute-start.7 = (bf16[272,512]{1,0:T(8,128)(2,1)}, bf16[272,512]{1,0:T(8,128)(2,1)S(1)}, u32[]{:S(2)}, u32[]{:S(2)}) collective-permute-start(bf16[272,512]{1,0:T(8,128)(2,1)} %get-tuple-element.76), channel_id=1, source_target_pairs={{0,4},{4,0},{8,12},{12,8},{16,20},{20,16},{24,28},{28,24},{1,5},{5... | collective-permute-start | bytes 835592 | tf_op jit(solution)/shard_map/ppermute | solution.py:608
  66.7 9.4 %collective-permute-start.8 = (bf16[272,512]{1,0:T(8,128)(2,1)}, bf16[272,512]{1,0:T(8,128)(2,1)S(1)}, u32[]{:S(2)}, u32[]{:S(2)}) collective-permute-start(bf16[272,512]{1,0:T(8,128)(2,1)} %get-tuple-element.77), channel_id=1, source_target_pairs={{0,8},{4,12},{8,0},{12,4},{16,24},{20,28},{24,16},{28,20},{1,9},{5... | collective-permute-start | bytes 835592 | tf_op jit(solution)/shard_map/ppermute | solution.py:608
  68.3 10.7 %collective-permute-start.9 = (bf16[272,512]{1,0:T(8,128)(2,1)}, bf16[272,512]{1,0:T(8,128)(2,1)S(1)}, u32[]{:S(2)}, u32[]{:S(2)}) collective-permute-start(bf16[272,512]{1,0:T(8,128)(2,1)} %get-tuple-element.78), channel_id=1, source_target_pairs={{0,12},{4,8},{8,4},{12,0},{16,28},{20,24},{24,20},{28,16},{1,13},{... | collective-permute-start | bytes 835592 | tf_op jit(solution)/shard_map/ppermute | solution.py:608
  68.7 13.8 %copy-start.26 = (bf16[272,512]{1,0:T(8,128)(2,1)S(1)}, bf16[272,512]{1,0:T(8,128)(2,1)}, u32[]{:S(2)}) copy-start(bf16[272,512]{1,0:T(8,128)(2,1)} %get-tuple-element.82) | copy-start | bytes 835588
  68.7 15.3 %copy-start.25 = (bf16[272,512]{1,0:T(8,128)(2,1)S(1)}, bf16[272,512]{1,0:T(8,128)(2,1)}, u32[]{:S(2)}) copy-start(bf16[272,512]{1,0:T(8,128)(2,1)} %get-tuple-element.83) | copy-start | bytes 835588
  68.7 16.9 %copy-start.24 = (bf16[272,512]{1,0:T(8,128)(2,1)S(1)}, bf16[272,512]{1,0:T(8,128)(2,1)}, u32[]{:S(2)}) copy-start(bf16[272,512]{1,0:T(8,128)(2,1)} %get-tuple-element.84) | copy-start | bytes 835588
  74.4 4.6 %copy-start.12 = (bf16[272,512]{1,0:T(8,128)(2,1)}, bf16[272,512]{1,0:T(8,128)(2,1)S(1)}, u32[]{:S(2)}) copy-start(bf16[272,512]{1,0:T(8,128)(2,1)S(1)} %collective-permute-done.7.refs_1_) | copy-start | bytes 835588
  76.0 3.0 %copy-start.13 = (bf16[272,512]{1,0:T(8,128)(2,1)}, bf16[272,512]{1,0:T(8,128)(2,1)S(1)}, u32[]{:S(2)}) copy-start(bf16[272,512]{1,0:T(8,128)(2,1)S(1)} %collective-permute-done.8.refs_2_) | copy-start | bytes 835588
  79.0 0.7 copy-start.14
  82.1 23.4 %collective-permute-start.10 = (bf16[528,512]{1,0:T(8,128)(2,1)}, bf16[528,512]{1,0:T(8,128)(2,1)S(1)}, u32[]{:S(2)}, u32[]{:S(2)}) collective-permute-start(bf16[528,512]{1,0:T(8,128)(2,1)} %gather.1), channel_id=1, source_target_pairs={{0,16},{4,20},{8,24},{12,28},{16,0},{20,4},{24,8},{28,12},{1,17},{... | collective-permute-start | bytes 1622024 | tf_op jit(solution)/shard_map/ppermute | solution.py:608
  82.5 9.4 %collective-permute-start.11 = (bf16[272,512]{1,0:T(8,128)(2,1)S(1)}, bf16[272,512]{1,0:T(8,128)(2,1)S(1)}, u32[]{:S(2)}, u32[]{:S(2)}) collective-permute-start(bf16[272,512]{1,0:T(8,128)(2,1)S(1)} %copy-done.26), channel_id=1, source_target_pairs={{0,4},{4,0},{8,12},{12,8},{16,20},{20,16},{24,28},{28,24},{1,5},{5... | collective-permute-start | bytes 835592 | tf_op jit(solution)/shard_map/ppermute | solution.py:608
  84.0 16.1 %collective-permute-start.12 = (bf16[272,512]{1,0:T(8,128)(2,1)S(1)}, bf16[272,512]{1,0:T(8,128)(2,1)S(1)}, u32[]{:S(2)}, u32[]{:S(2)}) collective-permute-start(bf16[272,512]{1,0:T(8,128)(2,1)S(1)} %copy-done.25), channel_id=1, source_target_pairs={{0,8},{4,12},{8,0},{12,4},{16,24},{20,28},{24,16},{28,20},{1,9},{5... | collective-permute-start | bytes 835592 | tf_op jit(solution)/shard_map/ppermute | solution.py:608
  85.5 17.5 %collective-permute-start.13 = (bf16[272,512]{1,0:T(8,128)(2,1)S(1)}, bf16[272,512]{1,0:T(8,128)(2,1)S(1)}, u32[]{:S(2)}, u32[]{:S(2)}) collective-permute-start(bf16[272,512]{1,0:T(8,128)(2,1)S(1)} %copy-done.24), channel_id=1, source_target_pairs={{0,12},{4,8},{8,4},{12,0},{16,28},{20,24},{24,20},{28,16},{1,13},{... | collective-permute-start | bytes 835592 | tf_op jit(solution)/shard_map/ppermute | solution.py:608
  90.4 20.2 %copy-start = (bf16[512,256]{1,0:T(8,128)(2,1)S(1)}, bf16[512,256]{1,0:T(8,128)(2,1)}, u32[]{:S(2)}) copy-start(bf16[512,256]{1,0:T(8,128)(2,1)} %scan.1.refs_4_.refs_0_) | copy-start | bytes 786436
  91.8 13.7 %copy-start.15 = (bf16[272,512]{1,0:T(8,128)(2,1)}, bf16[272,512]{1,0:T(8,128)(2,1)S(1)}, u32[]{:S(2)}) copy-start(bf16[272,512]{1,0:T(8,128)(2,1)S(1)} %collective-permute-done.11.refs_1_) | copy-start | bytes 835588
  100.1 5.5 %copy-start.16 = (bf16[272,512]{1,0:T(8,128)(2,1)}, bf16[272,512]{1,0:T(8,128)(2,1)S(1)}, u32[]{:S(2)}) copy-start(bf16[272,512]{1,0:T(8,128)(2,1)S(1)} %collective-permute-done.12.refs_2_) | copy-start | bytes 835588
  103.1 2.5 %copy-start.17 = (bf16[272,512]{1,0:T(8,128)(2,1)}, bf16[272,512]{1,0:T(8,128)(2,1)S(1)}, u32[]{:S(2)}) copy-start(bf16[272,512]{1,0:T(8,128)(2,1)S(1)} %collective-permute-done.13.refs_3_) | copy-start | bytes 835588
  105.5 0.8 copy-start.2
  109.2 15.0 %collective-permute-start.15 = (bf16[512,512]{1,0:T(8,128)(2,1)}, bf16[512,512]{1,0:T(8,128)(2,1)S(1)}, u32[]{:S(2)}, u32[]{:S(2)}) collective-permute-start(bf16[512,512]{1,0:T(8,128)(2,1)} %combine.1.refs_0_), channel_id=1, source_target_pairs={{0,2},{1,3},{2,0},{3,1},{4,6},{5,7},{6,4},{7,5},{8,10},{9,11},{10,... | collective-permute-start | bytes 1572872 | tf_op jit(solution)/shard_map/ppermute | solution.py:586
  110.7 17.1 %collective-permute-start.18 = (bf16[512,256]{1,0:T(8,128)(2,1)S(1)}, bf16[512,256]{1,0:T(8,128)(2,1)S(1)}, u32[]{:S(2)}, u32[]{:S(2)}) collective-permute-start(bf16[512,256]{1,0:T(8,128)(2,1)S(1)} %copy-done), channel_id=1, source_target_pairs={{0,2},{1,3},{2,0},{3,1},{4,6},{5,7},{6,4},{7,5},{8,10},{9,11},{10,... | collective-permute-start | bytes 786440 | tf_op jit(solution)/shard_map/ppermute | solution.py:586
  111.2 22.1 %collective-permute-start.14 = (bf16[512,512]{1,0:T(8,128)(2,1)}, bf16[512,512]{1,0:T(8,128)(2,1)S(1)}, u32[]{:S(2)}, u32[]{:S(2)}) collective-permute-start(bf16[512,512]{1,0:T(8,128)(2,1)} %combine.1.refs_0_), channel_id=1, source_target_pairs={{0,1},{1,0},{2,3},{3,2},{4,5},{5,4},{6,7},{7,6},{8,9},{9,8},{10,11... | collective-permute-start | bytes 1572872 | tf_op jit(solution)/shard_map/ppermute | solution.py:586
  124.2 9.1 %copy-start.3 = (bf16[512,512]{1,0:T(8,128)(2,1)}, bf16[512,512]{1,0:T(8,128)(2,1)S(1)}, u32[]{:S(2)}) copy-start(bf16[512,512]{1,0:T(8,128)(2,1)S(1)} %collective-permute-done.15.refs_2_) | copy-start | bytes 1572868
  124.2 9.1 %collective-permute-start.16 = (bf16[512,512]{1,0:T(8,128)(2,1)S(1)}, bf16[512,512]{1,0:T(8,128)(2,1)S(1)}, u32[]{:S(2)}, u32[]{:S(2)}) collective-permute-start(bf16[512,512]{1,0:T(8,128)(2,1)S(1)} %collective-permute-done.15.refs_2_), channel_id=1, source_target_pairs={{0,1},{1,0},{2,3},{3,2},{4,5},{5,4},{6,7},{7,6},{8,9},{9,8},{10,11... | collective-permute-start | bytes 1572872 | tf_op jit(solution)/shard_map/ppermute | solution.py:586
  124.2 3.6 %collective-permute-start.17 = (bf16[512,256]{1,0:T(8,128)(2,1)S(1)}, bf16[512,256]{1,0:T(8,128)(2,1)S(1)}, u32[]{:S(2)}, u32[]{:S(2)}) collective-permute-start(bf16[512,256]{1,0:T(8,128)(2,1)S(1)} %copy-done), channel_id=1, source_target_pairs={{0,1},{1,0},{2,3},{3,2},{4,5},{5,4},{6,7},{7,6},{8,9},{9,8},{10,11... | collective-permute-start | bytes 786440 | tf_op jit(solution)/shard_map/ppermute | solution.py:586
  127.8 1.5 %copy-start.20 = (bf16[512,256]{1,0:T(8,128)(2,1)}, bf16[512,256]{1,0:T(8,128)(2,1)S(1)}, u32[]{:S(2)}) copy-start(bf16[512,256]{1,0:T(8,128)(2,1)S(1)} %collective-permute-done.18.refs_2_) | copy-start | bytes 786436
  127.8 1.5 %collective-permute-start.19 = (bf16[512,256]{1,0:T(8,128)(2,1)S(1)}, bf16[512,256]{1,0:T(8,128)(2,1)S(1)}, u32[]{:S(2)}, u32[]{:S(2)}) collective-permute-start(bf16[512,256]{1,0:T(8,128)(2,1)S(1)} %collective-permute-done.18.refs_2_), channel_id=1, source_target_pairs={{0,1},{1,0},{2,3},{3,2},{4,5},{5,4},{6,7},{7,6},{8,9},{9,8},{10,11... | collective-permute-start | bytes 786440 | tf_op jit(solution)/shard_map/ppermute | solution.py:586
  127.8 1.5 %copy-start.21 = (bf16[512,256]{1,0:T(8,128)(2,1)}, bf16[512,256]{1,0:T(8,128)(2,1)S(1)}, u32[]{:S(2)}) copy-start(bf16[512,256]{1,0:T(8,128)(2,1)S(1)} %collective-permute-done.17.refs_1_) | copy-start | bytes 786436
  129.3 0.7 copy-start.22
  133.3 0.8 copy-start.4
  133.3 1.0 copy-start.5

commit v3 on v2

v3 whole, which is shorter than its diff:
```python
import functools
import jax
import jax.numpy as jnp
from jax import lax
from jax.experimental import pallas as pl
from jax.experimental.pallas import tpu as pltpu
from jax.sharding import PartitionSpec as P


XHEAD = 256
QBLOCK = 64
MBLOCK = 64
RHEAD = 64
LROWS = 16

FLOAT32 = jnp.float32
BFLOAT = jnp.bfloat16
PRECISE = lax.Precision.HIGHEST
VMEM = pltpu.VMEM
SMEM = pltpu.SMEM
GRANT = pltpu.CompilerParams(vmem_limit_bytes=14 * 1024 * 1024)
NT = (((1,), (1,)), ((), ()))
NN = (((1,), (0,)), ((), ()))
TN = (((0,), (0,)), ((), ()))


def dot(left, right, dims=NN, precision=None):
    return lax.dot_general(left, right, dims, precision=precision, preferred_element_type=FLOAT32)


def iota(shape, dim):
    return lax.broadcasted_iota(jnp.int32, shape, dim)


def whole(count):
    return [pl.BlockSpec(memory_space=VMEM)] * count


def in_hbm(*arrays):
    return [pltpu.with_memory_space_constraint(a, pltpu.HBM) for a in arrays]


def near_core(*arrays):
    return [pltpu.with_memory_space_constraint(a, VMEM) for a in arrays]


def after(count):
    return [pl.BlockSpec(memory_space=pl.ANY)] * count


def up16(count):
    return -(-count // 16) * 16


def entry(lines, row, lane):
    hit = (iota(lines.shape, 0) == row) & (iota(lines.shape, 1) == lane)
    return jnp.sum(jnp.where(hit, lines, 0.0)).astype(jnp.int32)


def write_group(out_ref, q_ref, blocks, passages):
    capacity = len(blocks)
    width = out_ref.shape[1]
    line = jnp.zeros((LROWS, width), FLOAT32)
    row, lane = iota(line.shape, 0), iota(line.shape, 1)
    for r in range(capacity):
        start = pl.multiple_of(jnp.maximum(blocks[r] - 1, 0) * QBLOCK, QBLOCK)
        out_ref[r * QBLOCK : (r + 1) * QBLOCK, :] = q_ref[pl.ds(start, QBLOCK), :]
        line = jnp.where((row == 0) & (lane == r), passages[r].astype(FLOAT32), line)
    out_ref[capacity * QBLOCK :, :] = line.astype(BFLOAT)


def query_kernel(pass_dev, owners, me_ref, ids_ref, tok_ref, w_ref, gain_ref, blk_ref, *refs):
    capacity = blk_ref.shape[1]
    per_block = ids_ref.shape[0]
    rows, width = tok_ref.shape[0], w_ref.shape[1]
    heads = width // XHEAD
    q_refs, group_refs = refs[:heads], refs[heads:-4]
    pidx_ref, fill_ref, sum_ref, all_ref = refs[-4:]
    step = pl.program_id(0)

    @pl.when(step == 0)
    def _():
        def clear(o, carry):
            fill_ref[o] = 0
            for r in range(capacity):
                pidx_ref[o, r] = 0
                blk_ref[o, r] = 0
            return carry

        lax.fori_loop(0, owners, clear, 0)

        def put(n, carry):
            passage = ids_ref[n % per_block, n // per_block]
            owner = passage // pass_dev
            rank = fill_ref[owner]
            fill_ref[owner] = rank + 1
            pidx_ref[owner, rank] = passage - owner * pass_dev
            blk_ref[owner, rank] = n // per_block + 1
            return carry

        lax.fori_loop(0, ids_ref.shape[1] * per_block, put, 0)
        sum_ref[...] = jnp.zeros_like(sum_ref)

    sum_ref[...] += dot(tok_ref[...], w_ref[...])

    @pl.when(step == pl.num_programs(0) - 1)
    def _():
        tail = q_refs[0].shape[0] - rows
        row, lane = iota((tail, 128), 0), iota((tail, 128), 1)

        def line(o, table):
            for r in range(capacity):
                table = jnp.where((row == o) & (lane == r), blk_ref[o, r].astype(FLOAT32), table)
                table = jnp.where((row == o) & (lane == capacity + r),
                                  pidx_ref[o, r].astype(FLOAT32), table)
            return table

        table = lax.fori_loop(0, owners, line, jnp.zeros((tail, 128), FLOAT32)).astype(BFLOAT)
        for h, q_ref in enumerate(q_refs):
            cols = slice(h * XHEAD, (h + 1) * XHEAD)
            raw = sum_ref[:, cols]
            scale = lax.rsqrt(jnp.mean(raw * raw, axis=-1, keepdims=True) + 1e-06)
            value = (raw * scale * gain_ref[:, cols]).astype(BFLOAT)
            q_ref[:rows, :] = value
            all_ref[:, cols] = value
            q_ref[rows:, :] = jnp.concatenate([table, jnp.zeros_like(table)], axis=1)
        for k, ref in enumerate(group_refs):
            owner = me_ref[0] ^ k
            write_group(ref, all_ref, [blk_ref[owner, r] for r in range(capacity)],
                        [pidx_ref[owner, r] for r in range(capacity)])


def make_queries(me, ids, owners, capacity, pass_dev, tokens, cross_query, score_gain):
    rows, width = tokens.shape[0], cross_query.shape[1]
    smem = pl.BlockSpec(memory_space=SMEM)
    group = VMEM((capacity * QBLOCK + LROWS, width), BFLOAT)
    count, heads = owners // 2, width // XHEAD
    steps = 4
    depth = tokens.shape[1] // steps
    outs = pl.pallas_call(
        functools.partial(query_kernel, pass_dev, owners),
        grid=(steps,),
        out_shape=[jax.ShapeDtypeStruct((owners, capacity), jnp.int32)]
        + [VMEM((rows + up16(owners), XHEAD), BFLOAT)] * heads + [group] * count,
        in_specs=[smem, smem, pl.BlockSpec((rows, depth), lambda i: (0, i)),
                  pl.BlockSpec((depth, width), lambda i: (i, 0))] + whole(1),
        out_specs=[smem] + whole(heads + count),
        scratch_shapes=[SMEM((owners, capacity), jnp.int32), SMEM((owners,), jnp.int32),
                        VMEM((rows, width), FLOAT32), VMEM((rows, width), BFLOAT)],
        compiler_params=GRANT,
        name="queries",
    )(me, *in_hbm(ids.T, tokens, cross_query, score_gain.reshape(1, -1)))
    return outs[0], outs[1 : 1 + heads], outs[1 + heads :]


def relay_kernel(rows, deps, me_ref, q_ref, *refs):
    blk_ref, *group_refs = refs[deps:]
    _, capacity = blk_ref.shape
    table = q_ref[rows:, :128].astype(FLOAT32)
    for k, ref in enumerate(group_refs):
        owner = me_ref[0] ^ k
        blocks = [entry(table, owner, r) for r in range(capacity)]
        for r in range(capacity):
            blk_ref[owner, r] = blocks[r]
        write_group(ref, q_ref, blocks, [entry(table, owner, capacity + r) for r in range(capacity)])


def relay(me, queries, rows, owners, capacity, deps):
    width = queries.shape[1]
    smem = pl.BlockSpec(memory_space=SMEM)
    group = VMEM((capacity * QBLOCK + LROWS, width), BFLOAT)
    count = owners // 2
    outs = pl.pallas_call(
        functools.partial(relay_kernel, rows, len(deps)),
        out_shape=[jax.ShapeDtypeStruct((owners, capacity), jnp.int32)] + [group] * count,
        in_specs=[smem] + whole(1) + after(len(deps)),
        out_specs=[smem] + whole(count),
        compiler_params=GRANT,
        name="relay",
    )(me, *near_core(queries), *deps)
    return outs[0], outs[1:]


def keyval_kernel(rows_ref, wk_ref, wv_ref, k_ref, v_ref):
    width = wk_ref.shape[1]
    rows = rows_ref[...]
    mine = pl.ds(pl.multiple_of(pl.program_id(0) * rows.shape[0], 16), rows.shape[0])
    for h in range(width // XHEAD):
        cols = slice(h * XHEAD, (h + 1) * XHEAD)
        raw = dot(rows, wk_ref[:, cols])
        scale = lax.rsqrt(jnp.mean(raw * raw, axis=-1, keepdims=True) + 1e-06)
        k_ref[mine, cols] = (raw * scale).astype(BFLOAT)
        v_ref[mine, cols] = dot(rows, wv_ref[:, cols]).astype(BFLOAT)


def make_keyvals(store, passage_key, passage_value):
    pass_dev, plen, model = store.shape
    width = passage_key.shape[1]
    group = max(g for g in range(1, 5) if pass_dev % g == 0)
    tile = group * plen
    shape = VMEM((pass_dev * plen, width), BFLOAT)
    return pl.pallas_call(
        keyval_kernel,
        grid=(pass_dev // group,),
        out_shape=[shape, shape],
        in_specs=[pl.BlockSpec((tile, model), lambda i: (i, 0))] + whole(2),
        out_specs=whole(2),
        compiler_params=GRANT,
        name="keyvals",
    )(*in_hbm(store.reshape(-1, model)), *near_core(passage_key, passage_value))


def project_kernel(
    tok_ref, mq_ref, mk_ref, mv_ref, dl_ref, rl_ref, gd_ref, du_ref, ru_ref, gu_ref,
    base_ref, shift_ref, dep_ref,
    q_ref, k_ref, v_ref, u_ref, rk_ref, lf_ref, gate_ref,
):
    tokens = tok_ref[...]
    width = mq_ref.shape[1]
    rank = dl_ref.shape[0]
    lows = dot(tokens, jnp.concatenate([dl_ref[...], rl_ref[...]], axis=0), NT)
    decay_low = jnp.tanh(lows[:, :rank]).astype(BFLOAT)
    rate_low = lows[:, rank:].astype(BFLOAT)
    gate_low = dot(tokens, gd_ref[...]).astype(BFLOAT)
    gate_ref[...] = jax.nn.sigmoid(dot(gate_low, gu_ref[...]))
    pre = base_ref[...] + dot(decay_low, du_ref[...])
    heads = shift_ref.shape[0]
    owner = (iota((heads, width), 0) == iota((heads, width), 1) // RHEAD).astype(FLOAT32)
    shift = dot(shift_ref[...], owner, TN, precision=PRECISE)
    lf_ref[...] = -jax.nn.sigmoid(pre + shift) * (2.718281828459045 ** -0.5)
    q_ref[...] = dot(tokens, mq_ref[...]).astype(BFLOAT)
    v_ref[...] = dot(tokens, mv_ref[...]).astype(BFLOAT)
    key = dot(tokens, mk_ref[...]).astype(BFLOAT)
    k_ref[...] = key
    key = key.astype(FLOAT32)
    same = (iota((width, width), 0) // RHEAD == iota((width, width), 1) // RHEAD).astype(FLOAT32)
    unit = key * lax.rsqrt(dot(key * key, same, precision=PRECISE) + 1e-06)
    u_ref[...] = unit
    rk_ref[...] = unit * jax.nn.sigmoid(dot(rate_low, ru_ref[...]))


def project(tokens, mix_query, mix_key, mix_value, decay_lower, decay_upper, decay_base,
            decay_shift, rate_lower, rate_upper, gate_down, gate_up, deps):
    rows = tokens.shape[0]
    width = mix_query.shape[1]
    half = VMEM((rows, width), BFLOAT)
    full = VMEM((rows, width), FLOAT32)
    return pl.pallas_call(
        project_kernel,
        out_shape=[half, half, half, full, full, full,
                   VMEM((rows, gate_up.shape[1]), FLOAT32)],
        in_specs=whole(12) + after(len(deps)),
        out_specs=whole(7),
        compiler_params=GRANT,
        name="project",
    )(*near_core(tokens, mix_query, mix_key, mix_value), decay_lower.T, rate_lower.T, gate_down,
      decay_upper, rate_upper, gate_up, decay_base.reshape(1, -1), decay_shift.T, *deps)


def parts2(value):
    high = value.astype(BFLOAT)
    return high, (value - high.astype(FLOAT32)).astype(BFLOAT)


def parts3(value):
    high = value.astype(BFLOAT)
    rest = value - high.astype(FLOAT32)
    return (high,) + parts2(rest)


def spread(value):
    rows, width = value.shape
    lane = iota((1, 128), 1) // RHEAD
    blank = jnp.zeros((rows, 128), value.dtype)
    blocks = []
    for h in range(width // RHEAD):
        mine = (h * RHEAD) // 128
        keep = (lane == h % (128 // RHEAD)).astype(value.dtype)
        cells = [blank] * (width // 128)
        cells[mine] = value[:, mine * 128 : (mine + 1) * 128] * keep
        blocks.append(jnp.concatenate(cells, axis=1) if len(cells) > 1 else cells[0])
    return jnp.concatenate(blocks, axis=0)


def fold(value):
    width = value.shape[1]
    lane = iota((1, 128), 1) // RHEAD
    cells = []
    for t in range(width // 128):
        cell = value[t * 128 : t * 128 + RHEAD, t * 128 : (t + 1) * 128]
        for p in range(1, 128 // RHEAD):
            start = t * 128 + p * RHEAD
            cell = jnp.where(lane == p, value[start : start + RHEAD, t * 128 : (t + 1) * 128], cell)
        cells.append(cell)
    return jnp.concatenate(cells, axis=1) if len(cells) > 1 else cells[0]


def left_of(value):
    high, low = parts2(value)
    return jnp.concatenate([high, low, high], axis=1)


def right_of(value):
    high, low = parts2(value)
    high, low = spread(high), spread(low)
    return jnp.concatenate([high, high, low], axis=0)


def right_nt(value):
    high, low = parts2(value)
    high, low = spread(high), spread(low)
    return jnp.concatenate([high, high, low], axis=1)


def across(left, right):
    lh, ll = parts2(left)
    rh, rl = parts2(right)
    return fold(dot(jnp.concatenate([lh, ll, lh], axis=0), jnp.concatenate([rh, rh, rl], axis=0), TN))


def prepare_chunks(queries, keys, values, units, rate_keys, fades):
    n = range(len(queries))
    length, width = queries[0].shape
    row = iota((length, width), 0)
    col = iota((length, width), 1) % RHEAD
    lower = (iota((length, length), 1) <= iota((length, length), 0)).astype(BFLOAT)
    cumul = []
    for c in n:
        sums = dot(lower, jnp.concatenate(parts3(fades[c]), axis=1))
        cumul.append(sums[:, :width] + sums[:, width : 2 * width] + sums[:, 2 * width :])
    ends = [cumul[c][length - 1 :, :] for c in n]
    grown = [jnp.exp(-cumul[c]) for c in n]
    pulled = [-units[c] * jnp.exp(cumul[c] - fades[c]) for c in n]
    read = [queries[c] * jnp.exp(cumul[c]) for c in n]
    both = [left_of(jnp.concatenate([pulled[c], read[c]], axis=0)) for c in n]
    from_rate = [dot(both[c], right_nt(rate_keys[c] * grown[c]), NT) for c in n]
    from_key = [dot(both[c], right_nt(keys[c] * grown[c]), NT) for c in n]
    strict, upto = col < row, col <= row
    rate_pull = [jnp.where(strict, from_rate[c][:length], 0.0) for c in n]
    rate_read = [left_of(jnp.where(upto, from_rate[c][length:], 0.0)) for c in n]
    key_both = [
        left_of(jnp.concatenate([jnp.where(strict, from_key[c][:length], 0.0),
                                 jnp.where(upto, from_key[c][length:], 0.0)], axis=0)) for c in n]

    def pick(size):
        return (row // (2 * size) == col // (2 * size)) & (row // size > col // size)

    first = pick(1)
    eye = (row == col).astype(FLOAT32)
    inverse = [eye + jnp.where(first, rate_pull[c], 0.0) for c in n]
    size = 2
    while size < length:
        keep = pick(size)
        mids = [dot(left_of(inverse[c]), right_of(jnp.where(keep, rate_pull[c], 0.0))) for c in n]
        adds = [dot(left_of(mids[c]), right_of(inverse[c])) for c in n]
        inverse = [inverse[c] + adds[c] for c in n]
        size *= 2
    inverse = [left_of(inverse[c]) for c in n]
    from_value = []
    for c in n:
        wide = spread(values[c])
        from_value.append(dot(key_both[c][:, : 2 * width], jnp.concatenate([wide, wide], axis=0)))
    moved = [dot(inverse[c], right_of(pulled[c])) for c in n]
    base = [dot(inverse[c], right_of(from_value[c][:length])) for c in n]
    query_end = [read[c] + dot(rate_read[c], right_of(moved[c])) for c in n]
    out_base = [from_value[c][length:] + dot(rate_read[c], right_of(base[c])) for c in n]
    left = [jnp.exp(ends[c] - cumul[c]) for c in n]
    step, add = [], []
    diag = iota((RHEAD, width), 0) == iota((RHEAD, width), 1) % RHEAD
    for c in n:
        rate_left = rate_keys[c] * left[c]
        step.append(jnp.where(diag, jnp.exp(ends[c]), 0.0) + across(moved[c], rate_left))
        add.append(across(jnp.concatenate([values[c].astype(FLOAT32), base[c]], axis=0),
                          jnp.concatenate([keys[c] * left[c], rate_left], axis=0)))
    return query_end, out_base, step, add


def prepare_kernel(start, deps, q_ref, k_ref, v_ref, u_ref, rk_ref, lf_ref, *refs):
    outs = refs[deps:]
    count = outs[0].shape[0] // MBLOCK
    spans = [slice((start + c) * MBLOCK, (start + c + 1) * MBLOCK) for c in range(count)]
    results = prepare_chunks(
        [q_ref[s].astype(FLOAT32) for s in spans], [k_ref[s].astype(FLOAT32) for s in spans],
        [v_ref[s] for s in spans], [u_ref[s] for s in spans], [rk_ref[s] for s in spans],
        [lf_ref[s] for s in spans])
    for ref, values in zip(outs, results):
        for c, value in enumerate(values):
            ref[c * MBLOCK : (c + 1) * MBLOCK] = value


def prepare(inputs, start, count, deps):
    width = inputs[0].shape[1]
    full = VMEM((count * MBLOCK, width), FLOAT32)
    return pl.pallas_call(
        functools.partial(prepare_kernel, start, len(deps)),
        out_shape=[full] * 4,
        in_specs=whole(6) + after(len(deps)),
        out_specs=whole(4),
        compiler_params=GRANT,
        name="prepare",
    )(*near_core(*inputs), *deps)


def head_mean(value, same):
    high, low = parts2(value)
    return dot(jnp.concatenate([high, low], axis=1), same) * (1.0 / RHEAD)


def scan_kernel(deps, pieces, gain_ref, *refs):
    prepared = [refs[4 * p : 4 * p + 4] for p in range(pieces)]
    out_ref, raw_ref = refs[4 * pieces + deps :]
    width = out_ref.shape[1]
    same = (iota((width, width), 0) // RHEAD == iota((width, width), 1) // RHEAD).astype(BFLOAT)
    same = jnp.concatenate([same, same], axis=0)
    state = None
    done = 0
    for qe_ref, ob_ref, st_ref, ad_ref in prepared:
        for c in range(qe_ref.shape[0] // MBLOCK):
            rows = slice(c * MBLOCK, (c + 1) * MBLOCK)
            out = ob_ref[rows, :]
            if state is None:
                state = ad_ref[rows, :]
            else:
                out = out + dot(left_of(qe_ref[rows, :]), right_nt(state), NT)
                state = dot(left_of(state), right_of(st_ref[rows, :])) + ad_ref[rows, :]
            raw_ref[done : done + MBLOCK, :] = out
            done += MBLOCK
    raw = raw_ref[...]
    centred = raw - head_mean(raw, same)
    var = head_mean(centred * centred, same)
    out_ref[...] = (centred * lax.rsqrt(var + 0.00064) * gain_ref[...]).astype(BFLOAT)


def scan(prepared, norm_gain, deps):
    width = prepared[0][0].shape[1]
    rows = sum(p[0].shape[0] for p in prepared)
    flat = [a for p in prepared for a in p]
    return pl.pallas_call(
        functools.partial(scan_kernel, len(deps), len(prepared)),
        out_shape=VMEM((rows, width), BFLOAT),
        in_specs=whole(1 + len(flat)) + after(len(deps)),
        out_specs=pl.BlockSpec(memory_space=VMEM),
        scratch_shapes=[VMEM((rows, width), FLOAT32)],
        compiler_params=GRANT,
        name="scan",
    )(norm_gain.reshape(1, -1), *near_core(*flat), *deps)


def attend_group(plen, first, q_ref, k_ref, v_ref, out_ref):
    width = q_ref.shape[1]
    heads = width // XHEAD
    capacity = (q_ref.shape[0] - LROWS) // QBLOCK
    line = q_ref[capacity * QBLOCK :, :128].astype(FLOAT32)
    units = [(r, h) for r in range(capacity) for h in range(heads)]
    spans = [pl.ds(pl.multiple_of(entry(line, 0, r) * plen, plen), plen) for r in range(capacity)]
    mine = [slice(r * QBLOCK, (r + 1) * QBLOCK) for r in range(capacity)]
    cols = [slice(h * XHEAD, (h + 1) * XHEAD) for h in range(heads)]
    held = [slice((first + h) * XHEAD, (first + h + 1) * XHEAD) for h in range(heads)]
    scores = [dot(q_ref[mine[r], cols[h]], k_ref[spans[r], held[h]], NT) for r, h in units]
    expon = [jnp.exp(s * XHEAD ** (-0.5)).astype(BFLOAT) for s in scores]
    ones = jnp.ones((8, plen), BFLOAT)
    totals = [dot(ones, e, NT)[:1] for e in expon]
    outs = [dot(e, v_ref[spans[r], held[h]]) for e, (r, h) in zip(expon, units)]
    sums = jnp.zeros((LROWS, QBLOCK), FLOAT32)
    rowid = iota((LROWS, QBLOCK), 0)
    for (r, h), out, total in zip(units, outs, totals):
        out_ref[mine[r], cols[h]] = out.astype(BFLOAT)
        high = total.astype(BFLOAT).astype(FLOAT32)
        where = 2 * (r * heads + h)
        sums = jnp.where(rowid == where, high, sums)
        sums = jnp.where(rowid == where + 1, total - high, sums)
    out_ref[capacity * QBLOCK :, :] = jnp.zeros((LROWS, width), BFLOAT)
    out_ref[capacity * QBLOCK :, :QBLOCK] = sums.astype(BFLOAT)


def attend_kernel(plen, first, count, deps, k_ref, v_ref, *refs):
    for q_ref, out_ref in zip(refs[:count], refs[count + deps :]):
        attend_group(plen, first, q_ref, k_ref, v_ref, out_ref)


def attend(groups, keys, values, plen, first, deps):
    count = len(groups)
    return pl.pallas_call(
        functools.partial(attend_kernel, plen, first, count, len(deps)),
        out_shape=[VMEM(g.shape, BFLOAT) for g in groups],
        in_specs=whole(2 + count) + after(len(deps)),
        out_specs=whole(count),
        compiler_params=GRANT,
        name="attend",
    )(*near_core(keys, values, *groups), *deps)


def add_group(blocks, head, part_ref, acc_ref, den_ref):
    heads = part_ref.shape[1] // XHEAD
    qrows = part_ref.shape[0] - LROWS
    lines = part_ref[qrows:, :QBLOCK].astype(FLOAT32)
    cols = slice(head * XHEAD, (head + 1) * XHEAD)
    for r, block in enumerate(blocks):
        @pl.when(block > 0)
        def _(r=r, block=block):
            rows = pl.ds(pl.multiple_of((block - 1) * QBLOCK, QBLOCK), QBLOCK)
            acc_ref[rows, :] += part_ref[r * QBLOCK : (r + 1) * QBLOCK, cols].astype(FLOAT32)
            at = 2 * (r * heads + head)
            den_ref[pl.ds(block - 1, 1), :] += lines[at : at + 1] + lines[at + 1 : at + 2]


def gather_kernel(count, deps, me_ref, blk_ref, *refs):
    parts = refs[:count]
    out_ref, acc_ref, den_ref = refs[count + deps :]
    capacity = blk_ref.shape[1]
    acc_ref[...] = jnp.zeros_like(acc_ref)
    den_ref[...] = jnp.zeros_like(den_ref)
    for k, part_ref in enumerate(parts):
        owner = me_ref[0] ^ k
        add_group([blk_ref[owner, r] for r in range(capacity)], 0, part_ref, acc_ref, den_ref)
    rows, lines = acc_ref.shape[0], den_ref.shape[0]
    out_ref[:rows, :] = acc_ref[...].astype(BFLOAT)
    high, low = parts2(den_ref[...])
    blank = jnp.zeros((lines, 128 - QBLOCK), BFLOAT)
    out_ref[rows:, :] = jnp.concatenate([high, blank, low, blank], axis=1)


def gather(me, blk, parts, rows, deps):
    lines = up16(rows // QBLOCK)
    smem = pl.BlockSpec(memory_space=SMEM)
    return pl.pallas_call(
        functools.partial(gather_kernel, len(parts), len(deps)),
        out_shape=VMEM((rows + lines, XHEAD), BFLOAT),
        in_specs=[smem, smem] + whole(len(parts)) + after(len(deps)),
        out_specs=pl.BlockSpec(memory_space=VMEM),
        scratch_shapes=[VMEM((rows, XHEAD), FLOAT32), VMEM((lines, QBLOCK), FLOAT32)],
        compiler_params=GRANT,
        name="gather",
    )(me, blk, *near_core(*parts), *deps)


def combine_kernel(count, deps, head, me_ref, blk_ref, far_ref, *refs):
    parts = refs[:count]
    out_ref, acc_ref, den_ref = refs[count + deps :]
    capacity = blk_ref.shape[1]
    rows = acc_ref.shape[0]
    acc_ref[...] = far_ref[:rows, :].astype(FLOAT32)
    tail = far_ref[rows:, :].astype(FLOAT32)
    den_ref[...] = tail[:, :QBLOCK] + tail[:, 128 : 128 + QBLOCK]
    for k, part_ref in enumerate(parts):
        owner = me_ref[0] ^ k
        add_group([blk_ref[owner, r] for r in range(capacity)], head, part_ref, acc_ref, den_ref)
    turned = jnp.transpose(den_ref[...])
    for b in range(rows // QBLOCK):
        mine = slice(b * QBLOCK, (b + 1) * QBLOCK)
        out_ref[mine, :] = (acc_ref[mine, :] / turned[:, b : b + 1]).astype(BFLOAT)


def combine(me, blk, far, parts, head, rows, deps):
    smem = pl.BlockSpec(memory_space=SMEM)
    return pl.pallas_call(
        functools.partial(combine_kernel, len(parts), len(deps), head),
        out_shape=VMEM((rows, XHEAD), BFLOAT),
        in_specs=[smem, smem] + whole(1 + len(parts)) + after(len(deps)),
        out_specs=pl.BlockSpec(memory_space=VMEM),
        scratch_shapes=[VMEM((rows, XHEAD), FLOAT32),
                        VMEM((far.shape[0] - rows, QBLOCK), FLOAT32)],
        compiler_params=GRANT,
        name="combine",
    )(me, blk, *near_core(far, *parts), *deps)


def gathered_dot(pieces, spots, blocks, me, w_ref):
    total = None
    for (j, h), piece in zip(spots, pieces):
        depth = piece.shape[1]
        rows = pl.ds(pl.multiple_of(((me ^ j) * blocks + h) * depth, depth), depth)
        part = dot(piece[...], w_ref[rows, :])
        total = part if total is None else total + part
    return total


def partial_kernel(spots, blocks, deps, me_ref, *refs):
    *pieces, w_ref = refs[: len(spots) + 1]
    refs[-1][...] = gathered_dot(pieces, spots, blocks, me_ref[0], w_ref)


def final_kernel(spots, blocks, deps, me_ref, *refs):
    *pieces, w_ref, some_ref, gate_ref, mixer_ref = refs[: len(spots) + 4]
    cross = some_ref[...] + gathered_dot(pieces, spots, blocks, me_ref[0], w_ref)
    refs[-1][...] = (mixer_ref[...] + gate_ref[...] * cross).astype(BFLOAT)


def over_tp(body, me, pieces, blocks, others, out, deps=()):
    spots = list(pieces)
    flat = [pieces[spot] for spot in spots]
    return pl.pallas_call(
        functools.partial(body, spots, blocks, len(deps)),
        out_shape=out((flat[0].shape[0], others[0].shape[1])),
        in_specs=[pl.BlockSpec(memory_space=SMEM)] + whole(len(flat) + len(others))
        + after(len(deps)),
        out_specs=pl.BlockSpec(memory_space=VMEM),
        compiler_params=GRANT,
    )(me, *near_core(*flat, *others), *deps)


def gather_tp(piece, count):
    pieces = {0: piece}
    bit = count // 2
    while bit:
        pairs = [(i, i ^ bit) for i in range(count)]
        for j in list(pieces):
            pieces[j ^ bit] = lax.ppermute(pieces[j], "tp", pairs)
        bit //= 2
    return [pieces[j] for j in range(count)]


def local(
    tokens, mix_query, mix_key, mix_value, decay_lower_map, decay_upper_map, decay_base,
    decay_shift, rate_lower_map, rate_upper_map, norm_gain, mix_out, cross_query, score_gain,
    passage_key, passage_value, cross_out, gate_down, gate_up, store, passage_ids,
):
    rows = tokens.shape[0]
    owners = lax.axis_size("st")
    shards = lax.axis_size("tp")
    pass_dev, plen, _ = store.shape
    per_block = passage_ids.shape[1]
    slots = passage_ids.shape[0] * per_block
    capacity = max(2, -(-slots // owners))
    me = lax.axis_index("tp").astype(jnp.int32).reshape(1)
    place = lax.axis_index("st").astype(jnp.int32).reshape(1)
    half = owners // 2

    def swap(value, bit):
        return lax.ppermute(value, "st", [(i, i ^ bit) for i in range(owners)])

    def swap_groups(groups):
        return [groups[0]] + [swap(groups[k], k) for k in range(1, half)]

    blk, queries, near = make_queries(
        place, passage_ids, owners, capacity, pass_dev, tokens, cross_query, score_gain)
    heads = len(queries)
    far_queries = [swap(queries[0], half)]
    near = swap_groups(near)
    keys, values = make_keyvals(store, passage_key, passage_value)
    for q in queries[1:]:
        q, keys = lax.optimization_barrier((q, keys))
        far_queries.append(swap(q, half))
    chunks = rows // MBLOCK
    pieces = [(0, 3), (3, 3), (6, 2)] if chunks == 8 else [(c, 1) for c in range(chunks)]
    prepared = []

    def some_chunks(dep):
        if not pieces:
            return dep
        prepared.append(prepare(mixer_in, *pieces.pop(0), [dep]))
        return prepared[-1][0]

    *mixer_in, gate = project(
        tokens, mix_query, mix_key, mix_value, decay_lower_map, decay_upper_map,
        decay_base, decay_shift, rate_lower_map, rate_upper_map, gate_down, gate_up, [keys])
    last = mixer_in[0]
    far = []
    for h in range(heads):
        far_blk, groups = relay(place, far_queries[h], rows, owners, capacity, [last])
        last = groups[0]
        far.append(swap_groups(groups))
        if h == 0:
            last = some_chunks(last)
    far_parts = []
    for h in range(heads):
        parts = attend(far[h], keys, values, plen, h, [last])
        last = parts[0]
        far_parts.append(swap_groups(parts))
        if h == 0:
            near_parts = attend(near, keys, values, plen, 0, [last])
            last = near_parts[0]
    returned = []
    for h in range(heads):
        sums = gather(place, far_blk, far_parts[h], rows, [last])
        if h == heads - 1:
            near_parts, sums = lax.optimization_barrier((near_parts, sums))
        returned.append(swap(sums, half))
        if h == heads - 1:
            near_parts = swap_groups(near_parts)
        last = some_chunks(sums)
    while pieces:
        last = some_chunks(last)
    mixer_heads = scan(prepared, norm_gain, [])
    mixer_all = gather_tp(mixer_heads, shards)
    last = mixer_heads
    cross = {}
    for h in range(heads):
        last = combine(place, blk, returned[h], near_parts, h, rows, [last])
        for k, piece in enumerate(gather_tp(last, shards)):
            cross[k, h] = piece
    inner = functools.partial(VMEM, dtype=FLOAT32)
    mixer_part = over_tp(partial_kernel, me, {(k, 0): p for k, p in enumerate(mixer_all)}, 1,
                         [mix_out], inner)
    late = [(k, h) for k, h in cross if h == heads - 1 and k > 1]
    some = over_tp(partial_kernel, me, {s: p for s, p in cross.items() if s not in late}, heads,
                   [cross_out], inner, [mixer_part])
    return over_tp(final_kernel, me, {s: cross[s] for s in late}, heads,
                   [cross_out, some, gate, mixer_part],
                   functools.partial(jax.ShapeDtypeStruct, dtype=BFLOAT))


def solution(mesh):
    placed = (
        P("st", None), P(None, "tp"), P(None, "tp"), P(None, "tp"), P(), P(None, "tp"), P("tp"),
        P("st", "tp"), P(), P(None, "tp"), P("tp"), P(None, "tp"), P(None, "tp"), P("tp"),
        P(None, "tp"), P(None, "tp"), P(None, "tp"), P(), P(None, "tp"), P("st", None, None),
        P("st", None),
    )
    return jax.shard_map(
        local, mesh=mesh, in_specs=placed, out_specs=P("st", "tp"), check_vma=False
    )
```

time: 139 us -> 117 us (0.84)
  the two profiles are of different devices: /device:TPU:0 before, /device:TPU:27 now
where the time goes in v3:
time: 117 us
  Pallas kernels  48.6 us (42%)
  starting transfers between devices  41.6 us (36%)
  waiting for transfers between devices  23.4 us (20%)
  local copies, waits for them, and re-layouts  2.97 us (3%)
    ppermute x9, starting transfers between devices, gather_tp(): pieces[j ^ bit] = lax.ppermute(pieces[j], 'tp', pairs)  21.9 us
    ppermute x22, starting transfers between devices, swap(): return lax.ppermute(value, 'st', [(i, i ^ bit) for i in range(owners)])  19.7 us
    ppermute x22, waiting for transfers between devices, swap(): return lax.ppermute(value, 'st', [(i, i ^ bit) for i in range(owners)])  16.7 us
    pallas_call x3, Pallas kernels, prepare(): pl.pallas_call(functools.partial(prepare_kernel, start, len(deps)), out_s...  12.2 us
    pallas_call x1, Pallas kernels, make_keyvals(): pl.pallas_call(keyval_kernel, grid=(pass_dev // group,), out_shape=[shape...  7.41 us
    ppermute x9, waiting for transfers between devices, gather_tp(): pieces[j ^ bit] = lax.ppermute(pieces[j], 'tp', pairs)  6.72 us
    pallas_call x1, Pallas kernels, make_queries(): pl.pallas_call(functools.partial(query_kernel, pass_dev, owners), grid=(s...  6.25 us
    pallas_call x3, Pallas kernels, over_tp(): pl.pallas_call(functools.partial(body, spots, blocks, len(deps)), out_sha...  6.09 us
  transfers between devices with their start and end apart: 31, of which 8 were waited for; matrix products, arithmetic and copies ran while one was open for 0% of the time, Pallas kernels for 34%

profile of v3, /device:TPU:27, one launch (start us, length us, event | category | flops | bytes accessed | tf_op | source)
XLA Modules:
  0.0 117.0 jit_solution(2163425857042380590)
XLA Ops:
  0.0 6.3 %queries.1 = (s32[8,4]{1,0:T(8,128)S(1)}, bf16[528,256]{1,0:T(8,128)(2,1)S(1)}, bf16[528,256]{1,0:T(8,128)(2,1)S(1)}, bf16[272,512]{1,0:T(8,128)(2,1)S(1)}, bf16...) custom-call(s32[1]{0:T(128)} %bitcast.1.me_ref, s32[4,8]{1,0:T(4,128)} %bitcast.16, ...), custom_call_target="tpu_custom_call" | custom-call | tf_op jit(solution)/shard_map/queries/pallas_call | solution.py:140
  6.8 7.4 %keyvals.1 = (bf16[1152,512]{1,0:T(8,128)(2,1)S(1)}, bf16[1152,512]{1,0:T(8,128)(2,1)S(1)}) custom-call(bf16[1152,2048]{1,0:T(8,128)(2,1)} %bitcast.15, bf16[2048,512]{1,0:T(8,128)(2,1)S(1)} %copy-done.2, bf16[2048,512]{1,0:T(8,128)(2,1)S(1)} %copy-done.3), custom_call_target="tpu_custom_call" | custom-call | tf_op jit(solution)/shard_map/keyvals/pallas_call | solution.py:202
  14.2 2.4 %collective-permute-start.7 = (bf16[528,256]{1,0:T(8,128)(2,1)S(1)}, bf16[528,256]{1,0:T(8,128)(2,1)S(1)}, u32[]{:S(2)}, u32[]{:S(2)}) collective-permute-start(bf16[528,256]{1,0:T(8,128)(2,1)S(1)} %get-tuple-element.76), channel_id=1, source_target_pairs={{0,16},{4,20},{8,24},{12,28},{16,0},{20,4},{24,8},{28,12},{1,17},{... | collective-permute-start | bytes 811016 | tf_op jit(solution)/shard_map/ppermute | solution.py:630
  16.7 2.2 %collective-permute-start.2 = (bf16[272,512]{1,0:T(8,128)(2,1)S(1)}, bf16[272,512]{1,0:T(8,128)(2,1)S(1)}, u32[]{:S(2)}, u32[]{:S(2)}) collective-permute-start(bf16[272,512]{1,0:T(8,128)(2,1)S(1)} %get-tuple-element.69), channel_id=1, source_target_pairs={{0,12},{4,8},{8,4},{12,0},{16,28},{20,24},{24,20},{28,16},{1,13},{... | collective-permute-start | bytes 835592 | tf_op jit(solution)/shard_map/ppermute | solution.py:630
  19.1 4.7 %project.1 = (bf16[512,256]{1,0:T(8,128)(2,1)S(1)}, bf16[512,256]{1,0:T(8,128)(2,1)S(1)}, bf16[512,256]{1,0:T(8,128)(2,1)S(1)}, f32[512,256]{1,0:T(8,128)S(1)}, ...) custom-call(bf16[512,2048]{1,0:T(8,128)(2,1)S(1)} %copy-done, ...), custom_call_target="tpu_custom_call" | custom-call | tf_op jit(solution)/shard_map/project/pallas_call | solution.py:248
  23.8 3.6 %collective-permute-done.3.q_ref = bf16[528,256]{1,0:T(8,128)(2,1)S(1)} collective-permute-done((bf16[528,256]{1,0:T(8,128)(2,1)S(1)}, bf16[528,256]{1,0:T(8,128)(2,1)S(1)}, u32[]{:S(2)}, u32[]{:S(2)}) %collective-permute-start.3) | collective-permute-done | bytes 270368 | tf_op jit(solution)/shard_map/ppermute | solution.py:630
  27.4 0.8 relay.2
  28.2 1.3 %collective-permute-start.4 = (bf16[272,256]{1,0:T(8,128)(2,1)S(1)}, bf16[272,256]{1,0:T(8,128)(2,1)S(1)}, u32[]{:S(2)}, u32[]{:S(2)}) collective-permute-start(bf16[272,256]{1,0:T(8,128)(2,1)S(1)} %get-tuple-element.73), channel_id=1, source_target_pairs={{0,4},{4,0},{8,12},{12,8},{16,20},{20,16},{24,28},{28,24},{1,5},{5... | collective-permute-start | bytes 417800 | tf_op jit(solution)/shard_map/ppermute | solution.py:630
  29.5 3.7 %collective-permute-done.7.q_ref = bf16[528,256]{1,0:T(8,128)(2,1)S(1)} collective-permute-done((bf16[528,256]{1,0:T(8,128)(2,1)S(1)}, bf16[528,256]{1,0:T(8,128)(2,1)S(1)}, u32[]{:S(2)}, u32[]{:S(2)}) %collective-permute-start.7) | collective-permute-done | bytes 270368 | tf_op jit(solution)/shard_map/ppermute | solution.py:630
  33.2 2.4 %collective-permute-start.6 = (bf16[272,256]{1,0:T(8,128)(2,1)S(1)}, bf16[272,256]{1,0:T(8,128)(2,1)S(1)}, u32[]{:S(2)}, u32[]{:S(2)}) collective-permute-start(bf16[272,256]{1,0:T(8,128)(2,1)S(1)} %get-tuple-element.75), channel_id=1, source_target_pairs={{0,12},{4,8},{8,4},{12,0},{16,28},{20,24},{24,20},{28,16},{1,13},{... | collective-permute-start | bytes 417800 | tf_op jit(solution)/shard_map/ppermute | solution.py:630
  35.6 4.2 %prepare.3 = (f32[192,256]{1,0:T(8,128)S(1)}, f32[192,256]{1,0:T(8,128)S(1)}, f32[192,256]{1,0:T(8,128)S(1)}, f32[192,256]{1,0:T(8,128)S(1)}) custom-call(bf16[512,256]{1,0:T(8,128)(2,1)S(1)} %get-tuple-element.71.refs_0_.q_ref, bf16[512,256]{1,0:T(8,128)(2,1)S(1)} %get-tuple-element.77.k_ref, bf16[512,256]{1,0:T(8,128)(2,1)S(1)} %get-tuple-element.78.v_ref, ...), custom_call_target="tpu_custom_call" | custom-call | tf_op jit(solution)/shard_map/prepare/pallas_call | solution.py:394
  39.8 0.9 relay.3
  41.0 0.9 collective-permute-done.5.refs_2_
  41.9 3.6 %collective-permute-done.6.refs_3_ = bf16[272,256]{1,0:T(8,128)(2,1)S(1)} collective-permute-done((bf16[272,256]{1,0:T(8,128)(2,1)S(1)}, bf16[272,256]{1,0:T(8,128)(2,1)S(1)}, u32[]{:S(2)}, u32[]{:S(2)}) %collective-permute-start.6) | collective-permute-done | bytes 139296 | tf_op jit(solution)/shard_map/ppermute | solution.py:630
  45.4 1.2 %attend.3 = (bf16[272,256]{1,0:T(8,128)(2,1)S(1)}, bf16[272,256]{1,0:T(8,128)(2,1)S(1)}, bf16[272,256]{1,0:T(8,128)(2,1)S(1)}, bf16[272,256]{1,0:T(8,128)(2,1)S(1)}) custom-call(bf16[1152,512]{1,0:T(8,128)(2,1)S(1)} %get-tuple-element.64.dep_ref.k_ref, bf16[1152,512]{1,0:T(8,128)(2,1)S(1)} %get-tuple-element.65.v_ref, ...), custom_call_target="tpu_custom_call" | custom-call | tf_op jit(solution)/shard_map/attend/pallas_call | solution.py:483
  46.7 0.4 collective-permute-start.14
  47.0 2.3 %collective-permute-start.15 = (bf16[272,256]{1,0:T(8,128)(2,1)S(1)}, bf16[272,256]{1,0:T(8,128)(2,1)S(1)}, u32[]{:S(2)}, u32[]{:S(2)}) collective-permute-start(bf16[272,256]{1,0:T(8,128)(2,1)S(1)} %get-tuple-element.98), channel_id=1, source_target_pairs={{0,8},{4,12},{8,0},{12,4},{16,24},{20,28},{24,16},{28,20},{1,9},{5... | collective-permute-start | bytes 417800 | tf_op jit(solution)/shard_map/ppermute | solution.py:630
  49.4 1.7 %attend.4 = (bf16[272,512]{1,0:T(8,128)(2,1)S(1)}, bf16[272,512]{1,0:T(8,128)(2,1)S(1)}, bf16[272,512]{1,0:T(8,128)(2,1)S(1)}, bf16[272,512]{1,0:T(8,128)(2,1)S(1)}) custom-call(bf16[1152,512]{1,0:T(8,128)(2,1)S(1)} %get-tuple-element.64.dep_ref.k_ref, bf16[1152,512]{1,0:T(8,128)(2,1)S(1)} %get-tuple-element.65.v_ref, ...), custom_call_target="tpu_custom_call" | custom-call | tf_op jit(solution)/shard_map/attend/pallas_call | solution.py:483
  51.2 1.2 %attend.5 = (bf16[272,256]{1,0:T(8,128)(2,1)S(1)}, bf16[272,256]{1,0:T(8,128)(2,1)S(1)}, bf16[272,256]{1,0:T(8,128)(2,1)S(1)}, bf16[272,256]{1,0:T(8,128)(2,1)S(1)}) custom-call(bf16[1152,512]{1,0:T(8,128)(2,1)S(1)} %get-tuple-element.64.dep_ref.k_ref, bf16[1152,512]{1,0:T(8,128)(2,1)S(1)} %get-tuple-element.65.v_ref, ...), custom_call_target="tpu_custom_call" | custom-call | tf_op jit(solution)/shard_map/attend/pallas_call | solution.py:483
  52.4 1.2 %collective-permute-start.11 = (bf16[272,256]{1,0:T(8,128)(2,1)S(1)}, bf16[272,256]{1,0:T(8,128)(2,1)S(1)}, u32[]{:S(2)}, u32[]{:S(2)}) collective-permute-start(bf16[272,256]{1,0:T(8,128)(2,1)S(1)} %get-tuple-element.94), channel_id=1, source_target_pairs={{0,4},{4,0},{8,12},{12,8},{16,20},{20,16},{24,28},{28,24},{1,5},{5... | collective-permute-start | bytes 417800 | tf_op jit(solution)/shard_map/ppermute | solution.py:630
  53.6 1.5 %collective-permute-start.12 = (bf16[272,256]{1,0:T(8,128)(2,1)S(1)}, bf16[272,256]{1,0:T(8,128)(2,1)S(1)}, u32[]{:S(2)}, u32[]{:S(2)}) collective-permute-start(bf16[272,256]{1,0:T(8,128)(2,1)S(1)} %get-tuple-element.95), channel_id=1, source_target_pairs={{0,8},{4,12},{8,0},{12,4},{16,24},{20,28},{24,16},{28,20},{1,9},{5... | collective-permute-start | bytes 417800 | tf_op jit(solution)/shard_map/ppermute | solution.py:630
  55.1 2.4 %collective-permute-done.16.refs_3_ = bf16[272,256]{1,0:T(8,128)(2,1)S(1)} collective-permute-done((bf16[272,256]{1,0:T(8,128)(2,1)S(1)}, bf16[272,256]{1,0:T(8,128)(2,1)S(1)}, u32[]{:S(2)}, u32[]{:S(2)}) %collective-permute-start.16) | collective-permute-done | bytes 139296 | tf_op jit(solution)/shard_map/ppermute | solution.py:630
  57.5 1.1 gather.2.refs_0_
  58.5 4.2 %prepare.4 = (f32[192,256]{1,0:T(8,128)S(1)}, f32[192,256]{1,0:T(8,128)S(1)}, f32[192,256]{1,0:T(8,128)S(1)}, f32[192,256]{1,0:T(8,128)S(1)}) custom-call(bf16[512,256]{1,0:T(8,128)(2,1)S(1)} %get-tuple-element.71.refs_0_.q_ref, bf16[512,256]{1,0:T(8,128)(2,1)S(1)} %get-tuple-element.77.k_ref, bf16[512,256]{1,0:T(8,128)(2,1)S(1)} %get-tuple-element.78.v_ref, ...), custom_call_target="tpu_custom_call" | custom-call | tf_op jit(solution)/shard_map/prepare/pallas_call | solution.py:394
  62.8 0.9 gather.3.refs_0_
  63.7 1.6 %collective-permute-start.19 = (bf16[272,512]{1,0:T(8,128)(2,1)S(1)}, bf16[272,512]{1,0:T(8,128)(2,1)S(1)}, u32[]{:S(2)}, u32[]{:S(2)}) collective-permute-start(bf16[272,512]{1,0:T(8,128)(2,1)S(1)} %get-tuple-element.104), channel_id=1, source_target_pairs={{0,8},{4,12},{8,0},{12,4},{16,24},{20,28},{24,16},{28,20},{1,9},{5... | collective-permute-start | bytes 835592 | tf_op jit(solution)/shard_map/ppermute | solution.py:630
  65.3 1.0 collective-permute-start.20
  66.3 2.4 %collective-permute-start.17 = (bf16[528,256]{1,0:T(8,128)(2,1)S(1)}, bf16[528,256]{1,0:T(8,128)(2,1)S(1)}, u32[]{:S(2)}, u32[]{:S(2)}) collective-permute-start(bf16[528,256]{1,0:T(8,128)(2,1)S(1)} %gather.3.refs_0_), channel_id=1, source_target_pairs={{0,16},{4,20},{8,24},{12,28},{16,0},{20,4},{24,8},{28,12},{1,17},{... | collective-permute-start | bytes 811016 | tf_op jit(solution)/shard_map/ppermute | solution.py:630
  68.7 3.8 %prepare.5 = (f32[128,256]{1,0:T(8,128)S(1)}, f32[128,256]{1,0:T(8,128)S(1)}, f32[128,256]{1,0:T(8,128)S(1)}, f32[128,256]{1,0:T(8,128)S(1)}) custom-call(bf16[512,256]{1,0:T(8,128)(2,1)S(1)} %get-tuple-element.71.refs_0_.q_ref, bf16[512,256]{1,0:T(8,128)(2,1)S(1)} %get-tuple-element.77.k_ref, bf16[512,256]{1,0:T(8,128)(2,1)S(1)} %get-tuple-element.78.v_ref, ...), custom_call_target="tpu_custom_call" | custom-call | tf_op jit(solution)/shard_map/prepare/pallas_call | solution.py:394
  72.5 2.2 %scan.1.refs_4_.refs_0_ = bf16[512,256]{1,0:T(8,128)(2,1)S(1)} custom-call(f32[1,256]{1,0:T(1,128)S(1)} %bitcast.14, f32[192,256]{1,0:T(8,128)S(1)} %get-tuple-element.82.refs_0_, f32[192,256]{1,0:T(8,128)S(1)} %get-tuple-element.106.refs_1_, f32[192,256]{1,0:T(8,128)S(1)} %get-tuple-element.107.refs_2_, f32[192,256]{1,0:T(8,128)S(1)} %get-tuple-element.108.refs_3_, ...), custom_call_target="tpu_custom_call" | custom-call | tf_op jit(solution)/shard_map/scan/pallas_call | solution.py:438
  74.7 2.5 %collective-permute-done.21.far_ref = bf16[528,256]{1,0:T(8,128)(2,1)S(1)} collective-permute-done((bf16[528,256]{1,0:T(8,128)(2,1)S(1)}, bf16[528,256]{1,0:T(8,128)(2,1)S(1)}, u32[]{:S(2)}, u32[]{:S(2)}) %collective-permute-start.21) | collective-permute-done | bytes 270368 | tf_op jit(solution)/shard_map/ppermute | solution.py:630
  77.2 1.2 %collective-permute-start.29 = (bf16[512,256]{1,0:T(8,128)(2,1)S(1)}, bf16[512,256]{1,0:T(8,128)(2,1)}, u32[]{:S(2)}, u32[]{:S(2)}) collective-permute-start(bf16[512,256]{1,0:T(8,128)(2,1)S(1)} %scan.1.refs_4_.refs_0_), channel_id=1, source_target_pairs={{0,2},{1,3},{2,0},{3,1},{4,6},{5,7},{6,4},{7,5},{8,10},{9,11},{10,... | collective-permute-start | bytes 786440 | tf_op jit(solution)/shard_map/ppermute | solution.py:608
  78.4 14.1 %collective-permute-start.28 = (bf16[512,256]{1,0:T(8,128)(2,1)S(1)}, bf16[512,256]{1,0:T(8,128)(2,1)S(1)}, u32[]{:S(2)}, u32[]{:S(2)}) collective-permute-start(bf16[512,256]{1,0:T(8,128)(2,1)S(1)} %scan.1.refs_4_.refs_0_), channel_id=1, source_target_pairs={{0,1},{1,0},{2,3},{3,2},{4,5},{5,4},{6,7},{7,6},{8,9},{9,8},{10,11... | collective-permute-start | bytes 786440 | tf_op jit(solution)/shard_map/ppermute | solution.py:608
  92.6 1.1 combine.2.refs_4_.refs_0_
  93.9 1.1 combine.3.refs_4_
  95.0 1.3 %collective-permute-start.22 = (bf16[512,256]{1,0:T(8,128)(2,1)S(1)}, bf16[512,256]{1,0:T(8,128)(2,1)S(1)}, u32[]{:S(2)}, u32[]{:S(2)}) collective-permute-start(bf16[512,256]{1,0:T(8,128)(2,1)S(1)} %combine.3.refs_4_), channel_id=1, source_target_pairs={{0,2},{1,3},{2,0},{3,1},{4,6},{5,7},{6,4},{7,5},{8,10},{9,11},{10,... | collective-permute-start | bytes 786440 | tf_op jit(solution)/shard_map/ppermute | solution.py:608
  96.3 1.8 %collective-permute-start.30 = (bf16[512,256]{1,0:T(8,128)(2,1)}, bf16[512,256]{1,0:T(8,128)(2,1)}, u32[]{:S(2)}, u32[]{:S(2)}) collective-permute-start(bf16[512,256]{1,0:T(8,128)(2,1)} %collective-permute-done.29.refs_2_), channel_id=1, source_target_pairs={{0,1},{1,0},{2,3},{3,2},{4,5},{5,4},{6,7},{7,6},{8,9},{9,8},{10,11... | collective-permute-start | bytes 786440 | tf_op jit(solution)/shard_map/ppermute | solution.py:608
  98.1 0.7 copy-done.13
  98.8 0.5 collective-permute-start.24
  99.3 2.7 %collective-permute-done.25.refs_2_ = bf16[512,256]{1,0:T(8,128)(2,1)S(1)} collective-permute-done((bf16[512,256]{1,0:T(8,128)(2,1)S(1)}, bf16[512,256]{1,0:T(8,128)(2,1)S(1)}, u32[]{:S(2)}, u32[]{:S(2)}) %collective-permute-start.25) | collective-permute-done | bytes 262176 | tf_op jit(solution)/shard_map/ppermute | solution.py:608
  102.0 1.6 %collective-permute-start.26 = (bf16[512,256]{1,0:T(8,128)(2,1)S(1)}, bf16[512,256]{1,0:T(8,128)(2,1)}, u32[]{:S(2)}, u32[]{:S(2)}) collective-permute-start(bf16[512,256]{1,0:T(8,128)(2,1)S(1)} %collective-permute-done.25.refs_2_), channel_id=1, source_target_pairs={{0,1},{1,0},{2,3},{3,2},{4,5},{5,4},{6,7},{7,6},{8,9},{9,8},{10,11... | collective-permute-start | bytes 786440 | tf_op jit(solution)/shard_map/ppermute | solution.py:608
  103.6 4.0 %collective-permute-done.22.refs_0_ = bf16[512,256]{1,0:T(8,128)(2,1)S(1)} collective-permute-done((bf16[512,256]{1,0:T(8,128)(2,1)S(1)}, bf16[512,256]{1,0:T(8,128)(2,1)S(1)}, u32[]{:S(2)}, u32[]{:S(2)}) %collective-permute-start.22) | collective-permute-done | bytes 262176 | tf_op jit(solution)/shard_map/ppermute | solution.py:608
  107.6 1.0 collective-permute-start.23
  108.6 1.2 %copy-done.9 = bf16[1024,512]{1,0:T(8,128)(2,1)S(1)} copy-done((bf16[1024,512]{1,0:T(8,128)(2,1)S(1)}, bf16[1024,512]{1,0:T(8,128)(2,1)}, u32[]{:S(2)}) %copy-start.9) | copy-done | bytes 1048600
  109.9 0.9 copy-done.14
  110.8 1.7 %shard_map.199.refs_7_.refs_5_ = f32[512,512]{1,0:T(8,128)S(1)} custom-call(s32[1]{0:T(128)} %bitcast.me_ref, bf16[512,256]{1,0:T(8,128)(2,1)S(1)} %scan.1.refs_4_.refs_0_, bf16[512,256]{1,0:T(8,128)(2,1)S(1)} %copy-done.14, bf16[512,256]{1,0:T(8,128)(2,1)} %collective-permute-done.29.refs_2_, bf16[512,256]{1,0:T(8,128)(2,1)} %collective-permute-done.30.refs_3_, ...), custom_call_target="tpu_custom_call" | custom-call | tf_op jit(solution)/shard_map/pallas_call | solution.py:592
  112.6 2.2 %shard_map.200.refs_3_ = f32[512,512]{1,0:T(8,128)S(1)} custom-call(s32[1]{0:T(128)} %bitcast.me_ref, bf16[512,256]{1,0:T(8,128)(2,1)S(1)} %combine.2.refs_4_.refs_0_, bf16[512,256]{1,0:T(8,128)(2,1)} %collective-permute-done.24.refs_1_, bf16[512,256]{1,0:T(8,128)(2,1)S(1)} %collective-permute-done.25.refs_2_, ...), custom_call_target="tpu_custom_call" | custom-call | tf_op jit(solution)/shard_map/pallas_call | solution.py:592
  114.8 2.2 %shard_map.201 = bf16[512,512]{1,0:T(8,128)(2,1)} custom-call(s32[1]{0:T(128)} %bitcast.me_ref, bf16[512,256]{1,0:T(8,128)(2,1)S(1)} %collective-permute-done.22.refs_0_, bf16[512,256]{1,0:T(8,128)(2,1)} %collective-permute-done.23.refs_1_, bf16[2048,512]{1,0:T(8,128)(2,1)S(1)} %copy-done.1, f32[512,512]{1,0:T(8,128)S(1)} %shard_map.200.refs_3_, ...), custom_call_target="tpu_custom_call" | custom-call | tf_op jit(solution)/shard_map/pallas_call | solution.py:592
  (75 shorter events, 1.5 us)
Async XLA Ops:
  0.0 6.6 %copy-start.2 = (bf16[2048,512]{1,0:T(8,128)(2,1)S(1)}, bf16[2048,512]{1,0:T(8,128)(2,1)}, u32[]{:S(2)}) copy-start(bf16[2048,512]{1,0:T(8,128)(2,1)} %wk_ref.1) | copy-start | bytes 6291460
  0.0 6.6 %copy-start.3 = (bf16[2048,512]{1,0:T(8,128)(2,1)S(1)}, bf16[2048,512]{1,0:T(8,128)(2,1)}, u32[]{:S(2)}) copy-start(bf16[2048,512]{1,0:T(8,128)(2,1)} %wv_ref.1) | copy-start | bytes 6291460
  6.3 26.9 %collective-permute-start = (bf16[272,512]{1,0:T(8,128)(2,1)S(1)}, bf16[272,512]{1,0:T(8,128)(2,1)S(1)}, u32[]{:S(2)}, u32[]{:S(2)}) collective-permute-start(bf16[272,512]{1,0:T(8,128)(2,1)S(1)} %get-tuple-element.67), channel_id=1, source_target_pairs={{0,4},{4,0},{8,12},{12,8},{16,20},{20,16},{24,28},{28,24},{1,5},{5... | collective-permute-start | bytes 835592 | tf_op jit(solution)/shard_map/ppermute | solution.py:630
  6.6 20.8 %collective-permute-start.3 = (bf16[528,256]{1,0:T(8,128)(2,1)S(1)}, bf16[528,256]{1,0:T(8,128)(2,1)S(1)}, u32[]{:S(2)}, u32[]{:S(2)}) collective-permute-start(bf16[528,256]{1,0:T(8,128)(2,1)S(1)} %get-tuple-element.70), channel_id=1, source_target_pairs={{0,16},{4,20},{8,24},{12,28},{16,0},{20,4},{24,8},{28,12},{1,17},{... | collective-permute-start | bytes 811016 | tf_op jit(solution)/shard_map/ppermute | solution.py:630
  6.6 12.3 %copy-start = (bf16[512,2048]{1,0:T(8,128)(2,1)S(1)}, bf16[512,2048]{1,0:T(8,128)(2,1)}, u32[]{:S(2)}) copy-start(bf16[512,2048]{1,0:T(8,128)(2,1)} %tok_ref.3) | copy-start | bytes 6291460
  6.6 12.3 %copy-start.4 = (bf16[2048,256]{1,0:T(8,128)(2,1)S(1)}, bf16[2048,256]{1,0:T(8,128)(2,1)}, u32[]{:S(2)}) copy-start(bf16[2048,256]{1,0:T(8,128)(2,1)} %mq_ref.1) | copy-start | bytes 3145732
  6.7 12.3 %copy-start.5 = (bf16[2048,256]{1,0:T(8,128)(2,1)S(1)}, bf16[2048,256]{1,0:T(8,128)(2,1)}, u32[]{:S(2)}) copy-start(bf16[2048,256]{1,0:T(8,128)(2,1)} %mk_ref.1) | copy-start | bytes 3145732
  6.7 12.3 %copy-start.6 = (bf16[2048,256]{1,0:T(8,128)(2,1)S(1)}, bf16[2048,256]{1,0:T(8,128)(2,1)}, u32[]{:S(2)}) copy-start(bf16[2048,256]{1,0:T(8,128)(2,1)} %mv_ref.1) | copy-start | bytes 3145732
  6.7 12.3 %copy-start.10 = (bf16[2048,128]{1,0:T(8,128)(2,1)S(1)}, bf16[2048,128]{1,0:T(8,128)(2,1)}, u32[]{:S(2)}) copy-start(bf16[2048,128]{1,0:T(8,128)(2,1)} %gd_ref.1) | copy-start | bytes 1572868
  6.7 12.3 %copy-start.11 = (bf16[2048,64]{0,1:T(8,128)(2,1)S(1)}, bf16[2048,64]{0,1:T(8,128)(2,1)}, u32[]{:S(2)}) copy-start(bf16[2048,64]{0,1:T(8,128)(2,1)} %param.25) | copy-start | bytes 786436
  6.7 12.3 %copy-start.12 = (bf16[2048,64]{0,1:T(8,128)(2,1)S(1)}, bf16[2048,64]{0,1:T(8,128)(2,1)}, u32[]{:S(2)}) copy-start(bf16[2048,64]{0,1:T(8,128)(2,1)} %param.29) | copy-start | bytes 786436
  6.7 12.3 %copy-start.15 = (bf16[128,512]{1,0:T(8,128)(2,1)S(1)}, bf16[128,512]{1,0:T(8,128)(2,1)}, u32[]{:S(2)}) copy-start(bf16[128,512]{1,0:T(8,128)(2,1)} %gu_ref.1) | copy-start | bytes 393220
  6.7 12.3 %copy-start.16 = (bf16[64,256]{1,0:T(8,128)(2,1)S(1)}, bf16[64,256]{1,0:T(8,128)(2,1)}, u32[]{:S(2)}) copy-start(bf16[64,256]{1,0:T(8,128)(2,1)} %du_ref.1) | copy-start | bytes 98308
  6.7 12.3 %copy-start.17 = (bf16[64,256]{1,0:T(8,128)(2,1)S(1)}, bf16[64,256]{1,0:T(8,128)(2,1)}, u32[]{:S(2)}) copy-start(bf16[64,256]{1,0:T(8,128)(2,1)} %ru_ref.1) | copy-start | bytes 98308
  6.8 12.3 %copy-start.18 = (f32[512,4]{0,1:T(4,128)S(1)}, f32[512,4]{0,1:T(4,128)}, u32[]{:S(2)}) copy-start(f32[512,4]{0,1:T(4,128)} %param.28) | copy-start | bytes 24580
  6.8 12.3 %copy-start.19 = (f32[256]{0:T(256)S(1)}, f32[256]{0:T(256)}, u32[]{:S(2)}) copy-start(f32[256]{0:T(256)} %param.27) | copy-start | bytes 3076
  14.2 19.0 %collective-permute-start.7 = (bf16[528,256]{1,0:T(8,128)(2,1)S(1)}, bf16[528,256]{1,0:T(8,128)(2,1)S(1)}, u32[]{:S(2)}, u32[]{:S(2)}) collective-permute-start(bf16[528,256]{1,0:T(8,128)(2,1)S(1)} %get-tuple-element.76), channel_id=1, source_target_pairs={{0,16},{4,20},{8,24},{12,28},{16,0},{20,4},{24,8},{28,12},{1,17},{... | collective-permute-start | bytes 811016 | tf_op jit(solution)/shard_map/ppermute | solution.py:630
  16.6 30.1 %collective-permute-start.1 = (bf16[272,512]{1,0:T(8,128)(2,1)S(1)}, bf16[272,512]{1,0:T(8,128)(2,1)S(1)}, u32[]{:S(2)}, u32[]{:S(2)}) collective-permute-start(bf16[272,512]{1,0:T(8,128)(2,1)S(1)} %get-tuple-element.68), channel_id=1, source_target_pairs={{0,8},{4,12},{8,0},{12,4},{16,24},{20,28},{24,16},{28,20},{1,9},{5... | collective-permute-start | bytes 835592 | tf_op jit(solution)/shard_map/ppermute | solution.py:630
  16.7 30.3 %collective-permute-start.2 = (bf16[272,512]{1,0:T(8,128)(2,1)S(1)}, bf16[272,512]{1,0:T(8,128)(2,1)S(1)}, u32[]{:S(2)}, u32[]{:S(2)}) collective-permute-start(bf16[272,512]{1,0:T(8,128)(2,1)S(1)} %get-tuple-element.69), channel_id=1, source_target_pairs={{0,12},{4,8},{8,4},{12,0},{16,28},{20,24},{24,20},{28,16},{1,13},{... | collective-permute-start | bytes 835592 | tf_op jit(solution)/shard_map/ppermute | solution.py:630
  23.8 22.9 %copy-start.7 = (f32[512,512]{1,0:T(8,128)}, f32[512,512]{1,0:T(8,128)S(1)}, u32[]{:S(2)}) copy-start(f32[512,512]{1,0:T(8,128)S(1)} %get-tuple-element.116.refs_4_) | copy-start | bytes 3145732
  28.2 12.4 %collective-permute-start.4 = (bf16[272,256]{1,0:T(8,128)(2,1)S(1)}, bf16[272,256]{1,0:T(8,128)(2,1)S(1)}, u32[]{:S(2)}, u32[]{:S(2)}) collective-permute-start(bf16[272,256]{1,0:T(8,128)(2,1)S(1)} %get-tuple-element.73), channel_id=1, source_target_pairs={{0,4},{4,0},{8,12},{12,8},{16,20},{20,16},{24,28},{28,24},{1,5},{5... | collective-permute-start | bytes 417800 | tf_op jit(solution)/shard_map/ppermute | solution.py:630
  33.2 8.7 %collective-permute-start.5 = (bf16[272,256]{1,0:T(8,128)(2,1)S(1)}, bf16[272,256]{1,0:T(8,128)(2,1)S(1)}, u32[]{:S(2)}, u32[]{:S(2)}) collective-permute-start(bf16[272,256]{1,0:T(8,128)(2,1)S(1)} %get-tuple-element.74), channel_id=1, source_target_pairs={{0,8},{4,12},{8,0},{12,4},{16,24},{20,28},{24,16},{28,20},{1,9},{5... | collective-permute-start | bytes 417800 | tf_op jit(solution)/shard_map/ppermute | solution.py:630
  33.2 12.2 %collective-permute-start.6 = (bf16[272,256]{1,0:T(8,128)(2,1)S(1)}, bf16[272,256]{1,0:T(8,128)(2,1)S(1)}, u32[]{:S(2)}, u32[]{:S(2)}) collective-permute-start(bf16[272,256]{1,0:T(8,128)(2,1)S(1)} %get-tuple-element.75), channel_id=1, source_target_pairs={{0,12},{4,8},{8,4},{12,0},{16,28},{20,24},{24,20},{28,16},{1,13},{... | collective-permute-start | bytes 417800 | tf_op jit(solution)/shard_map/ppermute | solution.py:630
  40.7 10.4 %collective-permute-start.8 = (bf16[272,256]{1,0:T(8,128)(2,1)S(1)}, bf16[272,256]{1,0:T(8,128)(2,1)S(1)}, u32[]{:S(2)}, u32[]{:S(2)}) collective-permute-start(bf16[272,256]{1,0:T(8,128)(2,1)S(1)} %get-tuple-element.90), channel_id=1, source_target_pairs={{0,4},{4,0},{8,12},{12,8},{16,20},{20,16},{24,28},{28,24},{1,5},{5... | collective-permute-start | bytes 417800 | tf_op jit(solution)/shard_map/ppermute | solution.py:630
  41.9 9.3 %collective-permute-start.9 = (bf16[272,256]{1,0:T(8,128)(2,1)S(1)}, bf16[272,256]{1,0:T(8,128)(2,1)S(1)}, u32[]{:S(2)}, u32[]{:S(2)}) collective-permute-start(bf16[272,256]{1,0:T(8,128)(2,1)S(1)} %get-tuple-element.91), channel_id=1, source_target_pairs={{0,8},{4,12},{8,0},{12,4},{16,24},{20,28},{24,16},{28,20},{1,9},{5... | collective-permute-start | bytes 417800 | tf_op jit(solution)/shard_map/ppermute | solution.py:630
  45.4 5.7 %collective-permute-start.10 = (bf16[272,256]{1,0:T(8,128)(2,1)S(1)}, bf16[272,256]{1,0:T(8,128)(2,1)S(1)}, u32[]{:S(2)}, u32[]{:S(2)}) collective-permute-start(bf16[272,256]{1,0:T(8,128)(2,1)S(1)} %get-tuple-element.92), channel_id=1, source_target_pairs={{0,12},{4,8},{8,4},{12,0},{16,28},{20,24},{24,20},{28,16},{1,13},{... | collective-permute-start | bytes 417800 | tf_op jit(solution)/shard_map/ppermute | solution.py:630
  46.7 8.4 %collective-permute-start.14 = (bf16[272,256]{1,0:T(8,128)(2,1)S(1)}, bf16[272,256]{1,0:T(8,128)(2,1)S(1)}, u32[]{:S(2)}, u32[]{:S(2)}) collective-permute-start(bf16[272,256]{1,0:T(8,128)(2,1)S(1)} %get-tuple-element.97), channel_id=1, source_target_pairs={{0,4},{4,0},{8,12},{12,8},{16,20},{20,16},{24,28},{28,24},{1,5},{5... | collective-permute-start | bytes 417800 | tf_op jit(solution)/shard_map/ppermute | solution.py:630
  47.0 8.1 %collective-permute-start.15 = (bf16[272,256]{1,0:T(8,128)(2,1)S(1)}, bf16[272,256]{1,0:T(8,128)(2,1)S(1)}, u32[]{:S(2)}, u32[]{:S(2)}) collective-permute-start(bf16[272,256]{1,0:T(8,128)(2,1)S(1)} %get-tuple-element.98), channel_id=1, source_target_pairs={{0,8},{4,12},{8,0},{12,4},{16,24},{20,28},{24,16},{28,20},{1,9},{5... | collective-permute-start | bytes 417800 | tf_op jit(solution)/shard_map/ppermute | solution.py:630
  51.1 6.4 %collective-permute-start.16 = (bf16[272,256]{1,0:T(8,128)(2,1)S(1)}, bf16[272,256]{1,0:T(8,128)(2,1)S(1)}, u32[]{:S(2)}, u32[]{:S(2)}) collective-permute-start(bf16[272,256]{1,0:T(8,128)(2,1)S(1)} %get-tuple-element.99), channel_id=1, source_target_pairs={{0,12},{4,8},{8,4},{12,0},{16,28},{20,24},{24,20},{28,16},{1,13},{... | collective-permute-start | bytes 417800 | tf_op jit(solution)/shard_map/ppermute | solution.py:630
  52.4 10.4 %collective-permute-start.11 = (bf16[272,256]{1,0:T(8,128)(2,1)S(1)}, bf16[272,256]{1,0:T(8,128)(2,1)S(1)}, u32[]{:S(2)}, u32[]{:S(2)}) collective-permute-start(bf16[272,256]{1,0:T(8,128)(2,1)S(1)} %get-tuple-element.94), channel_id=1, source_target_pairs={{0,4},{4,0},{8,12},{12,8},{16,20},{20,16},{24,28},{28,24},{1,5},{5... | collective-permute-start | bytes 417800 | tf_op jit(solution)/shard_map/ppermute | solution.py:630
  53.6 9.2 %collective-permute-start.12 = (bf16[272,256]{1,0:T(8,128)(2,1)S(1)}, bf16[272,256]{1,0:T(8,128)(2,1)S(1)}, u32[]{:S(2)}, u32[]{:S(2)}) collective-permute-start(bf16[272,256]{1,0:T(8,128)(2,1)S(1)} %get-tuple-element.95), channel_id=1, source_target_pairs={{0,8},{4,12},{8,0},{12,4},{16,24},{20,28},{24,16},{28,20},{1,9},{5... | collective-permute-start | bytes 417800 | tf_op jit(solution)/shard_map/ppermute | solution.py:630
  55.1 7.7 %collective-permute-start.13 = (bf16[272,256]{1,0:T(8,128)(2,1)S(1)}, bf16[272,256]{1,0:T(8,128)(2,1)S(1)}, u32[]{:S(2)}, u32[]{:S(2)}) collective-permute-start(bf16[272,256]{1,0:T(8,128)(2,1)S(1)} %get-tuple-element.96), channel_id=1, source_target_pairs={{0,12},{4,8},{8,4},{12,0},{16,28},{20,24},{24,20},{28,16},{1,13},{... | collective-permute-start | bytes 417800 | tf_op jit(solution)/shard_map/ppermute | solution.py:630
  62.7 9.8 %copy-start.20 = (f32[256]{0:T(256)S(1)}, f32[256]{0:T(256)}, u32[]{:S(2)}) copy-start(f32[256]{0:T(256)} %param.31) | copy-start | bytes 3076
  63.6 14.8 %collective-permute-start.18 = (bf16[272,512]{1,0:T(8,128)(2,1)S(1)}, bf16[272,512]{1,0:T(8,128)(2,1)S(1)}, u32[]{:S(2)}, u32[]{:S(2)}) collective-permute-start(bf16[272,512]{1,0:T(8,128)(2,1)S(1)} %get-tuple-element.103), channel_id=1, source_target_pairs={{0,4},{4,0},{8,12},{12,8},{16,20},{20,16},{24,28},{28,24},{1,5},{5... | collective-permute-start | bytes 835592 | tf_op jit(solution)/shard_map/ppermute | solution.py:630
  63.7 28.9 %collective-permute-start.19 = (bf16[272,512]{1,0:T(8,128)(2,1)S(1)}, bf16[272,512]{1,0:T(8,128)(2,1)S(1)}, u32[]{:S(2)}, u32[]{:S(2)}) collective-permute-start(bf16[272,512]{1,0:T(8,128)(2,1)S(1)} %get-tuple-element.104), channel_id=1, source_target_pairs={{0,8},{4,12},{8,0},{12,4},{16,24},{20,28},{24,16},{28,20},{1,9},{5... | collective-permute-start | bytes 835592 | tf_op jit(solution)/shard_map/ppermute | solution.py:630
  65.3 27.3 %collective-permute-start.20 = (bf16[272,512]{1,0:T(8,128)(2,1)S(1)}, bf16[272,512]{1,0:T(8,128)(2,1)S(1)}, u32[]{:S(2)}, u32[]{:S(2)}) collective-permute-start(bf16[272,512]{1,0:T(8,128)(2,1)S(1)} %get-tuple-element.105), channel_id=1, source_target_pairs={{0,12},{4,8},{8,4},{12,0},{16,28},{20,24},{24,20},{28,16},{1,13},{... | collective-permute-start | bytes 835592 | tf_op jit(solution)/shard_map/ppermute | solution.py:630
  66.3 10.8 %collective-permute-start.21 = (bf16[528,256]{1,0:T(8,128)(2,1)S(1)}, bf16[528,256]{1,0:T(8,128)(2,1)S(1)}, u32[]{:S(2)}, u32[]{:S(2)}) collective-permute-start(bf16[528,256]{1,0:T(8,128)(2,1)S(1)} %gather.2.refs_0_), channel_id=1, source_target_pairs={{0,16},{4,20},{8,24},{12,28},{16,0},{20,4},{24,8},{28,12},{1,17},{... | collective-permute-start | bytes 811016 | tf_op jit(solution)/shard_map/ppermute | solution.py:630
  66.3 27.6 %collective-permute-start.17 = (bf16[528,256]{1,0:T(8,128)(2,1)S(1)}, bf16[528,256]{1,0:T(8,128)(2,1)S(1)}, u32[]{:S(2)}, u32[]{:S(2)}) collective-permute-start(bf16[528,256]{1,0:T(8,128)(2,1)S(1)} %gather.3.refs_0_), channel_id=1, source_target_pairs={{0,16},{4,20},{8,24},{12,28},{16,0},{20,4},{24,8},{28,12},{1,17},{... | collective-permute-start | bytes 811016 | tf_op jit(solution)/shard_map/ppermute | solution.py:630
  77.2 19.1 %collective-permute-start.29 = (bf16[512,256]{1,0:T(8,128)(2,1)S(1)}, bf16[512,256]{1,0:T(8,128)(2,1)}, u32[]{:S(2)}, u32[]{:S(2)}) collective-permute-start(bf16[512,256]{1,0:T(8,128)(2,1)S(1)} %scan.1.refs_4_.refs_0_), channel_id=1, source_target_pairs={{0,2},{1,3},{2,0},{3,1},{4,6},{5,7},{6,4},{7,5},{8,10},{9,11},{10,... | collective-permute-start | bytes 786440 | tf_op jit(solution)/shard_map/ppermute | solution.py:608
  78.4 19.7 %collective-permute-start.28 = (bf16[512,256]{1,0:T(8,128)(2,1)S(1)}, bf16[512,256]{1,0:T(8,128)(2,1)S(1)}, u32[]{:S(2)}, u32[]{:S(2)}) collective-permute-start(bf16[512,256]{1,0:T(8,128)(2,1)S(1)} %scan.1.refs_4_.refs_0_), channel_id=1, source_target_pairs={{0,1},{1,0},{2,3},{3,2},{4,5},{5,4},{6,7},{7,6},{8,9},{9,8},{10,11... | collective-permute-start | bytes 786440 | tf_op jit(solution)/shard_map/ppermute | solution.py:608
  93.6 19.0 %copy-start.1 = (bf16[2048,512]{1,0:T(8,128)(2,1)S(1)}, bf16[2048,512]{1,0:T(8,128)(2,1)}, u32[]{:S(2)}) copy-start(bf16[2048,512]{1,0:T(8,128)(2,1)} %refs_2_.1) | copy-start | bytes 6291460
  93.6 8.4 %collective-permute-start.25 = (bf16[512,256]{1,0:T(8,128)(2,1)S(1)}, bf16[512,256]{1,0:T(8,128)(2,1)S(1)}, u32[]{:S(2)}, u32[]{:S(2)}) collective-permute-start(bf16[512,256]{1,0:T(8,128)(2,1)S(1)} %combine.2.refs_4_.refs_0_), channel_id=1, source_target_pairs={{0,2},{1,3},{2,0},{3,1},{4,6},{5,7},{6,4},{7,5},{8,10},{9,11},{10,... | collective-permute-start | bytes 786440 | tf_op jit(solution)/shard_map/ppermute | solution.py:608
  95.0 12.6 %collective-permute-start.22 = (bf16[512,256]{1,0:T(8,128)(2,1)S(1)}, bf16[512,256]{1,0:T(8,128)(2,1)S(1)}, u32[]{:S(2)}, u32[]{:S(2)}) collective-permute-start(bf16[512,256]{1,0:T(8,128)(2,1)S(1)} %combine.3.refs_4_), channel_id=1, source_target_pairs={{0,2},{1,3},{2,0},{3,1},{4,6},{5,7},{6,4},{7,5},{8,10},{9,11},{10,... | collective-permute-start | bytes 786440 | tf_op jit(solution)/shard_map/ppermute | solution.py:608
  96.3 12.3 %collective-permute-start.30 = (bf16[512,256]{1,0:T(8,128)(2,1)}, bf16[512,256]{1,0:T(8,128)(2,1)}, u32[]{:S(2)}, u32[]{:S(2)}) collective-permute-start(bf16[512,256]{1,0:T(8,128)(2,1)} %collective-permute-done.29.refs_2_), channel_id=1, source_target_pairs={{0,1},{1,0},{2,3},{3,2},{4,5},{5,4},{6,7},{7,6},{8,9},{9,8},{10,11... | collective-permute-start | bytes 786440 | tf_op jit(solution)/shard_map/ppermute | solution.py:608
  98.1 14.5 %collective-permute-start.27 = (bf16[512,256]{1,0:T(8,128)(2,1)S(1)}, bf16[512,256]{1,0:T(8,128)(2,1)}, u32[]{:S(2)}, u32[]{:S(2)}) collective-permute-start(bf16[512,256]{1,0:T(8,128)(2,1)S(1)} %combine.3.refs_4_), channel_id=1, source_target_pairs={{0,1},{1,0},{2,3},{3,2},{4,5},{5,4},{6,7},{7,6},{8,9},{9,8},{10,11... | collective-permute-start | bytes 786440 | tf_op jit(solution)/shard_map/ppermute | solution.py:608
  98.8 13.8 %collective-permute-start.24 = (bf16[512,256]{1,0:T(8,128)(2,1)S(1)}, bf16[512,256]{1,0:T(8,128)(2,1)}, u32[]{:S(2)}, u32[]{:S(2)}) collective-permute-start(bf16[512,256]{1,0:T(8,128)(2,1)S(1)} %combine.2.refs_4_.refs_0_), channel_id=1, source_target_pairs={{0,1},{1,0},{2,3},{3,2},{4,5},{5,4},{6,7},{7,6},{8,9},{9,8},{10,11... | collective-permute-start | bytes 786440 | tf_op jit(solution)/shard_map/ppermute | solution.py:608
  102.0 10.6 %collective-permute-start.26 = (bf16[512,256]{1,0:T(8,128)(2,1)S(1)}, bf16[512,256]{1,0:T(8,128)(2,1)}, u32[]{:S(2)}, u32[]{:S(2)}) collective-permute-start(bf16[512,256]{1,0:T(8,128)(2,1)S(1)} %collective-permute-done.25.refs_2_), channel_id=1, source_target_pairs={{0,1},{1,0},{2,3},{3,2},{4,5},{5,4},{6,7},{7,6},{8,9},{9,8},{10,11... | collective-permute-start | bytes 786440 | tf_op jit(solution)/shard_map/ppermute | solution.py:608
  107.6 7.1 %collective-permute-start.23 = (bf16[512,256]{1,0:T(8,128)(2,1)S(1)}, bf16[512,256]{1,0:T(8,128)(2,1)}, u32[]{:S(2)}, u32[]{:S(2)}) collective-permute-start(bf16[512,256]{1,0:T(8,128)(2,1)S(1)} %collective-permute-done.22.refs_0_), channel_id=1, source_target_pairs={{0,1},{1,0},{2,3},{3,2},{4,5},{5,4},{6,7},{7,6},{8,9},{9,8},{10,11... | collective-permute-start | bytes 786440 | tf_op jit(solution)/shard_map/ppermute | solution.py:608
  (4 other events, 5.1 us)

commit v4 on v3

--- a/solution.py
+++ b/solution.py
@@ -11,7 +11,7 @@
 QBLOCK = 64
 MBLOCK = 64
 RHEAD = 64
-LROWS = 16
+LROWS = 8
 
 FLOAT32 = jnp.float32
 BFLOAT = jnp.bfloat16
@@ -48,8 +48,8 @@
     return [pl.BlockSpec(memory_space=pl.ANY)] * count
 
 
-def up16(count):
-    return -(-count // 16) * 16
+def up8(count):
+    return -(-count // 8) * 8
 
 
 def entry(lines, row, lane):
@@ -89,16 +89,19 @@
 
         lax.fori_loop(0, owners, clear, 0)
 
-        def put(n, carry):
-            passage = ids_ref[n % per_block, n // per_block]
-            owner = passage // pass_dev
-            rank = fill_ref[owner]
-            fill_ref[owner] = rank + 1
-            pidx_ref[owner, rank] = passage - owner * pass_dev
-            blk_ref[owner, rank] = n // per_block + 1
+        scale = 65536 // pass_dev + 1
+
+        def put(b, carry):
+            for i in range(per_block):
+                passage = ids_ref[i, b]
+                owner = (passage * scale) >> 16
+                rank = fill_ref[owner]
+                fill_ref[owner] = rank + 1
+                pidx_ref[owner, rank] = passage - owner * pass_dev
+                blk_ref[owner, rank] = b + 1
             return carry
 
-        lax.fori_loop(0, ids_ref.shape[1] * per_block, put, 0)
+        lax.fori_loop(0, ids_ref.shape[1], put, 0)
         sum_ref[...] = jnp.zeros_like(sum_ref)
 
     sum_ref[...] += dot(tok_ref[...], w_ref[...])
@@ -141,7 +144,7 @@
         functools.partial(query_kernel, pass_dev, owners),
         grid=(steps,),
         out_shape=[jax.ShapeDtypeStruct((owners, capacity), jnp.int32)]
-        + [VMEM((rows + up16(owners), XHEAD), BFLOAT)] * heads + [group] * count,
+        + [VMEM((rows + up8(owners), XHEAD), BFLOAT)] * heads + [group] * count,
         in_specs=[smem, smem, pl.BlockSpec((rows, depth), lambda i: (0, i)),
                   pl.BlockSpec((depth, width), lambda i: (i, 0))] + whole(1),
         out_specs=[smem] + whole(heads + count),
@@ -446,7 +449,7 @@
     )(norm_gain.reshape(1, -1), *near_core(*flat), *deps)
 
 
-def attend_group(plen, first, q_ref, k_ref, v_ref, out_ref):
+def attend_group(plen, first, q_ref, k_ref, v_ref, out_refs):
     width = q_ref.shape[1]
     heads = width // XHEAD
     capacity = (q_ref.shape[0] - LROWS) // QBLOCK
@@ -461,47 +464,49 @@
     ones = jnp.ones((8, plen), BFLOAT)
     totals = [dot(ones, e, NT)[:1] for e in expon]
     outs = [dot(e, v_ref[spans[r], held[h]]) for e, (r, h) in zip(expon, units)]
-    sums = jnp.zeros((LROWS, QBLOCK), FLOAT32)
-    rowid = iota((LROWS, QBLOCK), 0)
+    rowid = iota((LROWS, 128), 0)
+    sums = [jnp.zeros((LROWS, 128), FLOAT32) for _ in range(heads)]
+    blank = jnp.zeros((1, 128 - QBLOCK), FLOAT32)
     for (r, h), out, total in zip(units, outs, totals):
-        out_ref[mine[r], cols[h]] = out.astype(BFLOAT)
+        out_refs[h][mine[r], :] = out.astype(BFLOAT)
+        total = jnp.concatenate([total, blank], axis=1)
         high = total.astype(BFLOAT).astype(FLOAT32)
-        where = 2 * (r * heads + h)
-        sums = jnp.where(rowid == where, high, sums)
-        sums = jnp.where(rowid == where + 1, total - high, sums)
-    out_ref[capacity * QBLOCK :, :] = jnp.zeros((LROWS, width), BFLOAT)
-    out_ref[capacity * QBLOCK :, :QBLOCK] = sums.astype(BFLOAT)
-
-
-def attend_kernel(plen, first, count, deps, k_ref, v_ref, *refs):
-    for q_ref, out_ref in zip(refs[:count], refs[count + deps :]):
-        attend_group(plen, first, q_ref, k_ref, v_ref, out_ref)
+        sums[h] = jnp.where(rowid == 2 * r, high, sums[h])
+        sums[h] = jnp.where(rowid == 2 * r + 1, total - high, sums[h])
+    for h, out_ref in enumerate(out_refs):
+        out_ref[capacity * QBLOCK :, :] = jnp.concatenate([sums[h], sums[h]], axis=1).astype(BFLOAT)
+
+
+def attend_kernel(plen, first, each, count, deps, k_ref, v_ref, *refs):
+    outs = refs[count + deps :]
+    for n, q_ref in enumerate(refs[:count]):
+        attend_group(plen, first, q_ref, k_ref, v_ref, outs[n * each : (n + 1) * each])
 
 
 def attend(groups, keys, values, plen, first, deps):
     count = len(groups)
-    return pl.pallas_call(
-        functools.partial(attend_kernel, plen, first, count, len(deps)),
-        out_shape=[VMEM(g.shape, BFLOAT) for g in groups],
+    rows, width = groups[0].shape
+    each = width // XHEAD
+    outs = pl.pallas_call(
+        functools.partial(attend_kernel, plen, first, each, count, len(deps)),
+        out_shape=[VMEM((rows, XHEAD), BFLOAT)] * (count * each),
         in_specs=whole(2 + count) + after(len(deps)),
-        out_specs=whole(count),
+        out_specs=whole(count * each),
         compiler_params=GRANT,
         name="attend",
     )(*near_core(keys, values, *groups), *deps)
-
-
-def add_group(blocks, head, part_ref, acc_ref, den_ref):
-    heads = part_ref.shape[1] // XHEAD
+    return [outs[h::each] for h in range(each)]
+
+
+def add_group(blocks, part_ref, acc_ref, den_ref):
     qrows = part_ref.shape[0] - LROWS
     lines = part_ref[qrows:, :QBLOCK].astype(FLOAT32)
-    cols = slice(head * XHEAD, (head + 1) * XHEAD)
     for r, block in enumerate(blocks):
         @pl.when(block > 0)
         def _(r=r, block=block):
             rows = pl.ds(pl.multiple_of((block - 1) * QBLOCK, QBLOCK), QBLOCK)
-            acc_ref[rows, :] += part_ref[r * QBLOCK : (r + 1) * QBLOCK, cols].astype(FLOAT32)
-            at = 2 * (r * heads + head)
-            den_ref[pl.ds(block - 1, 1), :] += lines[at : at + 1] + lines[at + 1 : at + 2]
+            acc_ref[rows, :] += part_ref[r * QBLOCK : (r + 1) * QBLOCK, :].astype(FLOAT32)
+            den_ref[pl.ds(block - 1, 1), :] += lines[2 * r : 2 * r + 1] + lines[2 * r + 1 : 2 * r + 2]
 
 
 def gather_kernel(count, deps, me_ref, blk_ref, *refs):
@@ -512,7 +517,7 @@
     den_ref[...] = jnp.zeros_like(den_ref)
     for k, part_ref in enumerate(parts):
         owner = me_ref[0] ^ k
-        add_group([blk_ref[owner, r] for r in range(capacity)], 0, part_ref, acc_ref, den_ref)
+        add_group([blk_ref[owner, r] for r in range(capacity)], part_ref, acc_ref, den_ref)
     rows, lines = acc_ref.shape[0], den_ref.shape[0]
     out_ref[:rows, :] = acc_ref[...].astype(BFLOAT)
     high, low = parts2(den_ref[...])
@@ -521,7 +526,7 @@
 
 
 def gather(me, blk, parts, rows, deps):
-    lines = up16(rows // QBLOCK)
+    lines = up8(rows // QBLOCK)
     smem = pl.BlockSpec(memory_space=SMEM)
     return pl.pallas_call(
         functools.partial(gather_kernel, len(parts), len(deps)),
@@ -534,7 +539,7 @@
     )(me, blk, *near_core(*parts), *deps)
 
 
-def combine_kernel(count, deps, head, me_ref, blk_ref, far_ref, *refs):
+def combine_kernel(count, deps, me_ref, blk_ref, far_ref, *refs):
     parts = refs[:count]
     out_ref, acc_ref, den_ref = refs[count + deps :]
     capacity = blk_ref.shape[1]
@@ -544,17 +549,17 @@
     den_ref[...] = tail[:, :QBLOCK] + tail[:, 128 : 128 + QBLOCK]
     for k, part_ref in enumerate(parts):
         owner = me_ref[0] ^ k
-        add_group([blk_ref[owner, r] for r in range(capacity)], head, part_ref, acc_ref, den_ref)
+        add_group([blk_ref[owner, r] for r in range(capacity)], part_ref, acc_ref, den_ref)
     turned = jnp.transpose(den_ref[...])
     for b in range(rows // QBLOCK):
         mine = slice(b * QBLOCK, (b + 1) * QBLOCK)
         out_ref[mine, :] = (acc_ref[mine, :] / turned[:, b : b + 1]).astype(BFLOAT)
 
 
-def combine(me, blk, far, parts, head, rows, deps):
+def combine(me, blk, far, parts, rows, deps):
     smem = pl.BlockSpec(memory_space=SMEM)
     return pl.pallas_call(
-        functools.partial(combine_kernel, len(parts), len(deps), head),
+        functools.partial(combine_kernel, len(parts), len(deps)),
         out_shape=VMEM((rows, XHEAD), BFLOAT),
         in_specs=[smem, smem] + whole(1 + len(parts)) + after(len(deps)),
         out_specs=pl.BlockSpec(memory_space=VMEM),
@@ -660,16 +665,15 @@
         far_blk, groups = relay(place, far_queries[h], rows, owners, capacity, [last])
         last = groups[0]
         far.append(swap_groups(groups))
-        if h == 0:
-            last = some_chunks(last)
+        last = some_chunks(last)
     far_parts = []
     for h in range(heads):
-        parts = attend(far[h], keys, values, plen, h, [last])
+        (parts,) = attend(far[h], keys, values, plen, h, [last])
         last = parts[0]
         far_parts.append(swap_groups(parts))
         if h == 0:
             near_parts = attend(near, keys, values, plen, 0, [last])
-            last = near_parts[0]
+            last = near_parts[0][0]
     returned = []
     for h in range(heads):
         sums = gather(place, far_blk, far_parts[h], rows, [last])
@@ -677,7 +681,9 @@
             near_parts, sums = lax.optimization_barrier((near_parts, sums))
         returned.append(swap(sums, half))
         if h == heads - 1:
-            near_parts = swap_groups(near_parts)
+            near_parts = [
+                swap_groups(p)
+                for p in near_parts]
         last = some_chunks(sums)
     while pieces:
         last = some_chunks(last)
@@ -686,7 +692,7 @@
     last = mixer_heads
     cross = {}
     for h in range(heads):
-        last = combine(place, blk, returned[h], near_parts, h, rows, [last])
+        last = combine(place, blk, returned[h], near_parts[h], rows, [last])
         for k, piece in enumerate(gather_tp(last, shards)):
             cross[k, h] = piece
     inner = functools.partial(VMEM, dtype=FLOAT32)

time: 117 us -> 121 us (1.034)
  the two profiles are of different devices: /device:TPU:27 before, /device:TPU:0 now
where the time goes in v4:
time: 121 us; the launch traced here: 120 us
  Pallas kernels  47.8 us (40%)
  starting transfers between devices  36 us (30%)
  waiting for transfers between devices  33.1 us (27%)
  local copies, waits for them, and re-layouts  2.97 us (2%)
    ppermute x25, starting transfers between devices, swap(): return lax.ppermute(value, 'st', [(i, i ^ bit) for i in range(owners)])  31.7 us
    ppermute x25, waiting for transfers between devices, swap(): return lax.ppermute(value, 'st', [(i, i ^ bit) for i in range(owners)])  22.7 us
    pallas_call x3, Pallas kernels, prepare(): pl.pallas_call(functools.partial(prepare_kernel, start, len(deps)), out_s...  12.2 us
    ppermute x9, waiting for transfers between devices, gather_tp(): pieces[j ^ bit] = lax.ppermute(pieces[j], 'tp', pairs)  10.4 us
    pallas_call x1, Pallas kernels, make_keyvals(): pl.pallas_call(keyval_kernel, grid=(pass_dev // group,), out_shape=[shape...  7.41 us
    pallas_call x3, Pallas kernels, over_tp(): pl.pallas_call(functools.partial(body, spots, blocks, len(deps)), out_sha...  6.09 us
    pallas_call x1, Pallas kernels, make_queries(): pl.pallas_call(functools.partial(query_kernel, pass_dev, owners), grid=(s...  5.48 us
    pallas_call x1, Pallas kernels, project(): pl.pallas_call(project_kernel, out_shape=[half, half, half, full, full, f...  4.7 us
  transfers between devices with their start and end apart: 34, of which 12 were waited for; matrix products, arithmetic and copies ran while one was open for 0% of the time, Pallas kernels for 33%

profile of v4, /device:TPU:0, one launch (start us, length us, event | category | flops | bytes accessed | tf_op | source)
XLA Modules:
  0.0 120.3 jit_solution(10447492953061436314)
XLA Ops:
  0.0 5.5 %queries.1 = (s32[8,4]{1,0:T(8,128)S(1)}, bf16[520,256]{1,0:T(8,128)(2,1)S(1)}, bf16[520,256]{1,0:T(8,128)(2,1)S(1)}, bf16[264,512]{1,0:T(8,128)(2,1)S(1)}, bf16...) custom-call(s32[1]{0:T(128)} %bitcast.1.me_ref, s32[4,8]{1,0:T(4,128)} %bitcast.16, ...), custom_call_target="tpu_custom_call" | custom-call | tf_op jit(solution)/shard_map/queries/pallas_call | solution.py:143
  5.5 3.0 %collective-permute-start = (bf16[264,512]{1,0:T(8,128)(2,1)S(1)}, bf16[264,512]{1,0:T(8,128)(2,1)S(1)}, u32[]{:S(2)}, u32[]{:S(2)}) collective-permute-start(bf16[264,512]{1,0:T(8,128)(2,1)S(1)} %get-tuple-element.75), channel_id=1, source_target_pairs={{0,4},{4,0},{8,12},{12,8},{16,20},{20,16},{24,28},{28,24},{1,5},{5... | collective-permute-start | bytes 811016 | tf_op jit(solution)/shard_map/ppermute | solution.py:635
  8.5 2.6 %collective-permute-start.3 = (bf16[520,256]{1,0:T(8,128)(2,1)S(1)}, bf16[520,256]{1,0:T(8,128)(2,1)S(1)}, u32[]{:S(2)}, u32[]{:S(2)}) collective-permute-start(bf16[520,256]{1,0:T(8,128)(2,1)S(1)} %get-tuple-element.78), channel_id=1, source_target_pairs={{0,16},{4,20},{8,24},{12,28},{16,0},{20,4},{24,8},{28,12},{1,17},{... | collective-permute-start | bytes 798728 | tf_op jit(solution)/shard_map/ppermute | solution.py:635
  11.3 7.4 %keyvals.1 = (bf16[1152,512]{1,0:T(8,128)(2,1)S(1)}, bf16[1152,512]{1,0:T(8,128)(2,1)S(1)}) custom-call(bf16[1152,2048]{1,0:T(8,128)(2,1)} %bitcast.15, bf16[2048,512]{1,0:T(8,128)(2,1)S(1)} %copy-done.2, bf16[2048,512]{1,0:T(8,128)(2,1)S(1)} %copy-done.3), custom_call_target="tpu_custom_call" | custom-call | tf_op jit(solution)/shard_map/keyvals/pallas_call | solution.py:205
  19.1 1.6 %collective-permute-start.1 = (bf16[264,512]{1,0:T(8,128)(2,1)S(1)}, bf16[264,512]{1,0:T(8,128)(2,1)S(1)}, u32[]{:S(2)}, u32[]{:S(2)}) collective-permute-start(bf16[264,512]{1,0:T(8,128)(2,1)S(1)} %get-tuple-element.76), channel_id=1, source_target_pairs={{0,8},{4,12},{8,0},{12,4},{16,24},{20,28},{24,16},{28,20},{1,9},{5... | collective-permute-start | bytes 811016 | tf_op jit(solution)/shard_map/ppermute | solution.py:635
  20.9 4.7 %project.1 = (bf16[512,256]{1,0:T(8,128)(2,1)S(1)}, bf16[512,256]{1,0:T(8,128)(2,1)S(1)}, bf16[512,256]{1,0:T(8,128)(2,1)S(1)}, f32[512,256]{1,0:T(8,128)S(1)}, ...) custom-call(bf16[512,2048]{1,0:T(8,128)(2,1)S(1)} %copy-done, ...), custom_call_target="tpu_custom_call" | custom-call | tf_op jit(solution)/shard_map/project/pallas_call | solution.py:251
  25.6 4.1 %collective-permute-done.3.q_ref = bf16[520,256]{1,0:T(8,128)(2,1)S(1)} collective-permute-done((bf16[520,256]{1,0:T(8,128)(2,1)S(1)}, bf16[520,256]{1,0:T(8,128)(2,1)S(1)}, u32[]{:S(2)}, u32[]{:S(2)}) %collective-permute-start.3) | collective-permute-done | bytes 266272 | tf_op jit(solution)/shard_map/ppermute | solution.py:635
  29.7 0.8 relay.2
  31.1 3.5 %collective-permute-done.7.q_ref = bf16[520,256]{1,0:T(8,128)(2,1)S(1)} collective-permute-done((bf16[520,256]{1,0:T(8,128)(2,1)S(1)}, bf16[520,256]{1,0:T(8,128)(2,1)S(1)}, u32[]{:S(2)}, u32[]{:S(2)}) %collective-permute-start.7) | collective-permute-done | bytes 266272 | tf_op jit(solution)/shard_map/ppermute | solution.py:635
  35.1 1.4 %collective-permute-start.6 = (bf16[264,256]{1,0:T(8,128)(2,1)S(1)}, bf16[264,256]{1,0:T(8,128)(2,1)S(1)}, u32[]{:S(2)}, u32[]{:S(2)}) collective-permute-start(bf16[264,256]{1,0:T(8,128)(2,1)S(1)} %get-tuple-element.83), channel_id=1, source_target_pairs={{0,12},{4,8},{8,4},{12,0},{16,28},{20,24},{24,20},{28,16},{1,13},{... | collective-permute-start | bytes 405512 | tf_op jit(solution)/shard_map/ppermute | solution.py:635
  36.5 4.2 %prepare.3 = (f32[192,256]{1,0:T(8,128)S(1)}, f32[192,256]{1,0:T(8,128)S(1)}, f32[192,256]{1,0:T(8,128)S(1)}, f32[192,256]{1,0:T(8,128)S(1)}) custom-call(bf16[512,256]{1,0:T(8,128)(2,1)S(1)} %get-tuple-element.79.refs_0_.q_ref, bf16[512,256]{1,0:T(8,128)(2,1)S(1)} %get-tuple-element.84.k_ref, bf16[512,256]{1,0:T(8,128)(2,1)S(1)} %get-tuple-element.85.v_ref, ...), custom_call_target="tpu_custom_call" | custom-call | tf_op jit(solution)/shard_map/prepare/pallas_call | solution.py:397
  40.7 0.9 relay.3
  41.5 1.6 %collective-permute-start.8 = (bf16[264,256]{1,0:T(8,128)(2,1)S(1)}, bf16[264,256]{1,0:T(8,128)(2,1)S(1)}, u32[]{:S(2)}, u32[]{:S(2)}) collective-permute-start(bf16[264,256]{1,0:T(8,128)(2,1)S(1)} %get-tuple-element.103), channel_id=1, source_target_pairs={{0,4},{4,0},{8,12},{12,8},{16,20},{20,16},{24,28},{28,24},{1,5},{5... | collective-permute-start | bytes 405512 | tf_op jit(solution)/shard_map/ppermute | solution.py:635
  43.7 2.4 %collective-permute-done.6.refs_3_ = bf16[264,256]{1,0:T(8,128)(2,1)S(1)} collective-permute-done((bf16[264,256]{1,0:T(8,128)(2,1)S(1)}, bf16[264,256]{1,0:T(8,128)(2,1)S(1)}, u32[]{:S(2)}, u32[]{:S(2)}) %collective-permute-start.6) | collective-permute-done | bytes 135200 | tf_op jit(solution)/shard_map/ppermute | solution.py:635
  46.2 4.2 %prepare.4 = (f32[192,256]{1,0:T(8,128)S(1)}, f32[192,256]{1,0:T(8,128)S(1)}, f32[192,256]{1,0:T(8,128)S(1)}, f32[192,256]{1,0:T(8,128)S(1)}) custom-call(bf16[512,256]{1,0:T(8,128)(2,1)S(1)} %get-tuple-element.79.refs_0_.q_ref, bf16[512,256]{1,0:T(8,128)(2,1)S(1)} %get-tuple-element.84.k_ref, bf16[512,256]{1,0:T(8,128)(2,1)S(1)} %get-tuple-element.85.v_ref, ...), custom_call_target="tpu_custom_call" | custom-call | tf_op jit(solution)/shard_map/prepare/pallas_call | solution.py:397
  50.4 1.4 %attend.3 = (bf16[264,256]{1,0:T(8,128)(2,1)S(1)}, bf16[264,256]{1,0:T(8,128)(2,1)S(1)}, bf16[264,256]{1,0:T(8,128)(2,1)S(1)}, bf16[264,256]{1,0:T(8,128)(2,1)S(1)}) custom-call(bf16[1152,512]{1,0:T(8,128)(2,1)S(1)} %get-tuple-element.72.dep_ref.k_ref, bf16[1152,512]{1,0:T(8,128)(2,1)S(1)} %get-tuple-element.73.v_ref, ...), custom_call_target="tpu_custom_call" | custom-call | tf_op jit(solution)/shard_map/attend/pallas_call | solution.py:490
  51.8 1.6 %collective-permute-start.14 = (bf16[264,256]{1,0:T(8,128)(2,1)S(1)}, bf16[264,256]{1,0:T(8,128)(2,1)S(1)}, u32[]{:S(2)}, u32[]{:S(2)}) collective-permute-start(bf16[264,256]{1,0:T(8,128)(2,1)S(1)} %get-tuple-element.110), channel_id=1, source_target_pairs={{0,4},{4,0},{8,12},{12,8},{16,20},{20,16},{24,28},{28,24},{1,5},{5... | collective-permute-start | bytes 405512 | tf_op jit(solution)/shard_map/ppermute | solution.py:635
  53.4 2.0 %collective-permute-start.15 = (bf16[264,256]{1,0:T(8,128)(2,1)S(1)}, bf16[264,256]{1,0:T(8,128)(2,1)S(1)}, u32[]{:S(2)}, u32[]{:S(2)}) collective-permute-start(bf16[264,256]{1,0:T(8,128)(2,1)S(1)} %get-tuple-element.111), channel_id=1, source_target_pairs={{0,8},{4,12},{8,0},{12,4},{16,24},{20,28},{24,16},{28,20},{1,9},{5... | collective-permute-start | bytes 405512 | tf_op jit(solution)/shard_map/ppermute | solution.py:635
  55.4 1.7 %attend.4 = (bf16[264,256]{1,0:T(8,128)(2,1)S(1)}, bf16[264,256]{1,0:T(8,128)(2,1)S(1)}, bf16[264,256]{1,0:T(8,128)(2,1)S(1)}, bf16[264,256]{1,0:T(8,128)(2,1)S(...) custom-call(bf16[1152,512]{1,0:T(8,128)(2,1)S(1)} %get-tuple-element, ...), custom_call_target="tpu_custom_call" | custom-call | tf_op jit(solution)/shard_map/attend/pallas_call | solution.py:490
  57.1 1.0 collective-permute-start.16
  58.1 1.2 attend.5
  59.9 1.9 %collective-permute-start.12 = (bf16[264,256]{1,0:T(8,128)(2,1)S(1)}, bf16[264,256]{1,0:T(8,128)(2,1)S(1)}, u32[]{:S(2)}, u32[]{:S(2)}) collective-permute-start(bf16[264,256]{1,0:T(8,128)(2,1)S(1)} %get-tuple-element.108), channel_id=1, source_target_pairs={{0,8},{4,12},{8,0},{12,4},{16,24},{20,28},{24,16},{28,20},{1,9},{5... | collective-permute-start | bytes 405512 | tf_op jit(solution)/shard_map/ppermute | solution.py:635
  61.9 1.0 collective-permute-start.13
  62.9 1.0 collective-permute-done.16.refs_3_
  63.9 0.8 gather.2.refs_0_
  64.7 3.8 %prepare.5 = (f32[128,256]{1,0:T(8,128)S(1)}, f32[128,256]{1,0:T(8,128)S(1)}, f32[128,256]{1,0:T(8,128)S(1)}, f32[128,256]{1,0:T(8,128)S(1)}) custom-call(bf16[512,256]{1,0:T(8,128)(2,1)S(1)} %get-tuple-element.79.refs_0_.q_ref, bf16[512,256]{1,0:T(8,128)(2,1)S(1)} %get-tuple-element.84.k_ref, bf16[512,256]{1,0:T(8,128)(2,1)S(1)} %get-tuple-element.85.v_ref, ...), custom_call_target="tpu_custom_call" | custom-call | tf_op jit(solution)/shard_map/prepare/pallas_call | solution.py:397
  68.8 0.8 gather.3
  69.7 1.9 %collective-permute-start.22 = (bf16[264,256]{1,0:T(8,128)(2,1)S(1)}, bf16[264,256]{1,0:T(8,128)(2,1)S(1)}, u32[]{:S(2)}, u32[]{:S(2)}) collective-permute-start(bf16[264,256]{1,0:T(8,128)(2,1)S(1)} %get-tuple-element.120), channel_id=1, source_target_pairs={{0,4},{4,0},{8,12},{12,8},{16,20},{20,16},{24,28},{28,24},{1,5},{5... | collective-permute-start | bytes 405512 | tf_op jit(solution)/shard_map/ppermute | solution.py:635
  71.6 1.6 %collective-permute-start.24 = (bf16[264,256]{1,0:T(8,128)(2,1)S(1)}, bf16[264,256]{1,0:T(8,128)(2,1)S(1)}, u32[]{:S(2)}, u32[]{:S(2)}) collective-permute-start(bf16[264,256]{1,0:T(8,128)(2,1)S(1)} %get-tuple-element.122), channel_id=1, source_target_pairs={{0,12},{4,8},{8,4},{12,0},{16,28},{20,24},{24,20},{28,16},{1,13},{... | collective-permute-start | bytes 405512 | tf_op jit(solution)/shard_map/ppermute | solution.py:635
  73.2 6.0 %collective-permute-start.21 = (bf16[520,256]{1,0:T(8,128)(2,1)S(1)}, bf16[520,256]{1,0:T(8,128)(2,1)S(1)}, u32[]{:S(2)}, u32[]{:S(2)}) collective-permute-start(bf16[520,256]{1,0:T(8,128)(2,1)S(1)} %gather.2.refs_0_), channel_id=1, source_target_pairs={{0,16},{4,20},{8,24},{12,28},{16,0},{20,4},{24,8},{28,12},{1,17},{... | collective-permute-start | bytes 798728 | tf_op jit(solution)/shard_map/ppermute | solution.py:635
  79.2 0.8 collective-permute-start.18
  80.1 0.9 collective-permute-start.19
  81.0 5.1 %collective-permute-done.24.refs_3_ = bf16[264,256]{1,0:T(8,128)(2,1)S(1)} collective-permute-done((bf16[264,256]{1,0:T(8,128)(2,1)S(1)}, bf16[264,256]{1,0:T(8,128)(2,1)S(1)}, u32[]{:S(2)}, u32[]{:S(2)}) %collective-permute-start.24) | collective-permute-done | bytes 135200 | tf_op jit(solution)/shard_map/ppermute | solution.py:635
  86.1 2.2 %scan.1.refs_4_.refs_0_ = bf16[512,256]{1,0:T(8,128)(2,1)S(1)} custom-call(f32[1,256]{1,0:T(1,128)S(1)} %bitcast.14, f32[192,256]{1,0:T(8,128)S(1)} %get-tuple-element.90.refs_0_, f32[192,256]{1,0:T(8,128)S(1)} %get-tuple-element.123.refs_1_, f32[192,256]{1,0:T(8,128)S(1)} %get-tuple-element.124.refs_2_, f32[192,256]{1,0:T(8,128)S(1)} %get-tuple-element.125.refs_3_, ...), custom_call_target="tpu_custom_call" | custom-call | tf_op jit(solution)/shard_map/scan/pallas_call | solution.py:441
  88.3 6.1 %collective-permute-done.21.far_ref = bf16[520,256]{1,0:T(8,128)(2,1)S(1)} collective-permute-done((bf16[520,256]{1,0:T(8,128)(2,1)S(1)}, bf16[520,256]{1,0:T(8,128)(2,1)S(1)}, u32[]{:S(2)}, u32[]{:S(2)}) %collective-permute-start.21) | collective-permute-done | bytes 266272 | tf_op jit(solution)/shard_map/ppermute | solution.py:635
  94.3 1.5 %collective-permute-start.32 = (bf16[512,256]{1,0:T(8,128)(2,1)S(1)}, bf16[512,256]{1,0:T(8,128)(2,1)}, u32[]{:S(2)}, u32[]{:S(2)}) collective-permute-start(bf16[512,256]{1,0:T(8,128)(2,1)S(1)} %scan.1.refs_4_.refs_0_), channel_id=1, source_target_pairs={{0,2},{1,3},{2,0},{3,1},{4,6},{5,7},{6,4},{7,5},{8,10},{9,11},{10,... | collective-permute-start | bytes 786440 | tf_op jit(solution)/shard_map/ppermute | solution.py:613
  95.8 1.1 combine.2.refs_4_.refs_0_
  97.7 1.1 combine.3.refs_4_
  98.7 1.6 %collective-permute-start.25 = (bf16[512,256]{1,0:T(8,128)(2,1)S(1)}, bf16[512,256]{1,0:T(8,128)(2,1)S(1)}, u32[]{:S(2)}, u32[]{:S(2)}) collective-permute-start(bf16[512,256]{1,0:T(8,128)(2,1)S(1)} %combine.3.refs_4_), channel_id=1, source_target_pairs={{0,2},{1,3},{2,0},{3,1},{4,6},{5,7},{6,4},{7,5},{8,10},{9,11},{10,... | collective-permute-start | bytes 786440 | tf_op jit(solution)/shard_map/ppermute | solution.py:613
  100.3 1.1 collective-permute-done.32.refs_2_
  101.9 0.7 copy-done.13
  102.6 4.3 %collective-permute-done.28.refs_2_ = bf16[512,256]{1,0:T(8,128)(2,1)S(1)} collective-permute-done((bf16[512,256]{1,0:T(8,128)(2,1)S(1)}, bf16[512,256]{1,0:T(8,128)(2,1)S(1)}, u32[]{:S(2)}, u32[]{:S(2)}) %collective-permute-start.28) | collective-permute-done | bytes 262176 | tf_op jit(solution)/shard_map/ppermute | solution.py:613
  106.9 5.0 %collective-permute-done.25.refs_0_ = bf16[512,256]{1,0:T(8,128)(2,1)S(1)} collective-permute-done((bf16[512,256]{1,0:T(8,128)(2,1)S(1)}, bf16[512,256]{1,0:T(8,128)(2,1)S(1)}, u32[]{:S(2)}, u32[]{:S(2)}) %collective-permute-start.25) | collective-permute-done | bytes 262176 | tf_op jit(solution)/shard_map/ppermute | solution.py:613
  111.9 1.2 %copy-done.9 = bf16[1024,512]{1,0:T(8,128)(2,1)S(1)} copy-done((bf16[1024,512]{1,0:T(8,128)(2,1)S(1)}, bf16[1024,512]{1,0:T(8,128)(2,1)}, u32[]{:S(2)}) %copy-start.9) | copy-done | bytes 1048600
  113.2 0.9 copy-done.14
  114.1 1.7 %shard_map.199.refs_7_.refs_5_ = f32[512,512]{1,0:T(8,128)S(1)} custom-call(s32[1]{0:T(128)} %bitcast.me_ref, bf16[512,256]{1,0:T(8,128)(2,1)S(1)} %scan.1.refs_4_.refs_0_, bf16[512,256]{1,0:T(8,128)(2,1)S(1)} %copy-done.14, bf16[512,256]{1,0:T(8,128)(2,1)} %collective-permute-done.32.refs_2_, bf16[512,256]{1,0:T(8,128)(2,1)} %collective-permute-done.33.refs_3_, ...), custom_call_target="tpu_custom_call" | custom-call | tf_op jit(solution)/shard_map/pallas_call | solution.py:597
  115.9 2.2 %shard_map.200.refs_3_ = f32[512,512]{1,0:T(8,128)S(1)} custom-call(s32[1]{0:T(128)} %bitcast.me_ref, bf16[512,256]{1,0:T(8,128)(2,1)S(1)} %combine.2.refs_4_.refs_0_, bf16[512,256]{1,0:T(8,128)(2,1)} %collective-permute-done.27.refs_1_, bf16[512,256]{1,0:T(8,128)(2,1)S(1)} %collective-permute-done.28.refs_2_, ...), custom_call_target="tpu_custom_call" | custom-call | tf_op jit(solution)/shard_map/pallas_call | solution.py:597
  118.1 2.2 %shard_map.201 = bf16[512,512]{1,0:T(8,128)(2,1)} custom-call(s32[1]{0:T(128)} %bitcast.me_ref, bf16[512,256]{1,0:T(8,128)(2,1)S(1)} %collective-permute-done.25.refs_0_, bf16[512,256]{1,0:T(8,128)(2,1)} %collective-permute-done.26.refs_1_, bf16[2048,512]{1,0:T(8,128)(2,1)S(1)} %copy-done.1, f32[512,512]{1,0:T(8,128)S(1)} %shard_map.200.refs_3_, ...), custom_call_target="tpu_custom_call" | custom-call | tf_op jit(solution)/shard_map/pallas_call | solution.py:597
  (81 shorter events, 4.6 us)
Async XLA Ops:
  0.0 11.1 %copy-start.2 = (bf16[2048,512]{1,0:T(8,128)(2,1)S(1)}, bf16[2048,512]{1,0:T(8,128)(2,1)}, u32[]{:S(2)}) copy-start(bf16[2048,512]{1,0:T(8,128)(2,1)} %wk_ref.1) | copy-start | bytes 6291460
  0.0 11.1 %copy-start.3 = (bf16[2048,512]{1,0:T(8,128)(2,1)S(1)}, bf16[2048,512]{1,0:T(8,128)(2,1)}, u32[]{:S(2)}) copy-start(bf16[2048,512]{1,0:T(8,128)(2,1)} %wv_ref.1) | copy-start | bytes 6291460
  5.5 29.6 %collective-permute-start = (bf16[264,512]{1,0:T(8,128)(2,1)S(1)}, bf16[264,512]{1,0:T(8,128)(2,1)S(1)}, u32[]{:S(2)}, u32[]{:S(2)}) collective-permute-start(bf16[264,512]{1,0:T(8,128)(2,1)S(1)} %get-tuple-element.75), channel_id=1, source_target_pairs={{0,4},{4,0},{8,12},{12,8},{16,20},{20,16},{24,28},{28,24},{1,5},{5... | collective-permute-start | bytes 811016 | tf_op jit(solution)/shard_map/ppermute | solution.py:635
  8.5 21.2 %collective-permute-start.3 = (bf16[520,256]{1,0:T(8,128)(2,1)S(1)}, bf16[520,256]{1,0:T(8,128)(2,1)S(1)}, u32[]{:S(2)}, u32[]{:S(2)}) collective-permute-start(bf16[520,256]{1,0:T(8,128)(2,1)S(1)} %get-tuple-element.78), channel_id=1, source_target_pairs={{0,16},{4,20},{8,24},{12,28},{16,0},{20,4},{24,8},{28,12},{1,17},{... | collective-permute-start | bytes 798728 | tf_op jit(solution)/shard_map/ppermute | solution.py:635
  11.1 9.7 %copy-start = (bf16[512,2048]{1,0:T(8,128)(2,1)S(1)}, bf16[512,2048]{1,0:T(8,128)(2,1)}, u32[]{:S(2)}) copy-start(bf16[512,2048]{1,0:T(8,128)(2,1)} %tok_ref.3) | copy-start | bytes 6291460
  11.1 9.7 %copy-start.4 = (bf16[2048,256]{1,0:T(8,128)(2,1)S(1)}, bf16[2048,256]{1,0:T(8,128)(2,1)}, u32[]{:S(2)}) copy-start(bf16[2048,256]{1,0:T(8,128)(2,1)} %mq_ref.1) | copy-start | bytes 3145732
  11.1 9.7 %copy-start.5 = (bf16[2048,256]{1,0:T(8,128)(2,1)S(1)}, bf16[2048,256]{1,0:T(8,128)(2,1)}, u32[]{:S(2)}) copy-start(bf16[2048,256]{1,0:T(8,128)(2,1)} %mk_ref.1) | copy-start | bytes 3145732
  11.2 9.7 %copy-start.6 = (bf16[2048,256]{1,0:T(8,128)(2,1)S(1)}, bf16[2048,256]{1,0:T(8,128)(2,1)}, u32[]{:S(2)}) copy-start(bf16[2048,256]{1,0:T(8,128)(2,1)} %mv_ref.1) | copy-start | bytes 3145732
  11.2 9.7 %copy-start.10 = (bf16[2048,128]{1,0:T(8,128)(2,1)S(1)}, bf16[2048,128]{1,0:T(8,128)(2,1)}, u32[]{:S(2)}) copy-start(bf16[2048,128]{1,0:T(8,128)(2,1)} %gd_ref.1) | copy-start | bytes 1572868
  11.2 9.7 %copy-start.11 = (bf16[2048,64]{0,1:T(8,128)(2,1)S(1)}, bf16[2048,64]{0,1:T(8,128)(2,1)}, u32[]{:S(2)}) copy-start(bf16[2048,64]{0,1:T(8,128)(2,1)} %param.25) | copy-start | bytes 786436
  11.2 9.7 %copy-start.12 = (bf16[2048,64]{0,1:T(8,128)(2,1)S(1)}, bf16[2048,64]{0,1:T(8,128)(2,1)}, u32[]{:S(2)}) copy-start(bf16[2048,64]{0,1:T(8,128)(2,1)} %param.29) | copy-start | bytes 786436
  11.2 9.7 %copy-start.15 = (bf16[128,512]{1,0:T(8,128)(2,1)S(1)}, bf16[128,512]{1,0:T(8,128)(2,1)}, u32[]{:S(2)}) copy-start(bf16[128,512]{1,0:T(8,128)(2,1)} %gu_ref.1) | copy-start | bytes 393220
  11.2 9.7 %copy-start.16 = (bf16[64,256]{1,0:T(8,128)(2,1)S(1)}, bf16[64,256]{1,0:T(8,128)(2,1)}, u32[]{:S(2)}) copy-start(bf16[64,256]{1,0:T(8,128)(2,1)} %du_ref.1) | copy-start | bytes 98308
  18.7 15.9 %collective-permute-start.7 = (bf16[520,256]{1,0:T(8,128)(2,1)S(1)}, bf16[520,256]{1,0:T(8,128)(2,1)S(1)}, u32[]{:S(2)}, u32[]{:S(2)}) collective-permute-start(bf16[520,256]{1,0:T(8,128)(2,1)S(1)} %get-tuple-element.89), channel_id=1, source_target_pairs={{0,16},{4,20},{8,24},{12,28},{16,0},{20,4},{24,8},{28,12},{1,17},{... | collective-permute-start | bytes 798728 | tf_op jit(solution)/shard_map/ppermute | solution.py:635
  19.1 32.7 %collective-permute-start.1 = (bf16[264,512]{1,0:T(8,128)(2,1)S(1)}, bf16[264,512]{1,0:T(8,128)(2,1)S(1)}, u32[]{:S(2)}, u32[]{:S(2)}) collective-permute-start(bf16[264,512]{1,0:T(8,128)(2,1)S(1)} %get-tuple-element.76), channel_id=1, source_target_pairs={{0,8},{4,12},{8,0},{12,4},{16,24},{20,28},{24,16},{28,20},{1,9},{5... | collective-permute-start | bytes 811016 | tf_op jit(solution)/shard_map/ppermute | solution.py:635
  20.7 32.7 %collective-permute-start.2 = (bf16[264,512]{1,0:T(8,128)(2,1)S(1)}, bf16[264,512]{1,0:T(8,128)(2,1)S(1)}, u32[]{:S(2)}, u32[]{:S(2)}) collective-permute-start(bf16[264,512]{1,0:T(8,128)(2,1)S(1)} %get-tuple-element.77), channel_id=1, source_target_pairs={{0,12},{4,8},{8,4},{12,0},{16,28},{20,24},{24,20},{28,16},{1,13},{... | collective-permute-start | bytes 811016 | tf_op jit(solution)/shard_map/ppermute | solution.py:635
  25.6 24.8 %copy-start.7 = (f32[512,512]{1,0:T(8,128)}, f32[512,512]{1,0:T(8,128)S(1)}, u32[]{:S(2)}) copy-start(f32[512,512]{1,0:T(8,128)S(1)} %get-tuple-element.132.refs_4_) | copy-start | bytes 3145732
  30.6 11.0 %collective-permute-start.4 = (bf16[264,256]{1,0:T(8,128)(2,1)S(1)}, bf16[264,256]{1,0:T(8,128)(2,1)S(1)}, u32[]{:S(2)}, u32[]{:S(2)}) collective-permute-start(bf16[264,256]{1,0:T(8,128)(2,1)S(1)} %get-tuple-element.81), channel_id=1, source_target_pairs={{0,4},{4,0},{8,12},{12,8},{16,20},{20,16},{24,28},{28,24},{1,5},{5... | collective-permute-start | bytes 405512 | tf_op jit(solution)/shard_map/ppermute | solution.py:635
  34.5 8.7 %collective-permute-start.5 = (bf16[264,256]{1,0:T(8,128)(2,1)S(1)}, bf16[264,256]{1,0:T(8,128)(2,1)S(1)}, u32[]{:S(2)}, u32[]{:S(2)}) collective-permute-start(bf16[264,256]{1,0:T(8,128)(2,1)S(1)} %get-tuple-element.82), channel_id=1, source_target_pairs={{0,8},{4,12},{8,0},{12,4},{16,24},{20,28},{24,16},{28,20},{1,9},{5... | collective-permute-start | bytes 405512 | tf_op jit(solution)/shard_map/ppermute | solution.py:635
  35.1 11.1 %collective-permute-start.6 = (bf16[264,256]{1,0:T(8,128)(2,1)S(1)}, bf16[264,256]{1,0:T(8,128)(2,1)S(1)}, u32[]{:S(2)}, u32[]{:S(2)}) collective-permute-start(bf16[264,256]{1,0:T(8,128)(2,1)S(1)} %get-tuple-element.83), channel_id=1, source_target_pairs={{0,12},{4,8},{8,4},{12,0},{16,28},{20,24},{24,20},{28,16},{1,13},{... | collective-permute-start | bytes 405512 | tf_op jit(solution)/shard_map/ppermute | solution.py:635
  41.5 15.5 %collective-permute-start.8 = (bf16[264,256]{1,0:T(8,128)(2,1)S(1)}, bf16[264,256]{1,0:T(8,128)(2,1)S(1)}, u32[]{:S(2)}, u32[]{:S(2)}) collective-permute-start(bf16[264,256]{1,0:T(8,128)(2,1)S(1)} %get-tuple-element.103), channel_id=1, source_target_pairs={{0,4},{4,0},{8,12},{12,8},{16,20},{20,16},{24,28},{28,24},{1,5},{5... | collective-permute-start | bytes 405512 | tf_op jit(solution)/shard_map/ppermute | solution.py:635
  43.3 14.8 %collective-permute-start.9 = (bf16[264,256]{1,0:T(8,128)(2,1)S(1)}, bf16[264,256]{1,0:T(8,128)(2,1)S(1)}, u32[]{:S(2)}, u32[]{:S(2)}) collective-permute-start(bf16[264,256]{1,0:T(8,128)(2,1)S(1)} %get-tuple-element.104), channel_id=1, source_target_pairs={{0,8},{4,12},{8,0},{12,4},{16,24},{20,28},{24,16},{28,20},{1,9},{5... | collective-permute-start | bytes 405512 | tf_op jit(solution)/shard_map/ppermute | solution.py:635
  46.2 11.9 %collective-permute-start.10 = (bf16[264,256]{1,0:T(8,128)(2,1)S(1)}, bf16[264,256]{1,0:T(8,128)(2,1)S(1)}, u32[]{:S(2)}, u32[]{:S(2)}) collective-permute-start(bf16[264,256]{1,0:T(8,128)(2,1)S(1)} %get-tuple-element.105), channel_id=1, source_target_pairs={{0,12},{4,8},{8,4},{12,0},{16,28},{20,24},{24,20},{28,16},{1,13},{... | collective-permute-start | bytes 405512 | tf_op jit(solution)/shard_map/ppermute | solution.py:635
  51.8 10.1 %collective-permute-start.14 = (bf16[264,256]{1,0:T(8,128)(2,1)S(1)}, bf16[264,256]{1,0:T(8,128)(2,1)S(1)}, u32[]{:S(2)}, u32[]{:S(2)}) collective-permute-start(bf16[264,256]{1,0:T(8,128)(2,1)S(1)} %get-tuple-element.110), channel_id=1, source_target_pairs={{0,4},{4,0},{8,12},{12,8},{16,20},{20,16},{24,28},{28,24},{1,5},{5... | collective-permute-start | bytes 405512 | tf_op jit(solution)/shard_map/ppermute | solution.py:635
  53.4 9.5 %collective-permute-start.15 = (bf16[264,256]{1,0:T(8,128)(2,1)S(1)}, bf16[264,256]{1,0:T(8,128)(2,1)S(1)}, u32[]{:S(2)}, u32[]{:S(2)}) collective-permute-start(bf16[264,256]{1,0:T(8,128)(2,1)S(1)} %get-tuple-element.111), channel_id=1, source_target_pairs={{0,8},{4,12},{8,0},{12,4},{16,24},{20,28},{24,16},{28,20},{1,9},{5... | collective-permute-start | bytes 405512 | tf_op jit(solution)/shard_map/ppermute | solution.py:635
  57.1 6.8 %collective-permute-start.16 = (bf16[264,256]{1,0:T(8,128)(2,1)S(1)}, bf16[264,256]{1,0:T(8,128)(2,1)S(1)}, u32[]{:S(2)}, u32[]{:S(2)}) collective-permute-start(bf16[264,256]{1,0:T(8,128)(2,1)S(1)} %get-tuple-element.112), channel_id=1, source_target_pairs={{0,12},{4,8},{8,4},{12,0},{16,28},{20,24},{24,20},{28,16},{1,13},{... | collective-permute-start | bytes 405512 | tf_op jit(solution)/shard_map/ppermute | solution.py:635
  59.3 9.3 %collective-permute-start.11 = (bf16[264,256]{1,0:T(8,128)(2,1)S(1)}, bf16[264,256]{1,0:T(8,128)(2,1)S(1)}, u32[]{:S(2)}, u32[]{:S(2)}) collective-permute-start(bf16[264,256]{1,0:T(8,128)(2,1)S(1)} %get-tuple-element.107), channel_id=1, source_target_pairs={{0,4},{4,0},{8,12},{12,8},{16,20},{20,16},{24,28},{28,24},{1,5},{5... | collective-permute-start | bytes 405512 | tf_op jit(solution)/shard_map/ppermute | solution.py:635
  59.9 8.6 %collective-permute-start.12 = (bf16[264,256]{1,0:T(8,128)(2,1)S(1)}, bf16[264,256]{1,0:T(8,128)(2,1)S(1)}, u32[]{:S(2)}, u32[]{:S(2)}) collective-permute-start(bf16[264,256]{1,0:T(8,128)(2,1)S(1)} %get-tuple-element.108), channel_id=1, source_target_pairs={{0,8},{4,12},{8,0},{12,4},{16,24},{20,28},{24,16},{28,20},{1,9},{5... | collective-permute-start | bytes 405512 | tf_op jit(solution)/shard_map/ppermute | solution.py:635
  61.9 6.9 %collective-permute-start.13 = (bf16[264,256]{1,0:T(8,128)(2,1)S(1)}, bf16[264,256]{1,0:T(8,128)(2,1)S(1)}, u32[]{:S(2)}, u32[]{:S(2)}) collective-permute-start(bf16[264,256]{1,0:T(8,128)(2,1)S(1)} %get-tuple-element.109), channel_id=1, source_target_pairs={{0,12},{4,8},{8,4},{12,0},{16,28},{20,24},{24,20},{28,16},{1,13},{... | collective-permute-start | bytes 405512 | tf_op jit(solution)/shard_map/ppermute | solution.py:635
  63.9 22.2 %copy-start.20 = (f32[256]{0:T(256)S(1)}, f32[256]{0:T(256)}, u32[]{:S(2)}) copy-start(f32[256]{0:T(256)} %param.31) | copy-start | bytes 3076
  69.7 9.6 %collective-permute-start.22 = (bf16[264,256]{1,0:T(8,128)(2,1)S(1)}, bf16[264,256]{1,0:T(8,128)(2,1)S(1)}, u32[]{:S(2)}, u32[]{:S(2)}) collective-permute-start(bf16[264,256]{1,0:T(8,128)(2,1)S(1)} %get-tuple-element.120), channel_id=1, source_target_pairs={{0,4},{4,0},{8,12},{12,8},{16,20},{20,16},{24,28},{28,24},{1,5},{5... | collective-permute-start | bytes 405512 | tf_op jit(solution)/shard_map/ppermute | solution.py:635
  71.6 8.4 %collective-permute-start.23 = (bf16[264,256]{1,0:T(8,128)(2,1)S(1)}, bf16[264,256]{1,0:T(8,128)(2,1)S(1)}, u32[]{:S(2)}, u32[]{:S(2)}) collective-permute-start(bf16[264,256]{1,0:T(8,128)(2,1)S(1)} %get-tuple-element.121), channel_id=1, source_target_pairs={{0,8},{4,12},{8,0},{12,4},{16,24},{20,28},{24,16},{28,20},{1,9},{5... | collective-permute-start | bytes 405512 | tf_op jit(solution)/shard_map/ppermute | solution.py:635
  71.6 14.4 %collective-permute-start.24 = (bf16[264,256]{1,0:T(8,128)(2,1)S(1)}, bf16[264,256]{1,0:T(8,128)(2,1)S(1)}, u32[]{:S(2)}, u32[]{:S(2)}) collective-permute-start(bf16[264,256]{1,0:T(8,128)(2,1)S(1)} %get-tuple-element.122), channel_id=1, source_target_pairs={{0,12},{4,8},{8,4},{12,0},{16,28},{20,24},{24,20},{28,16},{1,13},{... | collective-permute-start | bytes 405512 | tf_op jit(solution)/shard_map/ppermute | solution.py:635
  73.2 21.1 %collective-permute-start.21 = (bf16[520,256]{1,0:T(8,128)(2,1)S(1)}, bf16[520,256]{1,0:T(8,128)(2,1)S(1)}, u32[]{:S(2)}, u32[]{:S(2)}) collective-permute-start(bf16[520,256]{1,0:T(8,128)(2,1)S(1)} %gather.2.refs_0_), channel_id=1, source_target_pairs={{0,16},{4,20},{8,24},{12,28},{16,0},{20,4},{24,8},{28,12},{1,17},{... | collective-permute-start | bytes 798728 | tf_op jit(solution)/shard_map/ppermute | solution.py:635
  79.2 18.4 %collective-permute-start.17 = (bf16[520,256]{1,0:T(8,128)(2,1)S(1)}, bf16[520,256]{1,0:T(8,128)(2,1)S(1)}, u32[]{:S(2)}, u32[]{:S(2)}) collective-permute-start(bf16[520,256]{1,0:T(8,128)(2,1)S(1)} %gather.3), channel_id=1, source_target_pairs={{0,16},{4,20},{8,24},{12,28},{16,0},{20,4},{24,8},{28,12},{1,17},{... | collective-permute-start | bytes 798728 | tf_op jit(solution)/shard_map/ppermute | solution.py:635
  79.2 17.7 %collective-permute-start.18 = (bf16[264,256]{1,0:T(8,128)(2,1)S(1)}, bf16[264,256]{1,0:T(8,128)(2,1)S(1)}, u32[]{:S(2)}, u32[]{:S(2)}) collective-permute-start(bf16[264,256]{1,0:T(8,128)(2,1)S(1)} %get-tuple-element.116), channel_id=1, source_target_pairs={{0,4},{4,0},{8,12},{12,8},{16,20},{20,16},{24,28},{28,24},{1,5},{5... | collective-permute-start | bytes 405512 | tf_op jit(solution)/shard_map/ppermute | solution.py:635
  80.1 16.9 %collective-permute-start.19 = (bf16[264,256]{1,0:T(8,128)(2,1)S(1)}, bf16[264,256]{1,0:T(8,128)(2,1)S(1)}, u32[]{:S(2)}, u32[]{:S(2)}) collective-permute-start(bf16[264,256]{1,0:T(8,128)(2,1)S(1)} %get-tuple-element.117), channel_id=1, source_target_pairs={{0,8},{4,12},{8,0},{12,4},{16,24},{20,28},{24,16},{28,20},{1,9},{5... | collective-permute-start | bytes 405512 | tf_op jit(solution)/shard_map/ppermute | solution.py:635
  86.1 11.5 %collective-permute-start.20 = (bf16[264,256]{1,0:T(8,128)(2,1)S(1)}, bf16[264,256]{1,0:T(8,128)(2,1)S(1)}, u32[]{:S(2)}, u32[]{:S(2)}) collective-permute-start(bf16[264,256]{1,0:T(8,128)(2,1)S(1)} %get-tuple-element.118), channel_id=1, source_target_pairs={{0,12},{4,8},{8,4},{12,0},{16,28},{20,24},{24,20},{28,16},{1,13},{... | collective-permute-start | bytes 405512 | tf_op jit(solution)/shard_map/ppermute | solution.py:635
  94.3 7.1 %collective-permute-start.32 = (bf16[512,256]{1,0:T(8,128)(2,1)S(1)}, bf16[512,256]{1,0:T(8,128)(2,1)}, u32[]{:S(2)}, u32[]{:S(2)}) collective-permute-start(bf16[512,256]{1,0:T(8,128)(2,1)S(1)} %scan.1.refs_4_.refs_0_), channel_id=1, source_target_pairs={{0,2},{1,3},{2,0},{3,1},{4,6},{5,7},{6,4},{7,5},{8,10},{9,11},{10,... | collective-permute-start | bytes 786440 | tf_op jit(solution)/shard_map/ppermute | solution.py:613
  96.9 19.0 %copy-start.1 = (bf16[2048,512]{1,0:T(8,128)(2,1)S(1)}, bf16[2048,512]{1,0:T(8,128)(2,1)}, u32[]{:S(2)}) copy-start(bf16[2048,512]{1,0:T(8,128)(2,1)} %refs_2_.1) | copy-start | bytes 6291460
  96.9 5.0 %collective-permute-start.31 = (bf16[512,256]{1,0:T(8,128)(2,1)S(1)}, bf16[512,256]{1,0:T(8,128)(2,1)S(1)}, u32[]{:S(2)}, u32[]{:S(2)}) collective-permute-start(bf16[512,256]{1,0:T(8,128)(2,1)S(1)} %scan.1.refs_4_.refs_0_), channel_id=1, source_target_pairs={{0,1},{1,0},{2,3},{3,2},{4,5},{5,4},{6,7},{7,6},{8,9},{9,8},{10,11... | collective-permute-start | bytes 786440 | tf_op jit(solution)/shard_map/ppermute | solution.py:613
  97.0 9.9 %collective-permute-start.28 = (bf16[512,256]{1,0:T(8,128)(2,1)S(1)}, bf16[512,256]{1,0:T(8,128)(2,1)S(1)}, u32[]{:S(2)}, u32[]{:S(2)}) collective-permute-start(bf16[512,256]{1,0:T(8,128)(2,1)S(1)} %combine.2.refs_4_.refs_0_), channel_id=1, source_target_pairs={{0,2},{1,3},{2,0},{3,1},{4,6},{5,7},{6,4},{7,5},{8,10},{9,11},{10,... | collective-permute-start | bytes 786440 | tf_op jit(solution)/shard_map/ppermute | solution.py:613
  98.7 13.2 %collective-permute-start.25 = (bf16[512,256]{1,0:T(8,128)(2,1)S(1)}, bf16[512,256]{1,0:T(8,128)(2,1)S(1)}, u32[]{:S(2)}, u32[]{:S(2)}) collective-permute-start(bf16[512,256]{1,0:T(8,128)(2,1)S(1)} %combine.3.refs_4_), channel_id=1, source_target_pairs={{0,2},{1,3},{2,0},{3,1},{4,6},{5,7},{6,4},{7,5},{8,10},{9,11},{10,... | collective-permute-start | bytes 786440 | tf_op jit(solution)/shard_map/ppermute | solution.py:613
  101.4 10.5 %collective-permute-start.33 = (bf16[512,256]{1,0:T(8,128)(2,1)}, bf16[512,256]{1,0:T(8,128)(2,1)}, u32[]{:S(2)}, u32[]{:S(2)}) collective-permute-start(bf16[512,256]{1,0:T(8,128)(2,1)} %collective-permute-done.32.refs_2_), channel_id=1, source_target_pairs={{0,1},{1,0},{2,3},{3,2},{4,5},{5,4},{6,7},{7,6},{8,9},{9,8},{10,11... | collective-permute-start | bytes 786440 | tf_op jit(solution)/shard_map/ppermute | solution.py:613
  101.4 14.5 %collective-permute-start.30 = (bf16[512,256]{1,0:T(8,128)(2,1)S(1)}, bf16[512,256]{1,0:T(8,128)(2,1)}, u32[]{:S(2)}, u32[]{:S(2)}) collective-permute-start(bf16[512,256]{1,0:T(8,128)(2,1)S(1)} %combine.3.refs_4_), channel_id=1, source_target_pairs={{0,1},{1,0},{2,3},{3,2},{4,5},{5,4},{6,7},{7,6},{8,9},{9,8},{10,11... | collective-permute-start | bytes 786440 | tf_op jit(solution)/shard_map/ppermute | solution.py:613
  102.6 13.3 %collective-permute-start.27 = (bf16[512,256]{1,0:T(8,128)(2,1)S(1)}, bf16[512,256]{1,0:T(8,128)(2,1)}, u32[]{:S(2)}, u32[]{:S(2)}) collective-permute-start(bf16[512,256]{1,0:T(8,128)(2,1)S(1)} %combine.2.refs_4_.refs_0_), channel_id=1, source_target_pairs={{0,1},{1,0},{2,3},{3,2},{4,5},{5,4},{6,7},{7,6},{8,9},{9,8},{10,11... | collective-permute-start | bytes 786440 | tf_op jit(solution)/shard_map/ppermute | solution.py:613
  106.9 8.9 %collective-permute-start.29 = (bf16[512,256]{1,0:T(8,128)(2,1)S(1)}, bf16[512,256]{1,0:T(8,128)(2,1)}, u32[]{:S(2)}, u32[]{:S(2)}) collective-permute-start(bf16[512,256]{1,0:T(8,128)(2,1)S(1)} %collective-permute-done.28.refs_2_), channel_id=1, source_target_pairs={{0,1},{1,0},{2,3},{3,2},{4,5},{5,4},{6,7},{7,6},{8,9},{9,8},{10,11... | collective-permute-start | bytes 786440 | tf_op jit(solution)/shard_map/ppermute | solution.py:613
  111.9 6.1 %collective-permute-start.26 = (bf16[512,256]{1,0:T(8,128)(2,1)S(1)}, bf16[512,256]{1,0:T(8,128)(2,1)}, u32[]{:S(2)}, u32[]{:S(2)}) collective-permute-start(bf16[512,256]{1,0:T(8,128)(2,1)S(1)} %collective-permute-done.25.refs_0_), channel_id=1, source_target_pairs={{0,1},{1,0},{2,3},{3,2},{4,5},{5,4},{6,7},{7,6},{8,9},{9,8},{10,11... | collective-permute-start | bytes 786440 | tf_op jit(solution)/shard_map/ppermute | solution.py:613
  (7 other events, 34.1 us)
